TPU v7x, 256 devices: a 4x2x16 block of a 4x16x16 slice. The times are simulated.
256 devices in a mesh: grp: 2 (over y), sp: 16 (over z), tp: 8 (over x, core).
Axes of the slice: x: 4, y: 2, z: 16, core: 2. Of those that a mesh axis runs over, the one named last changes fastest.
The devices are a block of a 4x16x16 slice.
Arguments:
- latent: bfloat16 [12288, 4096], P(('grp', 'sp')), parts along dimension 0, may hold values from -6 to 6
- context: bfloat16 [512, 4096], P(('grp', 'sp')), parts along dimension 0, may hold values from -6 to 6
- cond_latent: bfloat16 [8192], P('grp'), parts along dimension 0, may hold values from -6 to 6
- cond_context: bfloat16 [4096], replicated, may hold values from -6 to 6
- w_shift: bfloat16 [4096, 4096], P('sp', 'tp'), may hold values from -0.09375 to 0.09375
- w_scale: bfloat16 [4096, 4096], P('sp', 'tp'), may hold values from -0.09375 to 0.09375
- w_gate: bfloat16 [4096, 4096], P('sp', 'tp'), may hold values from -0.1875 to 0.1875
- norm_gain: float32 [4096], replicated, may hold values from 0.1 to 1.9
- w_query: bfloat16 [4096, 2048], P(None, 'tp'), may hold values from -0.09375 to 0.09375
- w_key: bfloat16 [4096, 1024], P(None, 'tp'), may hold values from -0.09375 to 0.09375
- w_value: bfloat16 [4096, 1024], P(None, 'tp'), may hold values from -0.09375 to 0.09375
- q_gain: float32 [128], replicated, may hold values from 1 to 6.5, as said below
- k_gain: float32 [128], replicated, may hold values from 1 to 6.5, as said below
- w_out: bfloat16 [2048, 4096], P('tp'), may hold values from -0.5 to 0.5
Outputs:
- mixed: bfloat16 [12288, 4096], P(('grp', 'sp', 'tp')), parts along dimension 0
There are 2 independent parts, one for each index of `grp`. A program takes and returns all parts, laid end to end along the dimension named above; an argument that names none is the same for every part. Nothing has to cross between parts.
Inputs may be any that keep to these rules, and one draw needn't show every extreme that they name: `q_gain`: positive gains. `k_gain`: positive gains.
All inputs are finite; a program needn't handle non-finite values.
Results may differ from a plain program's by a relative error of at most 0.015.
The roundings to bfloat16 on the way count: a program that leaves them out, or rounds other values in their place, can miss the bound.
Values may be sent and summed in bfloat16 or wider, within the bound.
No kernel may reach another device: no remote copies, remote signals or barrier semaphores. Data moves between devices by JAX's collectives and lax.ppermute only.
A program may use at most 128 MiB of HBM per device.

v0:
```python
import functools

import jax
import jax.numpy as jnp
from jax import lax
from jax.experimental import pallas as pl
from jax.experimental.pallas import tpu as pltpu
from jax.sharding import PartitionSpec as P


HEAD = 128
GRID_W = 64
EPS = 1e-06
CONTEXT_LIFT = 1.5
ROPE_THETA = 10000.0
SCALING = HEAD ** -0.5
LOG2E = 1.4426950408889634


BF16 = jnp.bfloat16
F32 = jnp.float32
VM = pl.BlockSpec(memory_space=pltpu.VMEM)


def rotate_rows(v, cos, sin):
    lane = lax.broadcasted_iota(jnp.int32, v.shape, 1)
    quarter = HEAD // 4
    partner = jnp.where(
        lane % (2 * quarter) < quarter,
        pltpu.roll(v, HEAD - quarter, 1),
        pltpu.roll(v, quarter, 1),
    )
    return v * cos + partner * sin


def rms_head(v, gain):
    return v * lax.rsqrt(jnp.mean(v * v, axis=-1, keepdims=True) + EPS) * gain


def modulation_kernel(lat_hbm, ctx_hbm, scale_hbm, shift_hbm, gate_hbm, out_ref, cond_ref, act_ref, w_ref, sems):
    conds = [
        pltpu.make_async_copy(c, cond_ref.at[i], sems.at[3 + i]) for i, c in enumerate((lat_hbm, ctx_hbm))
    ]
    copies = [
        pltpu.make_async_copy(w, w_ref.at[i], sems.at[i])
        for i, w in enumerate((scale_hbm, shift_hbm, gate_hbm))
    ]
    for c in conds + copies:
        c.start()
    lines = w_ref.shape[1] // 128
    first = lax.axis_index("sp") * lines
    act = []
    for i, c in enumerate(conds):
        c.wait()
        v = cond_ref[i].astype(F32)
        act_ref[i] = v * jax.nn.sigmoid(v)
        act.append(jnp.concatenate([act_ref[i, pl.ds(first + j, 1), :] for j in range(lines)], axis=1))
    act = jnp.concatenate(act, axis=0).astype(BF16)
    pieces = w_ref.shape[2] // 128
    rows, context_rows = [], []
    for i, c in enumerate(copies):
        c.wait()
        part = jnp.dot(act, w_ref[i], preferred_element_type=F32)
        near = part[0:1].astype(BF16).astype(F32)
        rows += [near, part[0:1] - near]
        if i < 2:
            context_rows.append(part[1:2])
    tile = jnp.concatenate(
        [r[:, 128 * j:128 * j + 128] for r in rows + context_rows for j in range(pieces)], axis=0
    ).astype(BF16)
    for i in range(out_ref.shape[0]):
        out_ref[i] = tile


def sum_kernel(in_ref, out_ref):
    total = in_ref[0].astype(F32)
    for i in range(1, in_ref.shape[0]):
        total = total + in_ref[i].astype(F32)
    pieces = in_ref.shape[1] // 8
    for i in range(3):
        at = 2 * i * pieces
        out_ref[i * pieces:(i + 1) * pieces, :] = total[at:at + pieces] + total[at + pieces:at + 2 * pieces]
    out_ref[3 * pieces:5 * pieces, :] = total[6 * pieces:8 * pieces]
    out_ref[5 * pieces:, :] = jnp.zeros((out_ref.shape[0] - 5 * pieces, 128), F32)


def prepare_kernel(x_ref, c_ref, rx_ref, rc_ref):
    tok, width = x_ref.shape
    step = 16

    def rows_of(src, dst, rows):
        total = jnp.zeros((step, 128), F32)
        for j in range(width // 128):
            v = src[rows, 128 * j:128 * j + 128].astype(F32)
            total = total + v * v
        r = lax.rsqrt(jnp.sum(total, axis=-1, keepdims=True) / width + EPS)
        dst[rows, :] = jnp.broadcast_to(r, (step, 128))

    @pl.loop(0, tok // step)
    def _(i):
        rows_of(x_ref, rx_ref, pl.ds(pl.multiple_of(i * step, step), step))

    for i in range(c_ref.shape[0] // step):
        rows_of(c_ref, rc_ref, pl.ds(i * step, step))


def kv_kernel(
    x_ref, c_ref, rx_ref, rc_ref, own_ref, m1_ref, m3_ref, m2_ref, gain_ref, wk_ref, wv_ref, g_ref, cos_ref, sin_ref,
    kv_ref, nm_ref, gate_ref, both_ref, mod_ref, ab_ref, w_ref,
):
    tok, width = x_ref.shape
    ctx = c_ref.shape[0]
    n_tp = lax.axis_size("tp")
    chip, core = lax.axis_index("tp") // 2, lax.axis_index("tp") % 2
    n_x = n_tp // 2
    for back, ref in ((0, own_ref), (1, m1_ref), (3, m3_ref), (2, m2_ref)):
        source = lax.rem(chip + n_x - back, n_x)
        for c in range(2):
            mod_ref[2 * source + lax.rem(core + c, 2)] = ref[c]
    pieces = width // n_tp // 128
    for t in range(n_tp):
        for p in range(pieces):
            cs = slice((t * pieces + p) * 128, (t * pieces + p + 1) * 128)
            piece = [mod_ref[t, i * pieces + p:i * pieces + p + 1, :] for i in range(5)]
            gain = gain_ref[:, cs]
            ab_ref[0:1, cs] = gain * (1.0 + piece[0])
            ab_ref[1:2, cs] = piece[1]
            gate_ref[:, cs] = piece[2]
            ab_ref[2:3, cs] = gain * (1.0 + piece[3])
            ab_ref[3:4, cs] = piece[4]

    step = 64

    @pl.loop(0, tok // step)
    def _(i):
        rows = pl.ds(pl.multiple_of(i * step, step), step)
        r = rx_ref[rows, :]
        for j in range(width // 128):
            cs = slice(128 * j, 128 * j + 128)
            v = x_ref[rows, cs].astype(F32) * r
            nm_ref[rows, cs] = (v * ab_ref[0:1, cs] + ab_ref[1:2, cs]).astype(BF16)

    r = rc_ref[...]
    for j in range(width // 128):
        cs = slice(128 * j, 128 * j + 128)
        nm_ref[tok:tok + ctx, cs] = (c_ref[:, cs].astype(F32) * r * ab_ref[2:3, cs] + ab_ref[3:4, cs]).astype(BF16)

    @pl.loop(0, w_ref.shape[0] // 256)
    def _(i):
        rows = pl.ds(pl.multiple_of(i * 256, 256), 256)
        w_ref[rows, :HEAD] = wk_ref[rows, :]
        w_ref[rows, HEAD:] = wv_ref[rows, :]

    both_ref[...] = jnp.dot(nm_ref[...], w_ref[...], preferred_element_type=F32)
    kv_ref[:, HEAD:] = both_ref[:, HEAD:].astype(BF16)
    gain = g_ref[...]
    tile = 128

    @pl.loop(0, tok // tile)
    def _(i):
        rows = pl.ds(pl.multiple_of(i * tile, tile), tile)
        k = rotate_rows(rms_head(both_ref[rows, :HEAD], gain), cos_ref[rows, :], sin_ref[rows, :])
        kv_ref[rows, :HEAD] = k.astype(BF16)

    kv_ref[tok:tok + ctx, :HEAD] = rms_head(both_ref[tok:tok + ctx, :HEAD], gain).astype(BF16)


def q_kernel(nm_ref, w_ref, g_ref, cos_ref, sin_ref, q_ref, both_ref):
    tok = cos_ref.shape[0]
    heads = w_ref.shape[1] // HEAD
    gain = g_ref[...]
    tile = 128
    both_ref[...] = jnp.dot(nm_ref[:tok, :], w_ref[...], preferred_element_type=F32)

    @pl.loop(0, tok // tile)
    def _(i):
        rows = pl.ds(pl.multiple_of(i * tile, tile), tile)
        for h in range(heads):
            v = rotate_rows(
                rms_head(both_ref[rows, h * HEAD:(h + 1) * HEAD], gain), cos_ref[rows, :], sin_ref[rows, :]
            )
            q_ref[pl.ds(pl.multiple_of(h * tok + i * tile, tile), tile), :] = v.astype(BF16)


def attend_block(q_ref, kv_refs, vt_ref, m_ref, l_ref, acc_ref, cols, tok):
    q = q_ref[cols, :]
    scores = []
    for kv_ref in kv_refs:
        s = lax.dot_general(kv_ref[:, :HEAD], q, (((1,), (1,)), ((), ())), preferred_element_type=F32)
        scores += [s[:tok], s[tok:] + CONTEXT_LIFT / SCALING]
    old = m_ref[0:1, cols]
    new = old
    for s in scores:
        new = jnp.maximum(new, jnp.max(s, axis=0, keepdims=True))
    keep = jnp.exp2((old - new) * (SCALING * LOG2E))
    m_ref[0:1, cols] = new
    total = l_ref[0:1, cols] * keep
    out = acc_ref[:, cols] * keep
    for i in range(len(kv_refs)):
        p = jnp.exp2((jnp.concatenate(scores[2 * i:2 * i + 2], axis=0) - new) * (SCALING * LOG2E))
        total = total + jnp.sum(p, axis=0, keepdims=True)
        out = out + jnp.dot(vt_ref[i], p.astype(BF16), preferred_element_type=F32)
    l_ref[0:1, cols] = total
    acc_ref[:, cols] = out


def attend_kernel(n_kv, first, last, tok, *refs):
    q_ref, kv_refs = refs[0], refs[1:1 + n_kv]
    at = 1 + n_kv
    if not first:
        m_in, l_in, acc_in = refs[at:at + 3]
        at += 3
    if last:
        out_ref = refs[at]
        at += 1
        m_ref, l_ref, acc_ref = refs[at + 1:at + 4]
        vt_ref = refs[at]
    else:
        m_ref, l_ref, acc_ref = refs[at:at + 3]
        vt_ref = refs[at + 3]
    if first:
        m_ref[...] = jnp.full(m_ref.shape, -1e30, F32)
        l_ref[...] = jnp.zeros(l_ref.shape, F32)
        acc_ref[...] = jnp.zeros(acc_ref.shape, F32)
    else:
        m_ref[...] = m_in[...]
        l_ref[...] = l_in[...]
        acc_ref[...] = acc_in[...]
    for i, kv_ref in enumerate(kv_refs):
        vt_ref[i] = jnp.transpose(kv_ref[:, HEAD:])
    queries = q_ref.shape[0]
    width = 256

    @pl.loop(0, queries // width)
    def _(i):
        cols = pl.ds(pl.multiple_of(i * width, width), width)
        attend_block(q_ref, kv_refs, vt_ref, m_ref, l_ref, acc_ref, cols, tok)

    if last:
        for h in range(queries // tok):
            cols = slice(h * tok, (h + 1) * tok)
            done = acc_ref[:, cols] / l_ref[0:1, cols]
            out_ref[:, h * HEAD:(h + 1) * HEAD] = jnp.transpose(done).astype(BF16)


def attend(q, chunks, state, tok, last=False):
    queries = q.shape[0]
    first = state is None
    shapes = [
        jax.ShapeDtypeStruct((8, queries), F32),
        jax.ShapeDtypeStruct((8, queries), F32),
        jax.ShapeDtypeStruct((HEAD, queries), F32),
    ]
    rows = sum(c.shape[0] for c in chunks)
    turned = pltpu.VMEM((len(chunks), HEAD, chunks[0].shape[0]), BF16)
    cost = pl.CostEstimate(
        flops=4 * rows * queries * HEAD, transcendentals=rows * queries, bytes_accessed=1 << 20
    )
    operands = [q, *chunks] + ([] if first else list(state))
    if last:
        return pl.pallas_call(
            functools.partial(attend_kernel, len(chunks), first, True, tok),
            out_shape=jax.ShapeDtypeStruct((tok, queries // tok * HEAD), BF16),
            in_specs=[VM] * len(operands),
            out_specs=VM,
            scratch_shapes=[turned, *[pltpu.VMEM(s.shape, s.dtype) for s in shapes]],
            cost_estimate=cost,
            compiler_params=pltpu.CompilerParams(vmem_limit_bytes=16 << 20),
            name="attend_last",
        )(*operands)
    return pl.pallas_call(
        functools.partial(attend_kernel, len(chunks), first, False, tok),
        out_shape=shapes,
        in_specs=[VM] * len(operands),
        out_specs=[VM] * 3,
        scratch_shapes=[turned],
        input_output_aliases={} if first else {1 + len(chunks) + i: i for i in range(3)},
        cost_estimate=cost,
        compiler_params=pltpu.CompilerParams(vmem_limit_bytes=16 << 20),
        name="attend",
    )(*operands)


def shifted(x, axis, by):
    n = lax.axis_size(axis)
    return lax.ppermute(x, axis, [(i, (i + by) % n) for i in range(n)])


def along_ring(x, by):
    n_sp, n_tp = lax.axis_size("sp"), lax.axis_size("tp")
    pairs = []
    for z in range(n_sp):
        for t in range(n_tp):
            to = (z + (by if t % 2 else -by)) % n_sp
            pairs.append((z * n_tp + t, to * n_tp + t))
    return lax.ppermute(x, ("sp", "tp"), pairs)


def other_core(x):
    n = lax.axis_size("tp")
    return lax.ppermute(x, "tp", [(i, i ^ 1) for i in range(n)])


def body(
    latent, context, cond_latent, cond_context, w_shift, w_scale, w_gate, norm_gain,
    w_query, w_key, w_value, q_gain, k_gain, w_out,
):
    seq_index = lax.axis_index("sp")
    n_sp = lax.axis_size("sp")
    tp_index = lax.axis_index("tp")
    mod_rows, mod_cols = w_shift.shape
    tok, width = latent.shape
    ctx = context.shape[0]

    n_tp = lax.axis_size("tp")
    pieces = mod_cols // 128
    lines = -(-5 * pieces // 8) * 8
    partial_mod = pl.pallas_call(
        modulation_kernel,
        out_shape=jax.ShapeDtypeStruct((n_sp, 8 * pieces, 128), BF16),
        in_specs=[pl.BlockSpec(memory_space=pl.ANY)] * 5,
        out_specs=VM,
        scratch_shapes=[
            pltpu.VMEM((2, width // 128, 128), BF16),
            pltpu.VMEM((2, width // 128, 128), F32),
            pltpu.VMEM((3, mod_rows, mod_cols), BF16),
            pltpu.SemaphoreType.DMA((5,)),
        ],
        compiler_params=pltpu.CompilerParams(vmem_limit_bytes=60 << 20),
        name="modulation",
    )(cond_latent.reshape(-1, 128), cond_context.reshape(-1, 128), w_scale, w_shift, w_gate)
    gathered = lax.all_to_all(partial_mod, "sp", split_axis=0, concat_axis=0, tiled=True)
    rx, rc = pl.pallas_call(
        prepare_kernel,
        out_shape=[
            jax.ShapeDtypeStruct((tok, 128), F32),
            jax.ShapeDtypeStruct((ctx, 128), F32),
        ],
        in_specs=[VM] * 2,
        out_specs=[VM] * 2,
        compiler_params=pltpu.CompilerParams(vmem_limit_bytes=32 << 20),
        cost_estimate=pl.CostEstimate(flops=1 << 30, transcendentals=0, bytes_accessed=12 << 20),
        name="prepare",
    )(latent, context)
    positions = seq_index * tok + jnp.arange(tok, dtype=jnp.int32)
    freqs = HEAD // 4
    inverse = ROPE_THETA ** (-jnp.arange(freqs, dtype=F32) / freqs)
    row = (positions // GRID_W).astype(F32)[:, None] * inverse
    col = (positions % GRID_W).astype(F32)[:, None] * inverse
    cos = jnp.concatenate([jnp.cos(row), jnp.cos(row), jnp.cos(col), jnp.cos(col)], axis=1)
    sin = jnp.concatenate([-jnp.sin(row), jnp.sin(row), -jnp.sin(col), jnp.sin(col)], axis=1)

    gathered, rx, rc, cos, sin = lax.optimization_barrier((gathered, rx, rc, cos, sin))
    summed = pl.pallas_call(
        sum_kernel,
        out_shape=jax.ShapeDtypeStruct((lines, 128), F32),
        in_specs=[VM],
        out_specs=VM,
        compiler_params=pltpu.CompilerParams(vmem_limit_bytes=8 << 20),
        cost_estimate=pl.CostEstimate(flops=8 << 30, transcendentals=0, bytes_accessed=1 << 20),
        name="sum_parts",
    )(gathered)
    pair = jnp.stack([summed, other_core(summed)])
    columns = [pair, shifted(pair, "tp", 2), shifted(pair, "tp", -2), shifted(pair, "tp", 4)]

    kv, normed, gate = pl.pallas_call(
        kv_kernel,
        out_shape=[
            jax.ShapeDtypeStruct((tok + ctx, 2 * HEAD), BF16),
            jax.ShapeDtypeStruct((tok + ctx, width), BF16),
            jax.ShapeDtypeStruct((1, width), F32),
        ],
        in_specs=[VM] * 14,
        out_specs=[VM] * 3,
        scratch_shapes=[
            pltpu.VMEM((tok + ctx, 2 * HEAD), F32),
            pltpu.VMEM((n_tp, lines, 128), F32),
            pltpu.VMEM((8, width), F32),
            pltpu.VMEM((width, 2 * HEAD), BF16),
        ],
        cost_estimate=pl.CostEstimate(flops=2 * tok * width * 256, transcendentals=0, bytes_accessed=1 << 22),
        compiler_params=pltpu.CompilerParams(vmem_limit_bytes=24 << 20),
        name="project_kv",
    )(
        latent, context, rx, rc, *columns, norm_gain.reshape(1, width), w_key, w_value, k_gain.reshape(1, HEAD),
        cos, sin,
    )

    right, left = along_ring(kv, 1), along_ring(kv, -1)
    q = pl.pallas_call(
        q_kernel,
        out_shape=jax.ShapeDtypeStruct((w_query.shape[1] // HEAD * tok, HEAD), BF16),
        in_specs=[VM] * 5,
        out_specs=VM,
        scratch_shapes=[pltpu.VMEM((tok, w_query.shape[1]), F32)],
        cost_estimate=pl.CostEstimate(flops=2 * tok * width * 256, transcendentals=0, bytes_accessed=1 << 22),
        compiler_params=pltpu.CompilerParams(vmem_limit_bytes=24 << 20),
        name="project_q",
    )(normed, w_query, q_gain.reshape(1, HEAD), cos, sin)
    state = attend(q, [kv], None, tok)
    half = n_sp // 2
    for step in range(1, half):
        right, m = lax.optimization_barrier((right, state[0]))
        left, m = lax.optimization_barrier((left, m))
        state = [m, *state[1:]]
        now = [right, left]
        right = along_ring(right, 1)
        if step + 1 < half:
            left = along_ring(left, -1)
        state = attend(q, now, state, tok)
    attended = attend(q, [right], state, tok, last=True)

    n_x = lax.axis_size("tp") // 2
    core, chip = tp_index % 2, tp_index // 2
    share = tok // (2 * n_x)
    parts = attended.reshape(n_x, 2, share, attended.shape[1])
    parts = jnp.concatenate([parts, parts], axis=0)
    parts = lax.dynamic_slice_in_dim(parts, chip, n_x, 0)
    mine = lax.dynamic_index_in_dim(parts, core, 1, keepdims=False)
    theirs = lax.dynamic_index_in_dim(parts, 1 - core, 1, keepdims=False)
    far, near = (2,), (1, 3, 0)

    def product(side, which):
        rows = jnp.concatenate([side[i] for i in which]) if len(which) > 1 else side[which[0]]
        return jnp.dot(rows, w_out, preferred_element_type=F32)

    far_sent = other_core(product(theirs, far).astype(BF16))
    far_sum = (product(mine, far) + far_sent.astype(F32)).astype(BF16)
    theirs, far_sum = lax.optimization_barrier((theirs, far_sum))
    near_sent = other_core(product(theirs, near).astype(BF16))
    h = width // 2
    from_left = shifted(far_sum[:, :h], "tp", 2)
    from_right = shifted(far_sum[:, h:], "tp", -2)
    near_sum = product(mine, near) + near_sent.astype(F32)
    nxt, prv, own = (near_sum[i * share:(i + 1) * share] for i in range(3))
    halves = (nxt[:, h:].astype(BF16), prv[:, :h].astype(BF16))
    a1 = shifted(halves[0], "tp", 2)
    b0 = shifted(halves[1], "tp", -2)
    joined = ((nxt[:, :h] + from_left.astype(F32)).astype(BF16), (prv[:, h:] + from_right.astype(F32)).astype(BF16))
    a0 = shifted(joined[0], "tp", 2)
    b1 = shifted(joined[1], "tp", -2)
    own, a0, a1, b0, b1 = lax.optimization_barrier((own, a0, a1, b0, b1))
    left_half = own[:, :h] + a0.astype(F32) + b0.astype(F32)
    right_half = own[:, h:] + a1.astype(F32) + b1.astype(F32)
    return (gate * jnp.concatenate([left_half, right_half], axis=1)).astype(BF16)


def solution(mesh):
    placed = (
        P(("grp", "sp"), None),
        P(("grp", "sp"), None),
        P("grp"),
        P(),
        P("sp", "tp"),
        P("sp", "tp"),
        P("sp", "tp"),
        P(),
        P(None, "tp"),
        P(None, "tp"),
        P(None, "tp"),
        P(),
        P(),
        P("tp", None),
    )
    return jax.shard_map(
        body, mesh=mesh, in_specs=placed, out_specs=P(("grp", "sp", "tp"), None), check_vma=False
    )
```

profile of v0, /device:TPU:40, one launch (start us, length us, event | category | flops | bytes accessed | tf_op | source)
XLA Modules:
  0.0 142.0 jit_solution(5756215331920349822)
XLA Ops:
  2.3 24.0 %all-to-all-start = ((bf16[16,32,128]{2,1,0:T(8,128)(2,1)}), bf16[16,32,128]{2,1,0:T(8,128)(2,1)S(1)}, u32[]{:S(2)}, u32[]{:S(2)}) async-start(bf16[16,32,128]{2,1,0:T(8,128)(2,1)} %modulation.1), calls=%async_computation | async-start | bytes 262144 | tf_op jit(solution)/shard_map/all_to_all | solution.py:332
  29.1 3.0 %prepare.1 = (f32[384,128]{1,0:T(8,128)S(1)}, f32[16,128]{1,0:T(8,128)S(1)}) custom-call(bf16[384,4096]{1,0:T(8,128)(2,1)S(1)} %copy-done.1, bf16[16,4096]{1,0:T(8,128)(2,1)S(1)} %copy-done.6), custom_call_target="tpu_custom_call" | custom-call | flops 1073741824 | bytes 12582912 | tf_op jit(solution)/shard_map/prepare/pallas_call | solution.py:333
  34.1 6.9 %all-to-all-done.in_ref = bf16[16,32,128]{2,1,0:T(8,128)(2,1)S(1)} async-done(((bf16[16,32,128]{2,1,0:T(8,128)(2,1)}), bf16[16,32,128]{2,1,0:T(8,128)(2,1)S(1)}, u32[]{:S(2)}, u32[]{:S(2)}) %all-to-all-start) | async-done | bytes 131104 | tf_op jit(solution)/shard_map/all_to_all | solution.py:332
  42.3 3.3 %collective-permute-start.3 = (f32[2,24,128]{2,1,0:T(8,128)S(1)}, f32[2,24,128]{2,1,0:T(8,128)S(1)}, u32[]{:S(2)}, u32[]{:S(2)}) collective-permute-start(f32[2,24,128]{2,1,0:T(8,128)S(1)} %pad_maximum_fusion.2.own_ref), channel_id=1, source_target_pairs={{0,4},{1,5},{2,6},{3,7},{4,0},{5,1},{6,2},{7,3},{8,12},{9,13},{10,... | collective-permute-start | bytes 73736 | tf_op jit(solution)/shard_map/ppermute | solution.py:286
  51.7 3.4 %project_kv.1 = (bf16[400,256]{1,0:T(8,128)(2,1)S(1)}, bf16[400,4096]{1,0:T(8,128)(2,1)S(1)}, f32[1,4096]{1,0:T(1,128)S(1)}) custom-call(bf16[384,4096]{1,0:T(8,128)(2,1)S(1)} %copy-done.2, bf16[16,4096]{1,0:T(8,128)(2,1)S(1)} %copy-done.7, f32[384,128]{1,0:T(8,128)S(1)} %get-tuple-element.76.rx_ref, f32[16,128]{1,0:T(8,128)S(1)} %get-tuple-element.77.rc_ref, ...), custom_call_target="tpu_custom_call" | custom-call | flops 805306368 | bytes 4194304 | tf_op jit(solution)/shard_map/project_kv/pallas_call | solution.py:366
  55.1 2.4 %collective-permute-start.4 = (bf16[400,256]{1,0:T(8,128)(2,1)S(1)}, bf16[400,256]{1,0:T(8,128)(2,1)S(1)}, u32[]{:S(2)}, u32[]{:S(2)}) collective-permute-start(bf16[400,256]{1,0:T(8,128)(2,1)S(1)} %get-tuple-element.83.refs_1_), channel_id=1, source_target_pairs={{0,120},{1,9},{2,122},{3,11},{4,124},{5,13},{6,126},{7,15},{8,0},{... | collective-permute-start | bytes 614408 | tf_op jit(solution)/shard_map/ppermute | solution.py:296
  61.9 2.9 %collective-permute-start.5 = (bf16[400,256]{1,0:T(8,128)(2,1)S(1)}, bf16[400,256]{1,0:T(8,128)(2,1)S(1)}, u32[]{:S(2)}, u32[]{:S(2)}) collective-permute-start(bf16[400,256]{1,0:T(8,128)(2,1)S(1)} %collective-permute-done.4.refs_1_), channel_id=1, source_target_pairs={{0,120},{1,9},{2,122},{3,11},{4,124},{5,13},{6,126},{7,15},{8,0},{... | collective-permute-start | bytes 614408 | tf_op jit(solution)/shard_map/ppermute | solution.py:296
  65.4 2.3 %attend.9 = (f32[8,768]{1,0:T(8,128)S(1)}, f32[8,768]{1,0:T(8,128)S(1)}, f32[128,768]{1,0:T(8,128)S(1)}) custom-call(bf16[768,128]{1,0:T(8,128)(2,1)S(1)} %project_q.1.refs_0_, bf16[400,256]{1,0:T(8,128)(2,1)S(1)} %collective-permute-done.4.refs_1_, ...), custom_call_target="tpu_custom_call", output_to_operand_aliasing={{0}: (3, {}), {1}: (4, {}), {2}: (5, {})} | custom-call | flops 314572800 | bytes 1048576 | tf_op jit(solution)/shard_map/attend/pallas_call | solution.py:271
  68.0 3.7 %collective-permute-start.7 = (bf16[400,256]{1,0:T(8,128)(2,1)S(1)}, bf16[400,256]{1,0:T(8,128)(2,1)S(1)}, u32[]{:S(2)}, u32[]{:S(2)}) collective-permute-start(bf16[400,256]{1,0:T(8,128)(2,1)S(1)} %collective-permute-done.5.refs_1_), channel_id=1, source_target_pairs={{0,120},{1,9},{2,122},{3,11},{4,124},{5,13},{6,126},{7,15},{8,0},{... | collective-permute-start | bytes 614408 | tf_op jit(solution)/shard_map/ppermute | solution.py:296
  71.7 2.6 %collective-permute-done.8.refs_2_ = bf16[400,256]{1,0:T(8,128)(2,1)S(1)} collective-permute-done((bf16[400,256]{1,0:T(8,128)(2,1)S(1)}, bf16[400,256]{1,0:T(8,128)(2,1)S(1)}, u32[]{:S(2)}, u32[]{:S(2)}) %collective-permute-start.8) | collective-permute-done | bytes 204832 | tf_op jit(solution)/shard_map/ppermute | solution.py:296
  74.4 2.3 %attend.10 = (f32[8,768]{1,0:T(8,128)S(1)}, f32[8,768]{1,0:T(8,128)S(1)}, f32[128,768]{1,0:T(8,128)S(1)}) custom-call(bf16[768,128]{1,0:T(8,128)(2,1)S(1)} %project_q.1.refs_0_, bf16[400,256]{1,0:T(8,128)(2,1)S(1)} %collective-permute-done.5.refs_1_, ...), custom_call_target="tpu_custom_call", output_to_operand_aliasing={{0}: (3, {}), {1}: (4, {}), {2}: (5, {})} | custom-call | flops 314572800 | bytes 1048576 | tf_op jit(solution)/shard_map/attend/pallas_call | solution.py:271
  76.7 3.4 %collective-permute-start.9 = (bf16[400,256]{1,0:T(8,128)(2,1)S(1)}, bf16[400,256]{1,0:T(8,128)(2,1)S(1)}, u32[]{:S(2)}, u32[]{:S(2)}) collective-permute-start(bf16[400,256]{1,0:T(8,128)(2,1)S(1)} %collective-permute-done.7.refs_1_), channel_id=1, source_target_pairs={{0,120},{1,9},{2,122},{3,11},{4,124},{5,13},{6,126},{7,15},{8,0},{... | collective-permute-start | bytes 614408 | tf_op jit(solution)/shard_map/ppermute | solution.py:296
  80.1 2.6 %collective-permute-done.10.refs_2_ = bf16[400,256]{1,0:T(8,128)(2,1)S(1)} collective-permute-done((bf16[400,256]{1,0:T(8,128)(2,1)S(1)}, bf16[400,256]{1,0:T(8,128)(2,1)S(1)}, u32[]{:S(2)}, u32[]{:S(2)}) %collective-permute-start.10) | collective-permute-done | bytes 204832 | tf_op jit(solution)/shard_map/ppermute | solution.py:296
  82.7 2.3 %attend.11 = (f32[8,768]{1,0:T(8,128)S(1)}, f32[8,768]{1,0:T(8,128)S(1)}, f32[128,768]{1,0:T(8,128)S(1)}) custom-call(bf16[768,128]{1,0:T(8,128)(2,1)S(1)} %project_q.1.refs_0_, bf16[400,256]{1,0:T(8,128)(2,1)S(1)} %collective-permute-done.7.refs_1_, ...), custom_call_target="tpu_custom_call", output_to_operand_aliasing={{0}: (3, {}), {1}: (4, {}), {2}: (5, {})} | custom-call | flops 314572800 | bytes 1048576 | tf_op jit(solution)/shard_map/attend/pallas_call | solution.py:271
  85.1 3.3 %collective-permute-start.11 = (bf16[400,256]{1,0:T(8,128)(2,1)S(1)}, bf16[400,256]{1,0:T(8,128)(2,1)S(1)}, u32[]{:S(2)}, u32[]{:S(2)}) collective-permute-start(bf16[400,256]{1,0:T(8,128)(2,1)S(1)} %collective-permute-done.9.refs_1_), channel_id=1, source_target_pairs={{0,120},{1,9},{2,122},{3,11},{4,124},{5,13},{6,126},{7,15},{8,0},{... | collective-permute-start | bytes 614408 | tf_op jit(solution)/shard_map/ppermute | solution.py:296
  90.1 2.3 %attend.12 = (f32[8,768]{1,0:T(8,128)S(1)}, f32[8,768]{1,0:T(8,128)S(1)}, f32[128,768]{1,0:T(8,128)S(1)}) custom-call(bf16[768,128]{1,0:T(8,128)(2,1)S(1)} %project_q.1.refs_0_, bf16[400,256]{1,0:T(8,128)(2,1)S(1)} %collective-permute-done.9.refs_1_, ...), custom_call_target="tpu_custom_call", output_to_operand_aliasing={{0}: (3, {}), {1}: (4, {}), {2}: (5, {})} | custom-call | flops 314572800 | bytes 1048576 | tf_op jit(solution)/shard_map/attend/pallas_call | solution.py:271
  92.5 3.3 %collective-permute-start.13 = (bf16[400,256]{1,0:T(8,128)(2,1)S(1)}, bf16[400,256]{1,0:T(8,128)(2,1)S(1)}, u32[]{:S(2)}, u32[]{:S(2)}) collective-permute-start(bf16[400,256]{1,0:T(8,128)(2,1)S(1)} %collective-permute-done.11.refs_1_), channel_id=1, source_target_pairs={{0,120},{1,9},{2,122},{3,11},{4,124},{5,13},{6,126},{7,15},{8,0},{... | collective-permute-start | bytes 614408 | tf_op jit(solution)/shard_map/ppermute | solution.py:296
  97.1 2.3 %attend.13 = (f32[8,768]{1,0:T(8,128)S(1)}, f32[8,768]{1,0:T(8,128)S(1)}, f32[128,768]{1,0:T(8,128)S(1)}) custom-call(bf16[768,128]{1,0:T(8,128)(2,1)S(1)} %project_q.1.refs_0_, bf16[400,256]{1,0:T(8,128)(2,1)S(1)} %collective-permute-done.11.refs_1_, ...), custom_call_target="tpu_custom_call", output_to_operand_aliasing={{0}: (3, {}), {1}: (4, {}), {2}: (5, {})} | custom-call | flops 314572800 | bytes 1048576 | tf_op jit(solution)/shard_map/attend/pallas_call | solution.py:271
  100.7 3.7 %collective-permute-start.15 = (bf16[400,256]{1,0:T(8,128)(2,1)S(1)}, bf16[400,256]{1,0:T(8,128)(2,1)S(1)}, u32[]{:S(2)}, u32[]{:S(2)}) collective-permute-start(bf16[400,256]{1,0:T(8,128)(2,1)S(1)} %collective-permute-done.13.refs_1_), channel_id=1, source_target_pairs={{0,120},{1,9},{2,122},{3,11},{4,124},{5,13},{6,126},{7,15},{8,0},{... | collective-permute-start | bytes 614408 | tf_op jit(solution)/shard_map/ppermute | solution.py:296
  104.4 2.3 %attend.14 = (f32[8,768]{1,0:T(8,128)S(1)}, f32[8,768]{1,0:T(8,128)S(1)}, f32[128,768]{1,0:T(8,128)S(1)}) custom-call(bf16[768,128]{1,0:T(8,128)(2,1)S(1)} %project_q.1.refs_0_, bf16[400,256]{1,0:T(8,128)(2,1)S(1)} %collective-permute-done.13.refs_1_, ...), custom_call_target="tpu_custom_call", output_to_operand_aliasing={{0}: (3, {}), {1}: (4, {}), {2}: (5, {})} | custom-call | flops 314572800 | bytes 1048576 | tf_op jit(solution)/shard_map/attend/pallas_call | solution.py:271
  107.7 3.7 %collective-permute-start.17 = (bf16[400,256]{1,0:T(8,128)(2,1)S(1)}, bf16[400,256]{1,0:T(8,128)(2,1)S(1)}, u32[]{:S(2)}, u32[]{:S(2)}) collective-permute-start(bf16[400,256]{1,0:T(8,128)(2,1)S(1)} %collective-permute-done.15.refs_1_), channel_id=1, source_target_pairs={{0,120},{1,9},{2,122},{3,11},{4,124},{5,13},{6,126},{7,15},{8,0},{... | collective-permute-start | bytes 614408 | tf_op jit(solution)/shard_map/ppermute | solution.py:296
  111.5 3.3 %attend.15 = (f32[8,768]{1,0:T(8,128)S(1)}, f32[8,768]{1,0:T(8,128)S(1)}, f32[128,768]{1,0:T(8,128)S(1)}) custom-call(bf16[768,128]{1,0:T(8,128)(2,1)S(1)} %project_q.1.refs_0_, bf16[400,256]{1,0:T(8,128)(2,1)S(1)} %collective-permute-done.15.refs_1_, ...), custom_call_target="tpu_custom_call", output_to_operand_aliasing={{0}: (3, {}), {1}: (4, {}), {2}: (5, {})} | custom-call | flops 314572800 | bytes 1048576 | tf_op jit(solution)/shard_map/attend/pallas_call | solution.py:271
  123.6 4.0 %collective-permute-done.25 = bf16[48,2048]{1,0:T(8,128)(2,1)S(1)} collective-permute-done((bf16[48,2048]{1,0:T(8,128)(2,1)S(1)}, bf16[48,2048]{1,0:T(8,128)(2,1)S(1)}, u32[]{:S(2)}, u32[]{:S(2)}) %collective-permute-start.25) | collective-permute-done | bytes 196640 | tf_op jit(solution)/shard_map/ppermute | solution.py:286
  133.3 3.7 %collective-permute-done.26 = bf16[48,2048]{1,0:T(8,128)(2,1)S(1)} collective-permute-done((bf16[48,2048]{1,0:T(8,128)(2,1)S(1)}, bf16[48,2048]{1,0:T(8,128)(2,1)S(1)}, u32[]{:S(2)}, u32[]{:S(2)}) %collective-permute-start.26) | collective-permute-done | bytes 196640 | tf_op jit(solution)/shard_map/ppermute | solution.py:286
  (87 shorter events, 44.5 us)
Async XLA Ops:
  2.3 38.6 %all-to-all-start = ((bf16[16,32,128]{2,1,0:T(8,128)(2,1)}), bf16[16,32,128]{2,1,0:T(8,128)(2,1)S(1)}, u32[]{:S(2)}, u32[]{:S(2)}) async-start(bf16[16,32,128]{2,1,0:T(8,128)(2,1)} %modulation.1), calls=%async_computation | async-start | bytes 262144 | tf_op jit(solution)/shard_map/all_to_all | solution.py:332
  42.3 5.3 %collective-permute-start.3 = (f32[2,24,128]{2,1,0:T(8,128)S(1)}, f32[2,24,128]{2,1,0:T(8,128)S(1)}, u32[]{:S(2)}, u32[]{:S(2)}) collective-permute-start(f32[2,24,128]{2,1,0:T(8,128)S(1)} %pad_maximum_fusion.2.own_ref), channel_id=1, source_target_pairs={{0,4},{1,5},{2,6},{3,7},{4,0},{5,1},{6,2},{7,3},{8,12},{9,13},{10,... | collective-permute-start | bytes 73736 | tf_op jit(solution)/shard_map/ppermute | solution.py:286
  46.6 5.0 %collective-permute-start.1 = (f32[2,24,128]{2,1,0:T(8,128)S(1)}, f32[2,24,128]{2,1,0:T(8,128)S(1)}, u32[]{:S(2)}, u32[]{:S(2)}) collective-permute-start(f32[2,24,128]{2,1,0:T(8,128)S(1)} %pad_maximum_fusion.2.own_ref), channel_id=1, source_target_pairs={{0,2},{1,3},{2,4},{3,5},{4,6},{5,7},{6,0},{7,1},{8,10},{9,11},{10,... | collective-permute-start | bytes 73736 | tf_op jit(solution)/shard_map/ppermute | solution.py:286
  55.1 6.8 %collective-permute-start.4 = (bf16[400,256]{1,0:T(8,128)(2,1)S(1)}, bf16[400,256]{1,0:T(8,128)(2,1)S(1)}, u32[]{:S(2)}, u32[]{:S(2)}) collective-permute-start(bf16[400,256]{1,0:T(8,128)(2,1)S(1)} %get-tuple-element.83.refs_1_), channel_id=1, source_target_pairs={{0,120},{1,9},{2,122},{3,11},{4,124},{5,13},{6,126},{7,15},{8,0},{... | collective-permute-start | bytes 614408 | tf_op jit(solution)/shard_map/ppermute | solution.py:296
  57.5 7.9 %collective-permute-start.6 = (bf16[400,256]{1,0:T(8,128)(2,1)S(1)}, bf16[400,256]{1,0:T(8,128)(2,1)S(1)}, u32[]{:S(2)}, u32[]{:S(2)}) collective-permute-start(bf16[400,256]{1,0:T(8,128)(2,1)S(1)} %get-tuple-element.83.refs_1_), channel_id=1, source_target_pairs={{0,8},{1,121},{2,10},{3,123},{4,12},{5,125},{6,14},{7,127},{8,16},... | collective-permute-start | bytes 614408 | tf_op jit(solution)/shard_map/ppermute | solution.py:296
  61.9 6.2 %collective-permute-start.5 = (bf16[400,256]{1,0:T(8,128)(2,1)S(1)}, bf16[400,256]{1,0:T(8,128)(2,1)S(1)}, u32[]{:S(2)}, u32[]{:S(2)}) collective-permute-start(bf16[400,256]{1,0:T(8,128)(2,1)S(1)} %collective-permute-done.4.refs_1_), channel_id=1, source_target_pairs={{0,120},{1,9},{2,122},{3,11},{4,124},{5,13},{6,126},{7,15},{8,0},{... | collective-permute-start | bytes 614408 | tf_op jit(solution)/shard_map/ppermute | solution.py:296
  65.4 9.0 %collective-permute-start.8 = (bf16[400,256]{1,0:T(8,128)(2,1)S(1)}, bf16[400,256]{1,0:T(8,128)(2,1)S(1)}, u32[]{:S(2)}, u32[]{:S(2)}) collective-permute-start(bf16[400,256]{1,0:T(8,128)(2,1)S(1)} %collective-permute-done.6.refs_2_), channel_id=1, source_target_pairs={{0,8},{1,121},{2,10},{3,123},{4,12},{5,125},{6,14},{7,127},{8,16},... | collective-permute-start | bytes 614408 | tf_op jit(solution)/shard_map/ppermute | solution.py:296
  68.0 8.7 %collective-permute-start.7 = (bf16[400,256]{1,0:T(8,128)(2,1)S(1)}, bf16[400,256]{1,0:T(8,128)(2,1)S(1)}, u32[]{:S(2)}, u32[]{:S(2)}) collective-permute-start(bf16[400,256]{1,0:T(8,128)(2,1)S(1)} %collective-permute-done.5.refs_1_), channel_id=1, source_target_pairs={{0,120},{1,9},{2,122},{3,11},{4,124},{5,13},{6,126},{7,15},{8,0},{... | collective-permute-start | bytes 614408 | tf_op jit(solution)/shard_map/ppermute | solution.py:296
  74.4 8.3 %collective-permute-start.10 = (bf16[400,256]{1,0:T(8,128)(2,1)S(1)}, bf16[400,256]{1,0:T(8,128)(2,1)S(1)}, u32[]{:S(2)}, u32[]{:S(2)}) collective-permute-start(bf16[400,256]{1,0:T(8,128)(2,1)S(1)} %collective-permute-done.8.refs_2_), channel_id=1, source_target_pairs={{0,8},{1,121},{2,10},{3,123},{4,12},{5,125},{6,14},{7,127},{8,16},... | collective-permute-start | bytes 614408 | tf_op jit(solution)/shard_map/ppermute | solution.py:296
  76.7 8.3 %collective-permute-start.9 = (bf16[400,256]{1,0:T(8,128)(2,1)S(1)}, bf16[400,256]{1,0:T(8,128)(2,1)S(1)}, u32[]{:S(2)}, u32[]{:S(2)}) collective-permute-start(bf16[400,256]{1,0:T(8,128)(2,1)S(1)} %collective-permute-done.7.refs_1_), channel_id=1, source_target_pairs={{0,120},{1,9},{2,122},{3,11},{4,124},{5,13},{6,126},{7,15},{8,0},{... | collective-permute-start | bytes 614408 | tf_op jit(solution)/shard_map/ppermute | solution.py:296
  82.7 7.5 %collective-permute-start.12 = (bf16[400,256]{1,0:T(8,128)(2,1)S(1)}, bf16[400,256]{1,0:T(8,128)(2,1)S(1)}, u32[]{:S(2)}, u32[]{:S(2)}) collective-permute-start(bf16[400,256]{1,0:T(8,128)(2,1)S(1)} %collective-permute-done.10.refs_2_), channel_id=1, source_target_pairs={{0,8},{1,121},{2,10},{3,123},{4,12},{5,125},{6,14},{7,127},{8,16},... | collective-permute-start | bytes 614408 | tf_op jit(solution)/shard_map/ppermute | solution.py:296
  85.1 7.4 %collective-permute-start.11 = (bf16[400,256]{1,0:T(8,128)(2,1)S(1)}, bf16[400,256]{1,0:T(8,128)(2,1)S(1)}, u32[]{:S(2)}, u32[]{:S(2)}) collective-permute-start(bf16[400,256]{1,0:T(8,128)(2,1)S(1)} %collective-permute-done.9.refs_1_), channel_id=1, source_target_pairs={{0,120},{1,9},{2,122},{3,11},{4,124},{5,13},{6,126},{7,15},{8,0},{... | collective-permute-start | bytes 614408 | tf_op jit(solution)/shard_map/ppermute | solution.py:296
  90.1 7.0 %collective-permute-start.14 = (bf16[400,256]{1,0:T(8,128)(2,1)S(1)}, bf16[400,256]{1,0:T(8,128)(2,1)S(1)}, u32[]{:S(2)}, u32[]{:S(2)}) collective-permute-start(bf16[400,256]{1,0:T(8,128)(2,1)S(1)} %collective-permute-done.12.refs_2_), channel_id=1, source_target_pairs={{0,8},{1,121},{2,10},{3,123},{4,12},{5,125},{6,14},{7,127},{8,16},... | collective-permute-start | bytes 614408 | tf_op jit(solution)/shard_map/ppermute | solution.py:296
  92.5 8.2 %collective-permute-start.13 = (bf16[400,256]{1,0:T(8,128)(2,1)S(1)}, bf16[400,256]{1,0:T(8,128)(2,1)S(1)}, u32[]{:S(2)}, u32[]{:S(2)}) collective-permute-start(bf16[400,256]{1,0:T(8,128)(2,1)S(1)} %collective-permute-done.11.refs_1_), channel_id=1, source_target_pairs={{0,120},{1,9},{2,122},{3,11},{4,124},{5,13},{6,126},{7,15},{8,0},{... | collective-permute-start | bytes 614408 | tf_op jit(solution)/shard_map/ppermute | solution.py:296
  97.1 7.3 %collective-permute-start.16 = (bf16[400,256]{1,0:T(8,128)(2,1)S(1)}, bf16[400,256]{1,0:T(8,128)(2,1)S(1)}, u32[]{:S(2)}, u32[]{:S(2)}) collective-permute-start(bf16[400,256]{1,0:T(8,128)(2,1)S(1)} %collective-permute-done.14.refs_2_), channel_id=1, source_target_pairs={{0,8},{1,121},{2,10},{3,123},{4,12},{5,125},{6,14},{7,127},{8,16},... | collective-permute-start | bytes 614408 | tf_op jit(solution)/shard_map/ppermute | solution.py:296
  100.7 7.0 %collective-permute-start.15 = (bf16[400,256]{1,0:T(8,128)(2,1)S(1)}, bf16[400,256]{1,0:T(8,128)(2,1)S(1)}, u32[]{:S(2)}, u32[]{:S(2)}) collective-permute-start(bf16[400,256]{1,0:T(8,128)(2,1)S(1)} %collective-permute-done.13.refs_1_), channel_id=1, source_target_pairs={{0,120},{1,9},{2,122},{3,11},{4,124},{5,13},{6,126},{7,15},{8,0},{... | collective-permute-start | bytes 614408 | tf_op jit(solution)/shard_map/ppermute | solution.py:296
  104.4 7.1 %collective-permute-start.18 = (bf16[400,256]{1,0:T(8,128)(2,1)S(1)}, bf16[400,256]{1,0:T(8,128)(2,1)}, u32[]{:S(2)}, u32[]{:S(2)}) collective-permute-start(bf16[400,256]{1,0:T(8,128)(2,1)S(1)} %collective-permute-done.16.refs_2_), channel_id=1, source_target_pairs={{0,8},{1,121},{2,10},{3,123},{4,12},{5,125},{6,14},{7,127},{8,16},... | collective-permute-start | bytes 614408 | tf_op jit(solution)/shard_map/ppermute | solution.py:296
  107.7 7.1 %collective-permute-start.17 = (bf16[400,256]{1,0:T(8,128)(2,1)S(1)}, bf16[400,256]{1,0:T(8,128)(2,1)S(1)}, u32[]{:S(2)}, u32[]{:S(2)}) collective-permute-start(bf16[400,256]{1,0:T(8,128)(2,1)S(1)} %collective-permute-done.15.refs_1_), channel_id=1, source_target_pairs={{0,120},{1,9},{2,122},{3,11},{4,124},{5,13},{6,126},{7,15},{8,0},{... | collective-permute-start | bytes 614408 | tf_op jit(solution)/shard_map/ppermute | solution.py:296
  120.3 7.3 %collective-permute-start.25 = (bf16[48,2048]{1,0:T(8,128)(2,1)S(1)}, bf16[48,2048]{1,0:T(8,128)(2,1)S(1)}, u32[]{:S(2)}, u32[]{:S(2)}) collective-permute-start(bf16[48,2048]{1,0:T(8,128)(2,1)S(1)} %get-tuple-element.149), channel_id=1, source_target_pairs={{0,6},{1,7},{2,0},{3,1},{4,2},{5,3},{6,4},{7,5},{8,14},{9,15},{10,... | collective-permute-start | bytes 589832 | tf_op jit(solution)/shard_map/ppermute | solution.py:286
  120.5 8.5 %collective-permute-start.21 = (bf16[48,2048]{1,0:T(8,128)(2,1)S(1)}, bf16[48,2048]{1,0:T(8,128)(2,1)S(1)}, u32[]{:S(2)}, u32[]{:S(2)}) collective-permute-start(bf16[48,2048]{1,0:T(8,128)(2,1)S(1)} %get-tuple-element.150), channel_id=1, source_target_pairs={{0,2},{1,3},{2,4},{3,5},{4,6},{5,7},{6,0},{7,1},{8,10},{9,11},{10,... | collective-permute-start | bytes 589832 | tf_op jit(solution)/shard_map/ppermute | solution.py:286
  129.0 7.9 %collective-permute-start.26 = (bf16[48,2048]{1,0:T(8,128)(2,1)S(1)}, bf16[48,2048]{1,0:T(8,128)(2,1)S(1)}, u32[]{:S(2)}, u32[]{:S(2)}) collective-permute-start(bf16[48,2048]{1,0:T(8,128)(2,1)S(1)} %get-tuple-element.143), channel_id=1, source_target_pairs={{0,6},{1,7},{2,0},{3,1},{4,2},{5,3},{6,4},{7,5},{8,14},{9,15},{10,... | collective-permute-start | bytes 589832 | tf_op jit(solution)/shard_map/ppermute | solution.py:286
  129.3 9.0 %collective-permute-start.22 = (bf16[48,2048]{1,0:T(8,128)(2,1)S(1)}, bf16[48,2048]{1,0:T(8,128)(2,1)S(1)}, u32[]{:S(2)}, u32[]{:S(2)}) collective-permute-start(bf16[48,2048]{1,0:T(8,128)(2,1)S(1)} %get-tuple-element.144), channel_id=1, source_target_pairs={{0,2},{1,3},{2,4},{3,5},{4,6},{5,7},{6,0},{7,1},{8,10},{9,11},{10,... | collective-permute-start | bytes 589832 | tf_op jit(solution)/shard_map/ppermute | solution.py:286
  131.2 8.5 %collective-permute-start.24 = (bf16[48,2048]{1,0:T(8,128)(2,1)S(1)}, bf16[48,2048]{1,0:T(8,128)(2,1)S(1)}, u32[]{:S(2)}, u32[]{:S(2)}) collective-permute-start(bf16[48,2048]{1,0:T(8,128)(2,1)S(1)} %get-tuple-element.145), channel_id=1, source_target_pairs={{0,6},{1,7},{2,0},{3,1},{4,2},{5,3},{6,4},{7,5},{8,14},{9,15},{10,... | collective-permute-start | bytes 589832 | tf_op jit(solution)/shard_map/ppermute | solution.py:286
  132.6 8.5 %collective-permute-start.23 = (bf16[48,2048]{1,0:T(8,128)(2,1)S(1)}, bf16[48,2048]{1,0:T(8,128)(2,1)S(1)}, u32[]{:S(2)}, u32[]{:S(2)}) collective-permute-start(bf16[48,2048]{1,0:T(8,128)(2,1)S(1)} %get-tuple-element.146), channel_id=1, source_target_pairs={{0,2},{1,3},{2,4},{3,5},{4,6},{5,7},{6,0},{7,1},{8,10},{9,11},{10,... | collective-permute-start | bytes 589832 | tf_op jit(solution)/shard_map/ppermute | solution.py:286
  (15 other events, 205.3 us)
where the time goes:
time: 142 us
  starting transfers between devices  62.5 us (44%)
  waiting for transfers between devices  40.1 us (28%)
  Pallas kernels  31 us (22%)
  other arithmetic  3.01 us (2%)
  local copies, waits for them, and re-layouts  2.95 us (2%)
  matrix products  2.01 us (1%)
    ppermute x15, starting transfers between devices, along_ring(): return lax.ppermute(x, ('sp', 'tp'), pairs)  26.4 us
    all_to_all x1, starting transfers between devices, body(): lax.all_to_all(partial_mod, 'sp', split_axis=0, concat_axis=0, tiled=True)  24 us
    pallas_call x8, Pallas kernels, attend(): pl.pallas_call(functools.partial(attend_kernel, len(chunks), first, False...  18.9 us
    ppermute x9, waiting for transfers between devices, shifted(): return lax.ppermute(x, axis, [(i, (i + by) % n) for i in range(n)])  17.2 us
    ppermute x15, waiting for transfers between devices, along_ring(): return lax.ppermute(x, ('sp', 'tp'), pairs)  12.6 us
    ppermute x9, starting transfers between devices, shifted(): return lax.ppermute(x, axis, [(i, (i + by) % n) for i in range(n)])  11.6 us
    all_to_all x1, waiting for transfers between devices, body(): lax.all_to_all(partial_mod, 'sp', split_axis=0, concat_axis=0, tiled=True)  6.85 us
    pallas_call x1, Pallas kernels, body(): pl.pallas_call(kv_kernel, out_shape=[jax.ShapeDtypeStruct((tok + ctx, 2 *...  3.41 us
  transfers between devices with their start and end apart: 28, of which 22 were waited for; matrix products, arithmetic and copies ran while one was open for 2% of the time, Pallas kernels for 17%

commit v1 on v0

--- a/solution.py
+++ b/solution.py
@@ -84,7 +84,7 @@
     out_ref[5 * pieces:, :] = jnp.zeros((out_ref.shape[0] - 5 * pieces, 128), F32)
 
 
-def prepare_kernel(x_ref, c_ref, rx_ref, rc_ref):
+def prepare_kernel(x_ref, c_ref, wk_ref, wv_ref, rx_ref, rc_ref, w_ref):
     tok, width = x_ref.shape
     step = 16
 
@@ -103,10 +103,16 @@
     for i in range(c_ref.shape[0] // step):
         rows_of(c_ref, rc_ref, pl.ds(i * step, step))
 
+    @pl.loop(0, w_ref.shape[0] // 256)
+    def _(i):
+        rows = pl.ds(pl.multiple_of(i * 256, 256), 256)
+        w_ref[rows, :HEAD] = wk_ref[rows, :]
+        w_ref[rows, HEAD:] = wv_ref[rows, :]
+
 
 def kv_kernel(
-    x_ref, c_ref, rx_ref, rc_ref, own_ref, m1_ref, m3_ref, m2_ref, gain_ref, wk_ref, wv_ref, g_ref, cos_ref, sin_ref,
-    kv_ref, nm_ref, gate_ref, both_ref, mod_ref, ab_ref, w_ref,
+    x_ref, c_ref, rx_ref, rc_ref, own_ref, m1_ref, m3_ref, m2_ref, gain_ref, w_ref, g_ref, cos_ref, sin_ref,
+    kv_ref, nm_ref, gate_ref, both_ref, mod_ref, ab_ref,
 ):
     tok, width = x_ref.shape
     ctx = c_ref.shape[0]
@@ -129,29 +135,20 @@
             ab_ref[2:3, cs] = gain * (1.0 + piece[3])
             ab_ref[3:4, cs] = piece[4]
 
-    step = 64
-
-    @pl.loop(0, tok // step)
-    def _(i):
-        rows = pl.ds(pl.multiple_of(i * step, step), step)
-        r = rx_ref[rows, :]
-        for j in range(width // 128):
-            cs = slice(128 * j, 128 * j + 128)
-            v = x_ref[rows, cs].astype(F32) * r
-            nm_ref[rows, cs] = (v * ab_ref[0:1, cs] + ab_ref[1:2, cs]).astype(BF16)
-
-    r = rc_ref[...]
-    for j in range(width // 128):
-        cs = slice(128 * j, 128 * j + 128)
-        nm_ref[tok:tok + ctx, cs] = (c_ref[:, cs].astype(F32) * r * ab_ref[2:3, cs] + ab_ref[3:4, cs]).astype(BF16)
-
-    @pl.loop(0, w_ref.shape[0] // 256)
-    def _(i):
-        rows = pl.ds(pl.multiple_of(i * 256, 256), 256)
-        w_ref[rows, :HEAD] = wk_ref[rows, :]
-        w_ref[rows, HEAD:] = wv_ref[rows, :]
-
-    both_ref[...] = jnp.dot(nm_ref[...], w_ref[...], preferred_element_type=F32)
+    chunk, step = width // 4, 64
+    both = None
+    for k in range(0, width, chunk):
+        for j in range(k, k + chunk, 128):
+            cs = slice(j, j + 128)
+            for i in range(0, tok, step):
+                rows = slice(i, i + step)
+                v = x_ref[rows, cs].astype(F32) * rx_ref[rows, :]
+                nm_ref[rows, cs] = (v * ab_ref[0:1, cs] + ab_ref[1:2, cs]).astype(BF16)
+            v = c_ref[:, cs].astype(F32) * rc_ref[...]
+            nm_ref[tok:tok + ctx, cs] = (v * ab_ref[2:3, cs] + ab_ref[3:4, cs]).astype(BF16)
+        part = jnp.dot(nm_ref[:, k:k + chunk], w_ref[k:k + chunk, :], preferred_element_type=F32)
+        both = part if both is None else both + part
+    both_ref[...] = both
     kv_ref[:, HEAD:] = both_ref[:, HEAD:].astype(BF16)
     gain = g_ref[...]
     tile = 128
@@ -182,12 +179,14 @@
             q_ref[pl.ds(pl.multiple_of(h * tok + i * tile, tile), tile), :] = v.astype(BF16)
 
 
-def attend_block(q_ref, kv_refs, vt_ref, m_ref, l_ref, acc_ref, cols, tok):
+def attend_block(q_ref, kv_refs, vt_refs, m_ref, l_ref, acc_ref, cols, latents):
     q = q_ref[cols, :]
     scores = []
-    for kv_ref in kv_refs:
+    for kv_ref, lat in zip(kv_refs, latents, strict=True):
         s = lax.dot_general(kv_ref[:, :HEAD], q, (((1,), (1,)), ((), ())), preferred_element_type=F32)
-        scores += [s[:tok], s[tok:] + CONTEXT_LIFT / SCALING]
+        if lat < kv_ref.shape[0]:
+            s = jnp.concatenate([s[:lat], s[lat:] + CONTEXT_LIFT / SCALING], axis=0)
+        scores.append(s)
     old = m_ref[0:1, cols]
     new = old
     for s in scores:
@@ -196,15 +195,16 @@
     m_ref[0:1, cols] = new
     total = l_ref[0:1, cols] * keep
     out = acc_ref[:, cols] * keep
-    for i in range(len(kv_refs)):
-        p = jnp.exp2((jnp.concatenate(scores[2 * i:2 * i + 2], axis=0) - new) * (SCALING * LOG2E))
+    for s, vt_ref in zip(scores, vt_refs, strict=True):
+        p = jnp.exp2((s - new) * (SCALING * LOG2E))
         total = total + jnp.sum(p, axis=0, keepdims=True)
-        out = out + jnp.dot(vt_ref[i], p.astype(BF16), preferred_element_type=F32)
+        out = out + jnp.dot(vt_ref[...], p.astype(BF16), preferred_element_type=F32)
     l_ref[0:1, cols] = total
     acc_ref[:, cols] = out
 
 
-def attend_kernel(n_kv, first, last, tok, *refs):
+def attend_kernel(latents, first, last, tok, *refs):
+    n_kv = len(latents)
     q_ref, kv_refs = refs[0], refs[1:1 + n_kv]
     at = 1 + n_kv
     if not first:
@@ -213,11 +213,8 @@
     if last:
         out_ref = refs[at]
         at += 1
-        m_ref, l_ref, acc_ref = refs[at + 1:at + 4]
-        vt_ref = refs[at]
-    else:
-        m_ref, l_ref, acc_ref = refs[at:at + 3]
-        vt_ref = refs[at + 3]
+    m_ref, l_ref, acc_ref = refs[at:at + 3]
+    vt_refs = refs[at + 3:]
     if first:
         m_ref[...] = jnp.full(m_ref.shape, -1e30, F32)
         l_ref[...] = jnp.zeros(l_ref.shape, F32)
@@ -226,54 +223,58 @@
         m_ref[...] = m_in[...]
         l_ref[...] = l_in[...]
         acc_ref[...] = acc_in[...]
-    for i, kv_ref in enumerate(kv_refs):
-        vt_ref[i] = jnp.transpose(kv_ref[:, HEAD:])
+    for kv_ref, vt_ref in zip(kv_refs, vt_refs, strict=True):
+        vt_ref[...] = jnp.transpose(kv_ref[:, HEAD:])
     queries = q_ref.shape[0]
     width = 256
-
-    @pl.loop(0, queries // width)
-    def _(i):
-        cols = pl.ds(pl.multiple_of(i * width, width), width)
-        attend_block(q_ref, kv_refs, vt_ref, m_ref, l_ref, acc_ref, cols, tok)
-
     if last:
+        for i in range(0, queries, width):
+            attend_block(q_ref, kv_refs, vt_refs, m_ref, l_ref, acc_ref, slice(i, i + width), latents)
         for h in range(queries // tok):
             cols = slice(h * tok, (h + 1) * tok)
             done = acc_ref[:, cols] / l_ref[0:1, cols]
             out_ref[:, h * HEAD:(h + 1) * HEAD] = jnp.transpose(done).astype(BF16)
-
-
-def attend(q, chunks, state, tok, last=False):
+    else:
+
+        @pl.loop(0, queries // width)
+        def _(i):
+            cols = pl.ds(pl.multiple_of(i * width, width), width)
+            attend_block(q_ref, kv_refs, vt_refs, m_ref, l_ref, acc_ref, cols, latents)
+
+
+def attend(q, chunks, state, tok, latents=None, last=False):
     queries = q.shape[0]
     first = state is None
+    latents = latents or [tok] * len(chunks)
     shapes = [
         jax.ShapeDtypeStruct((8, queries), F32),
         jax.ShapeDtypeStruct((8, queries), F32),
         jax.ShapeDtypeStruct((HEAD, queries), F32),
     ]
     rows = sum(c.shape[0] for c in chunks)
-    turned = pltpu.VMEM((len(chunks), HEAD, chunks[0].shape[0]), BF16)
+    turned = [pltpu.VMEM((HEAD, c.shape[0]), BF16) for c in chunks]
     cost = pl.CostEstimate(
         flops=4 * rows * queries * HEAD, transcendentals=rows * queries, bytes_accessed=1 << 20
     )
     operands = [q, *chunks] + ([] if first else list(state))
+    kernel = functools.partial(attend_kernel, latents, first, last, tok)
     if last:
         return pl.pallas_call(
-            functools.partial(attend_kernel, len(chunks), first, True, tok),
+            kernel,
             out_shape=jax.ShapeDtypeStruct((tok, queries // tok * HEAD), BF16),
             in_specs=[VM] * len(operands),
             out_specs=VM,
-            scratch_shapes=[turned, *[pltpu.VMEM(s.shape, s.dtype) for s in shapes]],
+            scratch_shapes=[*[pltpu.VMEM(s.shape, s.dtype) for s in shapes], *turned],
             cost_estimate=cost,
             compiler_params=pltpu.CompilerParams(vmem_limit_bytes=16 << 20),
             name="attend_last",
         )(*operands)
     return pl.pallas_call(
-        functools.partial(attend_kernel, len(chunks), first, False, tok),
+        kernel,
         out_shape=shapes,
         in_specs=[VM] * len(operands),
         out_specs=[VM] * 3,
-        scratch_shapes=[turned],
+        scratch_shapes=turned,
         input_output_aliases={} if first else {1 + len(chunks) + i: i for i in range(3)},
         cost_estimate=cost,
         compiler_params=pltpu.CompilerParams(vmem_limit_bytes=16 << 20),
@@ -330,18 +331,19 @@
         name="modulation",
     )(cond_latent.reshape(-1, 128), cond_context.reshape(-1, 128), w_scale, w_shift, w_gate)
     gathered = lax.all_to_all(partial_mod, "sp", split_axis=0, concat_axis=0, tiled=True)
-    rx, rc = pl.pallas_call(
+    rx, rc, w_kv = pl.pallas_call(
         prepare_kernel,
         out_shape=[
             jax.ShapeDtypeStruct((tok, 128), F32),
             jax.ShapeDtypeStruct((ctx, 128), F32),
+            jax.ShapeDtypeStruct((width, 2 * HEAD), BF16),
         ],
-        in_specs=[VM] * 2,
-        out_specs=[VM] * 2,
+        in_specs=[VM] * 4,
+        out_specs=[VM] * 3,
         compiler_params=pltpu.CompilerParams(vmem_limit_bytes=32 << 20),
         cost_estimate=pl.CostEstimate(flops=1 << 30, transcendentals=0, bytes_accessed=12 << 20),
         name="prepare",
-    )(latent, context)
+    )(latent, context, w_key, w_value)
     positions = seq_index * tok + jnp.arange(tok, dtype=jnp.int32)
     freqs = HEAD // 4
     inverse = ROPE_THETA ** (-jnp.arange(freqs, dtype=F32) / freqs)
@@ -350,7 +352,7 @@
     cos = jnp.concatenate([jnp.cos(row), jnp.cos(row), jnp.cos(col), jnp.cos(col)], axis=1)
     sin = jnp.concatenate([-jnp.sin(row), jnp.sin(row), -jnp.sin(col), jnp.sin(col)], axis=1)
 
-    gathered, rx, rc, cos, sin = lax.optimization_barrier((gathered, rx, rc, cos, sin))
+    gathered, rx, rc, w_kv, cos, sin = lax.optimization_barrier((gathered, rx, rc, w_kv, cos, sin))
     summed = pl.pallas_call(
         sum_kernel,
         out_shape=jax.ShapeDtypeStruct((lines, 128), F32),
@@ -361,7 +363,8 @@
         name="sum_parts",
     )(gathered)
     pair = jnp.stack([summed, other_core(summed)])
-    columns = [pair, shifted(pair, "tp", 2), shifted(pair, "tp", -2), shifted(pair, "tp", 4)]
+    columns = [pair, shifted(pair, "tp", 2), shifted(pair, "tp", -2)]
+    columns.append(shifted(pair, "tp", 4))
 
     kv, normed, gate = pl.pallas_call(
         kv_kernel,
@@ -370,20 +373,18 @@
             jax.ShapeDtypeStruct((tok + ctx, width), BF16),
             jax.ShapeDtypeStruct((1, width), F32),
         ],
-        in_specs=[VM] * 14,
+        in_specs=[VM] * 13,
         out_specs=[VM] * 3,
         scratch_shapes=[
             pltpu.VMEM((tok + ctx, 2 * HEAD), F32),
             pltpu.VMEM((n_tp, lines, 128), F32),
             pltpu.VMEM((8, width), F32),
-            pltpu.VMEM((width, 2 * HEAD), BF16),
         ],
         cost_estimate=pl.CostEstimate(flops=2 * tok * width * 256, transcendentals=0, bytes_accessed=1 << 22),
         compiler_params=pltpu.CompilerParams(vmem_limit_bytes=24 << 20),
         name="project_kv",
     )(
-        latent, context, rx, rc, *columns, norm_gain.reshape(1, width), w_key, w_value, k_gain.reshape(1, HEAD),
-        cos, sin,
+        latent, context, rx, rc, *columns, norm_gain.reshape(1, width), w_kv, k_gain.reshape(1, HEAD), cos, sin
     )
 
     right, left = along_ring(kv, 1), along_ring(kv, -1)
@@ -399,16 +400,18 @@
     )(normed, w_query, q_gain.reshape(1, HEAD), cos, sin)
     state = attend(q, [kv], None, tok)
     half = n_sp // 2
+    cut = (tok + ctx) // 32 * 16
     for step in range(1, half):
         right, m = lax.optimization_barrier((right, state[0]))
         left, m = lax.optimization_barrier((left, m))
         state = [m, *state[1:]]
         now = [right, left]
+        if step + 1 == half:
+            right, left = right[:cut], left[cut:]
         right = along_ring(right, 1)
-        if step + 1 < half:
-            left = along_ring(left, -1)
+        left = along_ring(left, -1)
         state = attend(q, now, state, tok)
-    attended = attend(q, [right], state, tok, last=True)
+    attended = attend(q, [right, left], state, tok, [cut, tok - cut], last=True)
 
     n_x = lax.axis_size("tp") // 2
     core, chip = tp_index % 2, tp_index // 2
@@ -425,13 +428,16 @@
         return jnp.dot(rows, w_out, preferred_element_type=F32)
 
     far_sent = other_core(product(theirs, far).astype(BF16))
-    far_sum = (product(mine, far) + far_sent.astype(F32)).astype(BF16)
-    theirs, far_sum = lax.optimization_barrier((theirs, far_sum))
-    near_sent = other_core(product(theirs, near).astype(BF16))
+    own_far, own_near, their_near = lax.optimization_barrier(
+        (product(mine, far), product(mine, near), product(theirs, near).astype(BF16))
+    )
+    far_sum = (own_far + far_sent.astype(F32)).astype(BF16)
+    their_near, far_sum = lax.optimization_barrier((their_near, far_sum))
+    near_sent = other_core(their_near)
     h = width // 2
     from_left = shifted(far_sum[:, :h], "tp", 2)
     from_right = shifted(far_sum[:, h:], "tp", -2)
-    near_sum = product(mine, near) + near_sent.astype(F32)
+    near_sum = own_near + near_sent.astype(F32)
     nxt, prv, own = (near_sum[i * share:(i + 1) * share] for i in range(3))
     halves = (nxt[:, h:].astype(BF16), prv[:, :h].astype(BF16))
     a1 = shifted(halves[0], "tp", 2)

time: 142 us -> 144 us (1.014)
  local copies, waits for them, and re-layouts: 2.95 us -> 7.41 us
  Pallas kernels: 31 us -> 28.9 us
    ppermute x15 -> x16, waiting for transfers between devices: 12.6 us -> 17.4 us  [along_ring(): return lax.ppermute(x, ('sp', 'tp'), pairs)]
    all_to_all x1, waiting for transfers between devices: 6.85 us -> 2.6 us  [body(): lax.all_to_all(partial_mod, 'sp', split_axis=0, concat_axis=0, tiled=True)]
    unnamed x22 -> x26, local copies, waits for them, and re-layouts: 2.83 us -> 6.63 us
    pallas_call x9, Pallas kernels: 20.6 us -> 19 us  [the longest x8 18 us: attend(): pl.pallas_call(kernel, out_shape=shapes, in_specs=[VM] * len(operands), o...]
    ppermute x3, waiting for transfers between devices: 3.38 us -> 1.77 us  [other_core(): return lax.ppermute(x, 'tp', [(i, i ^ 1) for i in range(n)])]
    ppermute x15 -> x16, starting transfers between devices: 26.4 us -> 26.3 us  [along_ring(): return lax.ppermute(x, ('sp', 'tp'), pairs)]
  transfers between devices with their start and end apart: 28 -> 29, of which waited for: 22 -> 23; matrix products, arithmetic and copies ran while one was open for 2% -> 3% of each run, Pallas kernels for 17% -> 16%
where the time goes in v1:
time: 144 us
  starting transfers between devices  62.6 us (43%)
  waiting for transfers between devices  39 us (27%)
  Pallas kernels  28.9 us (20%)
  local copies, waits for them, and re-layouts  7.41 us (5%)
  other arithmetic  3.42 us (2%)
  matrix products  1.93 us (1%)
    ppermute x16, starting transfers between devices, along_ring(): return lax.ppermute(x, ('sp', 'tp'), pairs)  26.3 us
    all_to_all x1, starting transfers between devices, body(): lax.all_to_all(partial_mod, 'sp', split_axis=0, concat_axis=0, tiled=True)  24 us
    pallas_call x8, Pallas kernels, attend(): pl.pallas_call(kernel, out_shape=shapes, in_specs=[VM] * len(operands), o...  18 us
    ppermute x16, waiting for transfers between devices, along_ring(): return lax.ppermute(x, ('sp', 'tp'), pairs)  17.4 us
    ppermute x9, waiting for transfers between devices, shifted(): return lax.ppermute(x, axis, [(i, (i + by) % n) for i in range(n)])  17.2 us
    ppermute x9, starting transfers between devices, shifted(): return lax.ppermute(x, axis, [(i, (i + by) % n) for i in range(n)])  11.6 us
    unnamed x26, local copies, waits for them, and re-layouts  6.63 us
    pallas_call x1, Pallas kernels, body(): pl.pallas_call(prepare_kernel, out_shape=[jax.ShapeDtypeStruct((tok, 128)...  3.46 us
  transfers between devices with their start and end apart: 29, of which 23 were waited for; matrix products, arithmetic and copies ran while one was open for 3% of the time, Pallas kernels for 16%

profile of v1, /device:TPU:40, one launch (start us, length us, event | category | flops | bytes accessed | tf_op | source)
XLA Modules:
  0.0 143.6 jit_solution(1006606967161713089)
XLA Ops:
  2.3 24.0 %all-to-all-start = ((bf16[16,32,128]{2,1,0:T(8,128)(2,1)}), bf16[16,32,128]{2,1,0:T(8,128)(2,1)S(1)}, u32[]{:S(2)}, u32[]{:S(2)}) async-start(bf16[16,32,128]{2,1,0:T(8,128)(2,1)} %modulation.1), calls=%async_computation | async-start | bytes 262144 | tf_op jit(solution)/shard_map/all_to_all | solution.py:333
  31.6 3.5 %prepare.1 = (f32[384,128]{1,0:T(8,128)S(1)}, f32[16,128]{1,0:T(8,128)S(1)}, bf16[4096,256]{1,0:T(8,128)(2,1)S(1)}) custom-call(bf16[384,4096]{1,0:T(8,128)(2,1)S(1)} %copy-done.1, bf16[16,4096]{1,0:T(8,128)(2,1)S(1)} %copy-done.8, bf16[4096,128]{1,0:T(8,128)(2,1)S(1)} %copy-done.6, bf16[4096,128]{1,0:T(8,128)(2,1)S(1)} %copy-done.7), custom_call_target="tpu_custom_call" | custom-call | flops 1073741824 | bytes 12582912 | tf_op jit(solution)/shard_map/prepare/pallas_call | solution.py:334
  38.3 2.6 %all-to-all-done.in_ref = bf16[16,32,128]{2,1,0:T(8,128)(2,1)S(1)} async-done(((bf16[16,32,128]{2,1,0:T(8,128)(2,1)}), bf16[16,32,128]{2,1,0:T(8,128)(2,1)S(1)}, u32[]{:S(2)}, u32[]{:S(2)}) %all-to-all-start) | async-done | bytes 131104 | tf_op jit(solution)/shard_map/all_to_all | solution.py:333
  42.3 3.3 %collective-permute-start.3 = (f32[2,24,128]{2,1,0:T(8,128)S(1)}, f32[2,24,128]{2,1,0:T(8,128)S(1)}, u32[]{:S(2)}, u32[]{:S(2)}) collective-permute-start(f32[2,24,128]{2,1,0:T(8,128)S(1)} %pad_maximum_fusion.2.own_ref), channel_id=1, source_target_pairs={{0,4},{1,5},{2,6},{3,7},{4,0},{5,1},{6,2},{7,3},{8,12},{9,13},{10,... | collective-permute-start | bytes 73736 | tf_op jit(solution)/shard_map/ppermute | solution.py:287
  51.7 2.4 %project_kv.1 = (bf16[400,256]{1,0:T(8,128)(2,1)S(1)}, bf16[400,4096]{1,0:T(8,128)(2,1)S(1)}, f32[1,4096]{1,0:T(1,128)S(1)}) custom-call(bf16[384,4096]{1,0:T(8,128)(2,1)S(1)} %copy-done.2, bf16[16,4096]{1,0:T(8,128)(2,1)S(1)} %copy-done.9, f32[384,128]{1,0:T(8,128)S(1)} %get-tuple-element.82.rx_ref, f32[16,128]{1,0:T(8,128)S(1)} %get-tuple-element.83.rc_ref, ...), custom_call_target="tpu_custom_call" | custom-call | flops 805306368 | bytes 4194304 | tf_op jit(solution)/shard_map/project_kv/pallas_call | solution.py:369
  54.1 2.4 %collective-permute-start.4 = (bf16[400,256]{1,0:T(8,128)(2,1)S(1)}, bf16[400,256]{1,0:T(8,128)(2,1)S(1)}, u32[]{:S(2)}, u32[]{:S(2)}) collective-permute-start(bf16[400,256]{1,0:T(8,128)(2,1)S(1)} %get-tuple-element.90.refs_1_), channel_id=1, source_target_pairs={{0,120},{1,9},{2,122},{3,11},{4,124},{5,13},{6,126},{7,15},{8,0},{... | collective-permute-start | bytes 614408 | tf_op jit(solution)/shard_map/ppermute | solution.py:297
  60.9 2.9 %collective-permute-start.5 = (bf16[400,256]{1,0:T(8,128)(2,1)S(1)}, bf16[400,256]{1,0:T(8,128)(2,1)S(1)}, u32[]{:S(2)}, u32[]{:S(2)}) collective-permute-start(bf16[400,256]{1,0:T(8,128)(2,1)S(1)} %collective-permute-done.4.refs_1_), channel_id=1, source_target_pairs={{0,120},{1,9},{2,122},{3,11},{4,124},{5,13},{6,126},{7,15},{8,0},{... | collective-permute-start | bytes 614408 | tf_op jit(solution)/shard_map/ppermute | solution.py:297
  64.3 2.3 %attend.9 = (f32[8,768]{1,0:T(8,128)S(1)}, f32[8,768]{1,0:T(8,128)S(1)}, f32[128,768]{1,0:T(8,128)S(1)}) custom-call(bf16[768,128]{1,0:T(8,128)(2,1)S(1)} %project_q.1.refs_0_, bf16[400,256]{1,0:T(8,128)(2,1)S(1)} %collective-permute-done.4.refs_1_, ...), custom_call_target="tpu_custom_call", output_to_operand_aliasing={{0}: (3, {}), {1}: (4, {}), {2}: (5, {})} | custom-call | flops 314572800 | bytes 1048576 | tf_op jit(solution)/shard_map/attend/pallas_call | solution.py:272
  67.0 3.7 %collective-permute-start.7 = (bf16[400,256]{1,0:T(8,128)(2,1)S(1)}, bf16[400,256]{1,0:T(8,128)(2,1)S(1)}, u32[]{:S(2)}, u32[]{:S(2)}) collective-permute-start(bf16[400,256]{1,0:T(8,128)(2,1)S(1)} %collective-permute-done.5.refs_1_), channel_id=1, source_target_pairs={{0,120},{1,9},{2,122},{3,11},{4,124},{5,13},{6,126},{7,15},{8,0},{... | collective-permute-start | bytes 614408 | tf_op jit(solution)/shard_map/ppermute | solution.py:297
  70.7 2.6 %collective-permute-done.8.refs_2_ = bf16[400,256]{1,0:T(8,128)(2,1)S(1)} collective-permute-done((bf16[400,256]{1,0:T(8,128)(2,1)S(1)}, bf16[400,256]{1,0:T(8,128)(2,1)S(1)}, u32[]{:S(2)}, u32[]{:S(2)}) %collective-permute-start.8) | collective-permute-done | bytes 204832 | tf_op jit(solution)/shard_map/ppermute | solution.py:297
  73.4 2.3 %attend.10 = (f32[8,768]{1,0:T(8,128)S(1)}, f32[8,768]{1,0:T(8,128)S(1)}, f32[128,768]{1,0:T(8,128)S(1)}) custom-call(bf16[768,128]{1,0:T(8,128)(2,1)S(1)} %project_q.1.refs_0_, bf16[400,256]{1,0:T(8,128)(2,1)S(1)} %collective-permute-done.5.refs_1_, ...), custom_call_target="tpu_custom_call", output_to_operand_aliasing={{0}: (3, {}), {1}: (4, {}), {2}: (5, {})} | custom-call | flops 314572800 | bytes 1048576 | tf_op jit(solution)/shard_map/attend/pallas_call | solution.py:272
  75.7 3.3 %collective-permute-start.9 = (bf16[400,256]{1,0:T(8,128)(2,1)S(1)}, bf16[400,256]{1,0:T(8,128)(2,1)S(1)}, u32[]{:S(2)}, u32[]{:S(2)}) collective-permute-start(bf16[400,256]{1,0:T(8,128)(2,1)S(1)} %collective-permute-done.7.refs_1_), channel_id=1, source_target_pairs={{0,120},{1,9},{2,122},{3,11},{4,124},{5,13},{6,126},{7,15},{8,0},{... | collective-permute-start | bytes 614408 | tf_op jit(solution)/shard_map/ppermute | solution.py:297
  79.1 2.6 %collective-permute-done.10.refs_2_ = bf16[400,256]{1,0:T(8,128)(2,1)S(1)} collective-permute-done((bf16[400,256]{1,0:T(8,128)(2,1)S(1)}, bf16[400,256]{1,0:T(8,128)(2,1)S(1)}, u32[]{:S(2)}, u32[]{:S(2)}) %collective-permute-start.10) | collective-permute-done | bytes 204832 | tf_op jit(solution)/shard_map/ppermute | solution.py:297
  84.0 3.4 %collective-permute-start.11 = (bf16[400,256]{1,0:T(8,128)(2,1)S(1)}, bf16[400,256]{1,0:T(8,128)(2,1)S(1)}, u32[]{:S(2)}, u32[]{:S(2)}) collective-permute-start(bf16[400,256]{1,0:T(8,128)(2,1)S(1)} %collective-permute-done.9.refs_1_), channel_id=1, source_target_pairs={{0,120},{1,9},{2,122},{3,11},{4,124},{5,13},{6,126},{7,15},{8,0},{... | collective-permute-start | bytes 614408 | tf_op jit(solution)/shard_map/ppermute | solution.py:297
  89.1 2.3 %attend.12 = (f32[8,768]{1,0:T(8,128)S(1)}, f32[8,768]{1,0:T(8,128)S(1)}, f32[128,768]{1,0:T(8,128)S(1)}) custom-call(bf16[768,128]{1,0:T(8,128)(2,1)S(1)} %project_q.1.refs_0_, bf16[400,256]{1,0:T(8,128)(2,1)S(1)} %collective-permute-done.9.refs_1_, ...), custom_call_target="tpu_custom_call", output_to_operand_aliasing={{0}: (3, {}), {1}: (4, {}), {2}: (5, {})} | custom-call | flops 314572800 | bytes 1048576 | tf_op jit(solution)/shard_map/attend/pallas_call | solution.py:272
  91.5 3.4 %collective-permute-start.13 = (bf16[400,256]{1,0:T(8,128)(2,1)S(1)}, bf16[400,256]{1,0:T(8,128)(2,1)S(1)}, u32[]{:S(2)}, u32[]{:S(2)}) collective-permute-start(bf16[400,256]{1,0:T(8,128)(2,1)S(1)} %collective-permute-done.11.refs_1_), channel_id=1, source_target_pairs={{0,120},{1,9},{2,122},{3,11},{4,124},{5,13},{6,126},{7,15},{8,0},{... | collective-permute-start | bytes 614408 | tf_op jit(solution)/shard_map/ppermute | solution.py:297
  96.1 2.4 %attend.13 = (f32[8,768]{1,0:T(8,128)S(1)}, f32[8,768]{1,0:T(8,128)S(1)}, f32[128,768]{1,0:T(8,128)S(1)}) custom-call(bf16[768,128]{1,0:T(8,128)(2,1)S(1)} %project_q.1.refs_0_, bf16[400,256]{1,0:T(8,128)(2,1)S(1)} %collective-permute-done.11.refs_1_, ...), custom_call_target="tpu_custom_call", output_to_operand_aliasing={{0}: (3, {}), {1}: (4, {}), {2}: (5, {})} | custom-call | flops 314572800 | bytes 1048576 | tf_op jit(solution)/shard_map/attend/pallas_call | solution.py:272
  99.8 3.7 %collective-permute-start.15 = (bf16[400,256]{1,0:T(8,128)(2,1)S(1)}, bf16[400,256]{1,0:T(8,128)(2,1)S(1)}, u32[]{:S(2)}, u32[]{:S(2)}) collective-permute-start(bf16[400,256]{1,0:T(8,128)(2,1)S(1)} %collective-permute-done.13.refs_1_), channel_id=1, source_target_pairs={{0,120},{1,9},{2,122},{3,11},{4,124},{5,13},{6,126},{7,15},{8,0},{... | collective-permute-start | bytes 614408 | tf_op jit(solution)/shard_map/ppermute | solution.py:297
  103.5 2.3 %attend.14 = (f32[8,768]{1,0:T(8,128)S(1)}, f32[8,768]{1,0:T(8,128)S(1)}, f32[128,768]{1,0:T(8,128)S(1)}) custom-call(bf16[768,128]{1,0:T(8,128)(2,1)S(1)} %project_q.1.refs_0_, bf16[400,256]{1,0:T(8,128)(2,1)S(1)} %collective-permute-done.13.refs_1_, ...), custom_call_target="tpu_custom_call", output_to_operand_aliasing={{0}: (3, {}), {1}: (4, {}), {2}: (5, {})} | custom-call | flops 314572800 | bytes 1048576 | tf_op jit(solution)/shard_map/attend/pallas_call | solution.py:272
  107.6 3.8 %collective-permute-done.18.refs_2_ = bf16[400,256]{1,0:T(8,128)(2,1)S(1)} collective-permute-done((bf16[400,256]{1,0:T(8,128)(2,1)S(1)}, bf16[400,256]{1,0:T(8,128)(2,1)S(1)}, u32[]{:S(2)}, u32[]{:S(2)}) %collective-permute-start.18) | collective-permute-done | bytes 204832 | tf_op jit(solution)/shard_map/ppermute | solution.py:297
  112.5 3.2 %collective-permute-start.17 = (bf16[192,256]{1,0:T(8,128)(2,1)}, bf16[192,256]{1,0:T(8,128)(2,1)S(1)}, u32[]{:S(2)}, u32[]{:S(2)}) collective-permute-start(bf16[192,256]{1,0:T(8,128)(2,1)} %slice.73), channel_id=1, source_target_pairs={{0,120},{1,9},{2,122},{3,11},{4,124},{5,13},{6,126},{7,15},{8,0},{... | collective-permute-start | bytes 294920 | tf_op jit(solution)/shard_map/ppermute | solution.py:297
  115.7 2.3 %attend.15 = (f32[8,768]{1,0:T(8,128)S(1)}, f32[8,768]{1,0:T(8,128)S(1)}, f32[128,768]{1,0:T(8,128)S(1)}) custom-call(bf16[768,128]{1,0:T(8,128)(2,1)S(1)} %project_q.1.refs_0_, bf16[400,256]{1,0:T(8,128)(2,1)S(1)} %collective-permute-done.15.refs_1_, ...), custom_call_target="tpu_custom_call", output_to_operand_aliasing={{0}: (3, {}), {1}: (4, {}), {2}: (5, {})} | custom-call | flops 314572800 | bytes 1048576 | tf_op jit(solution)/shard_map/attend/pallas_call | solution.py:272
  125.2 4.2 %collective-permute-done.26 = bf16[48,2048]{1,0:T(8,128)(2,1)S(1)} collective-permute-done((bf16[48,2048]{1,0:T(8,128)(2,1)S(1)}, bf16[48,2048]{1,0:T(8,128)(2,1)S(1)}, u32[]{:S(2)}, u32[]{:S(2)}) %collective-permute-start.26) | collective-permute-done | bytes 196640 | tf_op jit(solution)/shard_map/ppermute | solution.py:287
  135.0 3.7 %collective-permute-done.27 = bf16[48,2048]{1,0:T(8,128)(2,1)S(1)} collective-permute-done((bf16[48,2048]{1,0:T(8,128)(2,1)S(1)}, bf16[48,2048]{1,0:T(8,128)(2,1)S(1)}, u32[]{:S(2)}, u32[]{:S(2)}) %collective-permute-start.27) | collective-permute-done | bytes 196640 | tf_op jit(solution)/shard_map/ppermute | solution.py:287
  (97 shorter events, 50.5 us)
Async XLA Ops:
  2.3 38.6 %all-to-all-start = ((bf16[16,32,128]{2,1,0:T(8,128)(2,1)}), bf16[16,32,128]{2,1,0:T(8,128)(2,1)S(1)}, u32[]{:S(2)}, u32[]{:S(2)}) async-start(bf16[16,32,128]{2,1,0:T(8,128)(2,1)} %modulation.1), calls=%async_computation | async-start | bytes 262144 | tf_op jit(solution)/shard_map/all_to_all | solution.py:333
  42.3 5.3 %collective-permute-start.3 = (f32[2,24,128]{2,1,0:T(8,128)S(1)}, f32[2,24,128]{2,1,0:T(8,128)S(1)}, u32[]{:S(2)}, u32[]{:S(2)}) collective-permute-start(f32[2,24,128]{2,1,0:T(8,128)S(1)} %pad_maximum_fusion.2.own_ref), channel_id=1, source_target_pairs={{0,4},{1,5},{2,6},{3,7},{4,0},{5,1},{6,2},{7,3},{8,12},{9,13},{10,... | collective-permute-start | bytes 73736 | tf_op jit(solution)/shard_map/ppermute | solution.py:287
  54.1 6.8 %collective-permute-start.4 = (bf16[400,256]{1,0:T(8,128)(2,1)S(1)}, bf16[400,256]{1,0:T(8,128)(2,1)S(1)}, u32[]{:S(2)}, u32[]{:S(2)}) collective-permute-start(bf16[400,256]{1,0:T(8,128)(2,1)S(1)} %get-tuple-element.90.refs_1_), channel_id=1, source_target_pairs={{0,120},{1,9},{2,122},{3,11},{4,124},{5,13},{6,126},{7,15},{8,0},{... | collective-permute-start | bytes 614408 | tf_op jit(solution)/shard_map/ppermute | solution.py:297
  56.5 7.9 %collective-permute-start.6 = (bf16[400,256]{1,0:T(8,128)(2,1)S(1)}, bf16[400,256]{1,0:T(8,128)(2,1)S(1)}, u32[]{:S(2)}, u32[]{:S(2)}) collective-permute-start(bf16[400,256]{1,0:T(8,128)(2,1)S(1)} %get-tuple-element.90.refs_1_), channel_id=1, source_target_pairs={{0,8},{1,121},{2,10},{3,123},{4,12},{5,125},{6,14},{7,127},{8,16},... | collective-permute-start | bytes 614408 | tf_op jit(solution)/shard_map/ppermute | solution.py:297
  60.9 6.2 %collective-permute-start.5 = (bf16[400,256]{1,0:T(8,128)(2,1)S(1)}, bf16[400,256]{1,0:T(8,128)(2,1)S(1)}, u32[]{:S(2)}, u32[]{:S(2)}) collective-permute-start(bf16[400,256]{1,0:T(8,128)(2,1)S(1)} %collective-permute-done.4.refs_1_), channel_id=1, source_target_pairs={{0,120},{1,9},{2,122},{3,11},{4,124},{5,13},{6,126},{7,15},{8,0},{... | collective-permute-start | bytes 614408 | tf_op jit(solution)/shard_map/ppermute | solution.py:297
  64.3 9.0 %collective-permute-start.8 = (bf16[400,256]{1,0:T(8,128)(2,1)S(1)}, bf16[400,256]{1,0:T(8,128)(2,1)S(1)}, u32[]{:S(2)}, u32[]{:S(2)}) collective-permute-start(bf16[400,256]{1,0:T(8,128)(2,1)S(1)} %collective-permute-done.6.refs_2_), channel_id=1, source_target_pairs={{0,8},{1,121},{2,10},{3,123},{4,12},{5,125},{6,14},{7,127},{8,16},... | collective-permute-start | bytes 614408 | tf_op jit(solution)/shard_map/ppermute | solution.py:297
  67.0 8.7 %collective-permute-start.7 = (bf16[400,256]{1,0:T(8,128)(2,1)S(1)}, bf16[400,256]{1,0:T(8,128)(2,1)S(1)}, u32[]{:S(2)}, u32[]{:S(2)}) collective-permute-start(bf16[400,256]{1,0:T(8,128)(2,1)S(1)} %collective-permute-done.5.refs_1_), channel_id=1, source_target_pairs={{0,120},{1,9},{2,122},{3,11},{4,124},{5,13},{6,126},{7,15},{8,0},{... | collective-permute-start | bytes 614408 | tf_op jit(solution)/shard_map/ppermute | solution.py:297
  73.4 8.3 %collective-permute-start.10 = (bf16[400,256]{1,0:T(8,128)(2,1)S(1)}, bf16[400,256]{1,0:T(8,128)(2,1)S(1)}, u32[]{:S(2)}, u32[]{:S(2)}) collective-permute-start(bf16[400,256]{1,0:T(8,128)(2,1)S(1)} %collective-permute-done.8.refs_2_), channel_id=1, source_target_pairs={{0,8},{1,121},{2,10},{3,123},{4,12},{5,125},{6,14},{7,127},{8,16},... | collective-permute-start | bytes 614408 | tf_op jit(solution)/shard_map/ppermute | solution.py:297
  75.7 8.3 %collective-permute-start.9 = (bf16[400,256]{1,0:T(8,128)(2,1)S(1)}, bf16[400,256]{1,0:T(8,128)(2,1)S(1)}, u32[]{:S(2)}, u32[]{:S(2)}) collective-permute-start(bf16[400,256]{1,0:T(8,128)(2,1)S(1)} %collective-permute-done.7.refs_1_), channel_id=1, source_target_pairs={{0,120},{1,9},{2,122},{3,11},{4,124},{5,13},{6,126},{7,15},{8,0},{... | collective-permute-start | bytes 614408 | tf_op jit(solution)/shard_map/ppermute | solution.py:297
  81.7 7.5 %collective-permute-start.12 = (bf16[400,256]{1,0:T(8,128)(2,1)S(1)}, bf16[400,256]{1,0:T(8,128)(2,1)S(1)}, u32[]{:S(2)}, u32[]{:S(2)}) collective-permute-start(bf16[400,256]{1,0:T(8,128)(2,1)S(1)} %collective-permute-done.10.refs_2_), channel_id=1, source_target_pairs={{0,8},{1,121},{2,10},{3,123},{4,12},{5,125},{6,14},{7,127},{8,16},... | collective-permute-start | bytes 614408 | tf_op jit(solution)/shard_map/ppermute | solution.py:297
  84.0 7.4 %collective-permute-start.11 = (bf16[400,256]{1,0:T(8,128)(2,1)S(1)}, bf16[400,256]{1,0:T(8,128)(2,1)S(1)}, u32[]{:S(2)}, u32[]{:S(2)}) collective-permute-start(bf16[400,256]{1,0:T(8,128)(2,1)S(1)} %collective-permute-done.9.refs_1_), channel_id=1, source_target_pairs={{0,120},{1,9},{2,122},{3,11},{4,124},{5,13},{6,126},{7,15},{8,0},{... | collective-permute-start | bytes 614408 | tf_op jit(solution)/shard_map/ppermute | solution.py:297
  89.1 7.0 %collective-permute-start.14 = (bf16[400,256]{1,0:T(8,128)(2,1)S(1)}, bf16[400,256]{1,0:T(8,128)(2,1)S(1)}, u32[]{:S(2)}, u32[]{:S(2)}) collective-permute-start(bf16[400,256]{1,0:T(8,128)(2,1)S(1)} %collective-permute-done.12.refs_2_), channel_id=1, source_target_pairs={{0,8},{1,121},{2,10},{3,123},{4,12},{5,125},{6,14},{7,127},{8,16},... | collective-permute-start | bytes 614408 | tf_op jit(solution)/shard_map/ppermute | solution.py:297
  91.5 8.3 %collective-permute-start.13 = (bf16[400,256]{1,0:T(8,128)(2,1)S(1)}, bf16[400,256]{1,0:T(8,128)(2,1)S(1)}, u32[]{:S(2)}, u32[]{:S(2)}) collective-permute-start(bf16[400,256]{1,0:T(8,128)(2,1)S(1)} %collective-permute-done.11.refs_1_), channel_id=1, source_target_pairs={{0,120},{1,9},{2,122},{3,11},{4,124},{5,13},{6,126},{7,15},{8,0},{... | collective-permute-start | bytes 614408 | tf_op jit(solution)/shard_map/ppermute | solution.py:297
  96.1 7.3 %collective-permute-start.16 = (bf16[400,256]{1,0:T(8,128)(2,1)S(1)}, bf16[400,256]{1,0:T(8,128)(2,1)S(1)}, u32[]{:S(2)}, u32[]{:S(2)}) collective-permute-start(bf16[400,256]{1,0:T(8,128)(2,1)S(1)} %collective-permute-done.14.refs_2_), channel_id=1, source_target_pairs={{0,8},{1,121},{2,10},{3,123},{4,12},{5,125},{6,14},{7,127},{8,16},... | collective-permute-start | bytes 614408 | tf_op jit(solution)/shard_map/ppermute | solution.py:297
  99.8 7.9 %collective-permute-start.15 = (bf16[400,256]{1,0:T(8,128)(2,1)S(1)}, bf16[400,256]{1,0:T(8,128)(2,1)S(1)}, u32[]{:S(2)}, u32[]{:S(2)}) collective-permute-start(bf16[400,256]{1,0:T(8,128)(2,1)S(1)} %collective-permute-done.13.refs_1_), channel_id=1, source_target_pairs={{0,120},{1,9},{2,122},{3,11},{4,124},{5,13},{6,126},{7,15},{8,0},{... | collective-permute-start | bytes 614408 | tf_op jit(solution)/shard_map/ppermute | solution.py:297
  103.5 8.0 %collective-permute-start.18 = (bf16[400,256]{1,0:T(8,128)(2,1)S(1)}, bf16[400,256]{1,0:T(8,128)(2,1)S(1)}, u32[]{:S(2)}, u32[]{:S(2)}) collective-permute-start(bf16[400,256]{1,0:T(8,128)(2,1)S(1)} %collective-permute-done.16.refs_2_), channel_id=1, source_target_pairs={{0,8},{1,121},{2,10},{3,123},{4,12},{5,125},{6,14},{7,127},{8,16},... | collective-permute-start | bytes 614408 | tf_op jit(solution)/shard_map/ppermute | solution.py:297
  111.5 6.8 %collective-permute-start.19 = (bf16[208,256]{1,0:T(8,128)(2,1)S(1)}, bf16[208,256]{1,0:T(8,128)(2,1)S(1)}, u32[]{:S(2)}, u32[]{:S(2)}) collective-permute-start(bf16[208,256]{1,0:T(8,128)(2,1)S(1)} %slice.74), channel_id=1, source_target_pairs={{0,8},{1,121},{2,10},{3,123},{4,12},{5,125},{6,14},{7,127},{8,16},... | collective-permute-start | bytes 319496 | tf_op jit(solution)/shard_map/ppermute | solution.py:297
  112.5 5.7 %collective-permute-start.17 = (bf16[192,256]{1,0:T(8,128)(2,1)}, bf16[192,256]{1,0:T(8,128)(2,1)S(1)}, u32[]{:S(2)}, u32[]{:S(2)}) collective-permute-start(bf16[192,256]{1,0:T(8,128)(2,1)} %slice.73), channel_id=1, source_target_pairs={{0,120},{1,9},{2,122},{3,11},{4,124},{5,13},{6,126},{7,15},{8,0},{... | collective-permute-start | bytes 294920 | tf_op jit(solution)/shard_map/ppermute | solution.py:297
  122.2 7.1 %collective-permute-start.26 = (bf16[48,2048]{1,0:T(8,128)(2,1)S(1)}, bf16[48,2048]{1,0:T(8,128)(2,1)S(1)}, u32[]{:S(2)}, u32[]{:S(2)}) collective-permute-start(bf16[48,2048]{1,0:T(8,128)(2,1)S(1)} %get-tuple-element.161), channel_id=1, source_target_pairs={{0,6},{1,7},{2,0},{3,1},{4,2},{5,3},{6,4},{7,5},{8,14},{9,15},{10,... | collective-permute-start | bytes 589832 | tf_op jit(solution)/shard_map/ppermute | solution.py:287
  122.4 8.4 %collective-permute-start.22 = (bf16[48,2048]{1,0:T(8,128)(2,1)S(1)}, bf16[48,2048]{1,0:T(8,128)(2,1)S(1)}, u32[]{:S(2)}, u32[]{:S(2)}) collective-permute-start(bf16[48,2048]{1,0:T(8,128)(2,1)S(1)} %get-tuple-element.162), channel_id=1, source_target_pairs={{0,2},{1,3},{2,4},{3,5},{4,6},{5,7},{6,0},{7,1},{8,10},{9,11},{10,... | collective-permute-start | bytes 589832 | tf_op jit(solution)/shard_map/ppermute | solution.py:287
  130.8 7.9 %collective-permute-start.27 = (bf16[48,2048]{1,0:T(8,128)(2,1)S(1)}, bf16[48,2048]{1,0:T(8,128)(2,1)S(1)}, u32[]{:S(2)}, u32[]{:S(2)}) collective-permute-start(bf16[48,2048]{1,0:T(8,128)(2,1)S(1)} %get-tuple-element.155), channel_id=1, source_target_pairs={{0,6},{1,7},{2,0},{3,1},{4,2},{5,3},{6,4},{7,5},{8,14},{9,15},{10,... | collective-permute-start | bytes 589832 | tf_op jit(solution)/shard_map/ppermute | solution.py:287
  131.1 8.9 %collective-permute-start.23 = (bf16[48,2048]{1,0:T(8,128)(2,1)S(1)}, bf16[48,2048]{1,0:T(8,128)(2,1)S(1)}, u32[]{:S(2)}, u32[]{:S(2)}) collective-permute-start(bf16[48,2048]{1,0:T(8,128)(2,1)S(1)} %get-tuple-element.156), channel_id=1, source_target_pairs={{0,2},{1,3},{2,4},{3,5},{4,6},{5,7},{6,0},{7,1},{8,10},{9,11},{10,... | collective-permute-start | bytes 589832 | tf_op jit(solution)/shard_map/ppermute | solution.py:287
  132.9 8.4 %collective-permute-start.25 = (bf16[48,2048]{1,0:T(8,128)(2,1)S(1)}, bf16[48,2048]{1,0:T(8,128)(2,1)S(1)}, u32[]{:S(2)}, u32[]{:S(2)}) collective-permute-start(bf16[48,2048]{1,0:T(8,128)(2,1)S(1)} %get-tuple-element.157), channel_id=1, source_target_pairs={{0,6},{1,7},{2,0},{3,1},{4,2},{5,3},{6,4},{7,5},{8,14},{9,15},{10,... | collective-permute-start | bytes 589832 | tf_op jit(solution)/shard_map/ppermute | solution.py:287
  134.3 8.4 %collective-permute-start.24 = (bf16[48,2048]{1,0:T(8,128)(2,1)S(1)}, bf16[48,2048]{1,0:T(8,128)(2,1)S(1)}, u32[]{:S(2)}, u32[]{:S(2)}) collective-permute-start(bf16[48,2048]{1,0:T(8,128)(2,1)S(1)} %get-tuple-element.158), channel_id=1, source_target_pairs={{0,2},{1,3},{2,4},{3,5},{4,6},{5,7},{6,0},{7,1},{8,10},{9,11},{10,... | collective-permute-start | bytes 589832 | tf_op jit(solution)/shard_map/ppermute | solution.py:287
  (18 other events, 204.1 us)

commit v2 on v1

--- a/solution.py
+++ b/solution.py
@@ -203,13 +203,14 @@
     acc_ref[:, cols] = out
 
 
-def attend_kernel(latents, first, last, tok, *refs):
+def attend_kernel(latents, first, last, tok, beats, *refs):
     n_kv = len(latents)
     q_ref, kv_refs = refs[0], refs[1:1 + n_kv]
     at = 1 + n_kv
     if not first:
         m_in, l_in, acc_in = refs[at:at + 3]
         at += 3
+    at += beats
     if last:
         out_ref = refs[at]
         at += 1
@@ -242,10 +243,10 @@
             attend_block(q_ref, kv_refs, vt_refs, m_ref, l_ref, acc_ref, cols, latents)
 
 
-def attend(q, chunks, state, tok, latents=None, last=False):
+def attend(q, chunks, state, tok, beat=None, last=False):
     queries = q.shape[0]
     first = state is None
-    latents = latents or [tok] * len(chunks)
+    latents = [tok] * len(chunks)
     shapes = [
         jax.ShapeDtypeStruct((8, queries), F32),
         jax.ShapeDtypeStruct((8, queries), F32),
@@ -256,8 +257,8 @@
     cost = pl.CostEstimate(
         flops=4 * rows * queries * HEAD, transcendentals=rows * queries, bytes_accessed=1 << 20
     )
-    operands = [q, *chunks] + ([] if first else list(state))
-    kernel = functools.partial(attend_kernel, latents, first, last, tok)
+    operands = [q, *chunks] + ([] if first else list(state)) + ([] if beat is None else [beat])
+    kernel = functools.partial(attend_kernel, latents, first, last, tok, beat is not None)
     if last:
         return pl.pallas_call(
             kernel,
@@ -400,18 +401,17 @@
     )(normed, w_query, q_gain.reshape(1, HEAD), cos, sin)
     state = attend(q, [kv], None, tok)
     half = n_sp // 2
-    cut = (tok + ctx) // 32 * 16
     for step in range(1, half):
+        beat = other_core(state[0]) if step in (1, 3, 5) else None
         right, m = lax.optimization_barrier((right, state[0]))
         left, m = lax.optimization_barrier((left, m))
         state = [m, *state[1:]]
         now = [right, left]
-        if step + 1 == half:
-            right, left = right[:cut], left[cut:]
         right = along_ring(right, 1)
-        left = along_ring(left, -1)
-        state = attend(q, now, state, tok)
-    attended = attend(q, [right, left], state, tok, [cut, tok - cut], last=True)
+        if step + 1 < half:
+            left = along_ring(left, -1)
+        state = attend(q, now, state, tok, beat=beat)
+    attended = attend(q, [right], state, tok, last=True)
 
     n_x = lax.axis_size("tp") // 2
     core, chip = tp_index % 2, tp_index // 2

time: 144 us -> 144 us (level)
    ppermute x16 -> x15, waiting for transfers between devices: 17.4 us -> 13.2 us  [along_ring(): return lax.ppermute(x, ('sp', 'tp'), pairs)]
    ppermute x3 -> x6, waiting for transfers between devices: 1.77 us -> 4.7 us  [other_core(): return lax.ppermute(x, 'tp', [(i, i ^ 1) for i in range(n)])]
    ppermute x16 -> x15, starting transfers between devices: 26.3 us -> 27.4 us  [along_ring(): return lax.ppermute(x, ('sp', 'tp'), pairs)]
  transfers between devices with their start and end apart: 29 -> 31, of which waited for: 23 -> 23; matrix products, arithmetic and copies ran while one was open for 3% -> 3% of each run, Pallas kernels for 16% -> 17%
where the time goes in v2:
time: 144 us
  starting transfers between devices  63.7 us (44%)
  waiting for transfers between devices  37.7 us (26%)
  Pallas kernels  30.2 us (21%)
  local copies, waits for them, and re-layouts  6.74 us (5%)
  other arithmetic  3.42 us (2%)
  matrix products  1.93 us (1%)
    ppermute x15, starting transfers between devices, along_ring(): return lax.ppermute(x, ('sp', 'tp'), pairs)  27.4 us
    all_to_all x1, starting transfers between devices, body(): lax.all_to_all(partial_mod, 'sp', split_axis=0, concat_axis=0, tiled=True)  24 us
    pallas_call x8, Pallas kernels, attend(): pl.pallas_call(kernel, out_shape=shapes, in_specs=[VM] * len(operands), o...  19 us
    ppermute x9, waiting for transfers between devices, shifted(): return lax.ppermute(x, axis, [(i, (i + by) % n) for i in range(n)])  17.2 us
    ppermute x15, waiting for transfers between devices, along_ring(): return lax.ppermute(x, ('sp', 'tp'), pairs)  13.2 us
    ppermute x9, starting transfers between devices, shifted(): return lax.ppermute(x, axis, [(i, (i + by) % n) for i in range(n)])  11.6 us
    unnamed x26, local copies, waits for them, and re-layouts  6.62 us
    ppermute x6, waiting for transfers between devices, other_core(): return lax.ppermute(x, 'tp', [(i, i ^ 1) for i in range(n)])  4.7 us
  transfers between devices with their start and end apart: 31, of which 23 were waited for; matrix products, arithmetic and copies ran while one was open for 3% of the time, Pallas kernels for 17%

profile of v2, /device:TPU:40, one launch (start us, length us, event | category | flops | bytes accessed | tf_op | source)
XLA Modules:
  0.0 144.1 jit_solution(3566744590006241339)
XLA Ops:
  0.0 2.3 %modulation.1 = bf16[16,32,128]{2,1,0:T(8,128)(2,1)} custom-call(bf16[32,128]{1,0:T(8,128)(2,1)} %bitcast.38, bf16[32,128]{1,0:T(8,128)(2,1)} %bitcast.39, bf16[256,512]{1,0:T(8,128)(2,1)} %scale_hbm.1, bf16[256,512]{1,0:T(8,128)(2,1)} %shift_hbm.1, bf16[256,512]{1,0:T(8,128)(2,1)} %gate_hbm.1), custom_call_target="tpu_custom_call" | custom-call | tf_op jit(solution)/shard_map/modulation/pallas_call | solution.py:320
  2.3 24.0 %all-to-all-start = ((bf16[16,32,128]{2,1,0:T(8,128)(2,1)}), bf16[16,32,128]{2,1,0:T(8,128)(2,1)S(1)}, u32[]{:S(2)}, u32[]{:S(2)}) async-start(bf16[16,32,128]{2,1,0:T(8,128)(2,1)} %modulation.1), calls=%async_computation | async-start | bytes 262144 | tf_op jit(solution)/shard_map/all_to_all | solution.py:334
  31.6 3.5 %prepare.1 = (f32[384,128]{1,0:T(8,128)S(1)}, f32[16,128]{1,0:T(8,128)S(1)}, bf16[4096,256]{1,0:T(8,128)(2,1)S(1)}) custom-call(bf16[384,4096]{1,0:T(8,128)(2,1)S(1)} %copy-done.1, bf16[16,4096]{1,0:T(8,128)(2,1)S(1)} %copy-done.8, bf16[4096,128]{1,0:T(8,128)(2,1)S(1)} %copy-done.6, bf16[4096,128]{1,0:T(8,128)(2,1)S(1)} %copy-done.7), custom_call_target="tpu_custom_call" | custom-call | flops 1073741824 | bytes 12582912 | tf_op jit(solution)/shard_map/prepare/pallas_call | solution.py:335
  38.3 2.6 %all-to-all-done.in_ref = bf16[16,32,128]{2,1,0:T(8,128)(2,1)S(1)} async-done(((bf16[16,32,128]{2,1,0:T(8,128)(2,1)}), bf16[16,32,128]{2,1,0:T(8,128)(2,1)S(1)}, u32[]{:S(2)}, u32[]{:S(2)}) %all-to-all-start) | async-done | bytes 131104 | tf_op jit(solution)/shard_map/all_to_all | solution.py:334
  42.3 3.3 %collective-permute-start.3 = (f32[2,24,128]{2,1,0:T(8,128)S(1)}, f32[2,24,128]{2,1,0:T(8,128)S(1)}, u32[]{:S(2)}, u32[]{:S(2)}) collective-permute-start(f32[2,24,128]{2,1,0:T(8,128)S(1)} %pad_maximum_fusion.2.own_ref), channel_id=1, source_target_pairs={{0,4},{1,5},{2,6},{3,7},{4,0},{5,1},{6,2},{7,3},{8,12},{9,13},{10,... | collective-permute-start | bytes 73736 | tf_op jit(solution)/shard_map/ppermute | solution.py:288
  49.4 2.2 %collective-permute-done.1.m1_ref = f32[2,24,128]{2,1,0:T(8,128)S(1)} collective-permute-done((f32[2,24,128]{2,1,0:T(8,128)S(1)}, f32[2,24,128]{2,1,0:T(8,128)S(1)}, u32[]{:S(2)}, u32[]{:S(2)}) %collective-permute-start.1) | collective-permute-done | bytes 24608 | tf_op jit(solution)/shard_map/ppermute | solution.py:288
  51.7 2.4 %project_kv.1 = (bf16[400,256]{1,0:T(8,128)(2,1)S(1)}, bf16[400,4096]{1,0:T(8,128)(2,1)S(1)}, f32[1,4096]{1,0:T(1,128)S(1)}) custom-call(bf16[384,4096]{1,0:T(8,128)(2,1)S(1)} %copy-done.2, bf16[16,4096]{1,0:T(8,128)(2,1)S(1)} %copy-done.9, f32[384,128]{1,0:T(8,128)S(1)} %get-tuple-element.82.rx_ref, f32[16,128]{1,0:T(8,128)S(1)} %get-tuple-element.83.rc_ref, ...), custom_call_target="tpu_custom_call" | custom-call | flops 805306368 | bytes 4194304 | tf_op jit(solution)/shard_map/project_kv/pallas_call | solution.py:370
  54.1 2.4 %collective-permute-start.4 = (bf16[400,256]{1,0:T(8,128)(2,1)S(1)}, bf16[400,256]{1,0:T(8,128)(2,1)S(1)}, u32[]{:S(2)}, u32[]{:S(2)}) collective-permute-start(bf16[400,256]{1,0:T(8,128)(2,1)S(1)} %get-tuple-element.90.refs_1_), channel_id=1, source_target_pairs={{0,120},{1,9},{2,122},{3,11},{4,124},{5,13},{6,126},{7,15},{8,0},{... | collective-permute-start | bytes 614408 | tf_op jit(solution)/shard_map/ppermute | solution.py:298
  60.9 2.9 %collective-permute-start.5 = (bf16[400,256]{1,0:T(8,128)(2,1)S(1)}, bf16[400,256]{1,0:T(8,128)(2,1)S(1)}, u32[]{:S(2)}, u32[]{:S(2)}) collective-permute-start(bf16[400,256]{1,0:T(8,128)(2,1)S(1)} %collective-permute-done.4.refs_1_), channel_id=1, source_target_pairs={{0,120},{1,9},{2,122},{3,11},{4,124},{5,13},{6,126},{7,15},{8,0},{... | collective-permute-start | bytes 614408 | tf_op jit(solution)/shard_map/ppermute | solution.py:298
  65.0 2.4 %attend.9 = (f32[8,768]{1,0:T(8,128)S(1)}, f32[8,768]{1,0:T(8,128)S(1)}, f32[128,768]{1,0:T(8,128)S(1)}) custom-call(bf16[768,128]{1,0:T(8,128)(2,1)S(1)} %project_q.1.refs_0_, bf16[400,256]{1,0:T(8,128)(2,1)S(1)} %collective-permute-done.4.refs_1_, ...), custom_call_target="tpu_custom_call", output_to_operand_aliasing={{0}: (3, {}), {1}: (4, {}), {2}: (5, {})} | custom-call | flops 314572800 | bytes 1048576 | tf_op jit(solution)/shard_map/attend/pallas_call | solution.py:273
  69.1 3.7 %collective-permute-start.8 = (bf16[400,256]{1,0:T(8,128)(2,1)S(1)}, bf16[400,256]{1,0:T(8,128)(2,1)S(1)}, u32[]{:S(2)}, u32[]{:S(2)}) collective-permute-start(bf16[400,256]{1,0:T(8,128)(2,1)S(1)} %collective-permute-done.5.refs_1_), channel_id=1, source_target_pairs={{0,120},{1,9},{2,122},{3,11},{4,124},{5,13},{6,126},{7,15},{8,0},{... | collective-permute-start | bytes 614408 | tf_op jit(solution)/shard_map/ppermute | solution.py:298
  72.8 2.3 %attend.10 = (f32[8,768]{1,0:T(8,128)S(1)}, f32[8,768]{1,0:T(8,128)S(1)}, f32[128,768]{1,0:T(8,128)S(1)}) custom-call(bf16[768,128]{1,0:T(8,128)(2,1)S(1)} %project_q.1.refs_0_, bf16[400,256]{1,0:T(8,128)(2,1)S(1)} %collective-permute-done.5.refs_1_, ...), custom_call_target="tpu_custom_call", output_to_operand_aliasing={{0}: (3, {}), {1}: (4, {}), {2}: (5, {})} | custom-call | flops 314572800 | bytes 1048576 | tf_op jit(solution)/shard_map/attend/pallas_call | solution.py:273
  77.2 3.7 %collective-permute-start.10 = (bf16[400,256]{1,0:T(8,128)(2,1)S(1)}, bf16[400,256]{1,0:T(8,128)(2,1)S(1)}, u32[]{:S(2)}, u32[]{:S(2)}) collective-permute-start(bf16[400,256]{1,0:T(8,128)(2,1)S(1)} %collective-permute-done.8.refs_1_), channel_id=1, source_target_pairs={{0,120},{1,9},{2,122},{3,11},{4,124},{5,13},{6,126},{7,15},{8,0},{... | collective-permute-start | bytes 614408 | tf_op jit(solution)/shard_map/ppermute | solution.py:298
  82.1 2.4 %attend.11 = (f32[8,768]{1,0:T(8,128)S(1)}, f32[8,768]{1,0:T(8,128)S(1)}, f32[128,768]{1,0:T(8,128)S(1)}) custom-call(bf16[768,128]{1,0:T(8,128)(2,1)S(1)} %project_q.1.refs_0_, bf16[400,256]{1,0:T(8,128)(2,1)S(1)} %collective-permute-done.8.refs_1_, ...), custom_call_target="tpu_custom_call", output_to_operand_aliasing={{0}: (3, {}), {1}: (4, {}), {2}: (5, {})} | custom-call | flops 314572800 | bytes 1048576 | tf_op jit(solution)/shard_map/attend/pallas_call | solution.py:273
  86.2 3.7 %collective-permute-start.13 = (bf16[400,256]{1,0:T(8,128)(2,1)S(1)}, bf16[400,256]{1,0:T(8,128)(2,1)S(1)}, u32[]{:S(2)}, u32[]{:S(2)}) collective-permute-start(bf16[400,256]{1,0:T(8,128)(2,1)S(1)} %collective-permute-done.10.refs_1_), channel_id=1, source_target_pairs={{0,120},{1,9},{2,122},{3,11},{4,124},{5,13},{6,126},{7,15},{8,0},{... | collective-permute-start | bytes 614408 | tf_op jit(solution)/shard_map/ppermute | solution.py:298
  89.9 2.4 %attend.12 = (f32[8,768]{1,0:T(8,128)S(1)}, f32[8,768]{1,0:T(8,128)S(1)}, f32[128,768]{1,0:T(8,128)S(1)}) custom-call(bf16[768,128]{1,0:T(8,128)(2,1)S(1)} %project_q.1.refs_0_, bf16[400,256]{1,0:T(8,128)(2,1)S(1)} %collective-permute-done.10.refs_1_, ...), custom_call_target="tpu_custom_call", output_to_operand_aliasing={{0}: (3, {}), {1}: (4, {}), {2}: (5, {})} | custom-call | flops 314572800 | bytes 1048576 | tf_op jit(solution)/shard_map/attend/pallas_call | solution.py:273
  94.3 3.7 %collective-permute-start.15 = (bf16[400,256]{1,0:T(8,128)(2,1)S(1)}, bf16[400,256]{1,0:T(8,128)(2,1)S(1)}, u32[]{:S(2)}, u32[]{:S(2)}) collective-permute-start(bf16[400,256]{1,0:T(8,128)(2,1)S(1)} %collective-permute-done.13.refs_1_), channel_id=1, source_target_pairs={{0,120},{1,9},{2,122},{3,11},{4,124},{5,13},{6,126},{7,15},{8,0},{... | collective-permute-start | bytes 614408 | tf_op jit(solution)/shard_map/ppermute | solution.py:298
  99.2 2.4 %attend.13 = (f32[8,768]{1,0:T(8,128)S(1)}, f32[8,768]{1,0:T(8,128)S(1)}, f32[128,768]{1,0:T(8,128)S(1)}) custom-call(bf16[768,128]{1,0:T(8,128)(2,1)S(1)} %project_q.1.refs_0_, bf16[400,256]{1,0:T(8,128)(2,1)S(1)} %collective-permute-done.13.refs_1_, ...), custom_call_target="tpu_custom_call", output_to_operand_aliasing={{0}: (3, {}), {1}: (4, {}), {2}: (5, {})} | custom-call | flops 314572800 | bytes 1048576 | tf_op jit(solution)/shard_map/attend/pallas_call | solution.py:273
  103.3 3.7 %collective-permute-start.18 = (bf16[400,256]{1,0:T(8,128)(2,1)S(1)}, bf16[400,256]{1,0:T(8,128)(2,1)S(1)}, u32[]{:S(2)}, u32[]{:S(2)}) collective-permute-start(bf16[400,256]{1,0:T(8,128)(2,1)S(1)} %collective-permute-done.15.refs_1_), channel_id=1, source_target_pairs={{0,120},{1,9},{2,122},{3,11},{4,124},{5,13},{6,126},{7,15},{8,0},{... | collective-permute-start | bytes 614408 | tf_op jit(solution)/shard_map/ppermute | solution.py:298
  107.0 2.3 %attend.14 = (f32[8,768]{1,0:T(8,128)S(1)}, f32[8,768]{1,0:T(8,128)S(1)}, f32[128,768]{1,0:T(8,128)S(1)}) custom-call(bf16[768,128]{1,0:T(8,128)(2,1)S(1)} %project_q.1.refs_0_, bf16[400,256]{1,0:T(8,128)(2,1)S(1)} %collective-permute-done.15.refs_1_, ...), custom_call_target="tpu_custom_call", output_to_operand_aliasing={{0}: (3, {}), {1}: (4, {}), {2}: (5, {})} | custom-call | flops 314572800 | bytes 1048576 | tf_op jit(solution)/shard_map/attend/pallas_call | solution.py:273
  111.4 3.7 %collective-permute-start.20 = (bf16[400,256]{1,0:T(8,128)(2,1)S(1)}, bf16[400,256]{1,0:T(8,128)(2,1)S(1)}, u32[]{:S(2)}, u32[]{:S(2)}) collective-permute-start(bf16[400,256]{1,0:T(8,128)(2,1)S(1)} %collective-permute-done.18.refs_1_), channel_id=1, source_target_pairs={{0,120},{1,9},{2,122},{3,11},{4,124},{5,13},{6,126},{7,15},{8,0},{... | collective-permute-start | bytes 614408 | tf_op jit(solution)/shard_map/ppermute | solution.py:298
  115.1 3.3 %attend.15 = (f32[8,768]{1,0:T(8,128)S(1)}, f32[8,768]{1,0:T(8,128)S(1)}, f32[128,768]{1,0:T(8,128)S(1)}) custom-call(bf16[768,128]{1,0:T(8,128)(2,1)S(1)} %project_q.1.refs_0_, bf16[400,256]{1,0:T(8,128)(2,1)S(1)} %collective-permute-done.18.refs_1_, ...), custom_call_target="tpu_custom_call", output_to_operand_aliasing={{0}: (3, {}), {1}: (4, {}), {2}: (5, {})} | custom-call | flops 314572800 | bytes 1048576 | tf_op jit(solution)/shard_map/attend/pallas_call | solution.py:273
  125.7 4.2 %collective-permute-done.28 = bf16[48,2048]{1,0:T(8,128)(2,1)S(1)} collective-permute-done((bf16[48,2048]{1,0:T(8,128)(2,1)S(1)}, bf16[48,2048]{1,0:T(8,128)(2,1)S(1)}, u32[]{:S(2)}, u32[]{:S(2)}) %collective-permute-start.28) | collective-permute-done | bytes 196640 | tf_op jit(solution)/shard_map/ppermute | solution.py:288
  135.7 3.7 %collective-permute-done.29 = bf16[48,2048]{1,0:T(8,128)(2,1)S(1)} collective-permute-done((bf16[48,2048]{1,0:T(8,128)(2,1)S(1)}, bf16[48,2048]{1,0:T(8,128)(2,1)S(1)}, u32[]{:S(2)}, u32[]{:S(2)}) %collective-permute-start.29) | collective-permute-done | bytes 196640 | tf_op jit(solution)/shard_map/ppermute | solution.py:288
  (99 shorter events, 50.8 us)
Async XLA Ops:
  2.3 38.6 %all-to-all-start = ((bf16[16,32,128]{2,1,0:T(8,128)(2,1)}), bf16[16,32,128]{2,1,0:T(8,128)(2,1)S(1)}, u32[]{:S(2)}, u32[]{:S(2)}) async-start(bf16[16,32,128]{2,1,0:T(8,128)(2,1)} %modulation.1), calls=%async_computation | async-start | bytes 262144 | tf_op jit(solution)/shard_map/all_to_all | solution.py:334
  42.3 5.3 %collective-permute-start.3 = (f32[2,24,128]{2,1,0:T(8,128)S(1)}, f32[2,24,128]{2,1,0:T(8,128)S(1)}, u32[]{:S(2)}, u32[]{:S(2)}) collective-permute-start(f32[2,24,128]{2,1,0:T(8,128)S(1)} %pad_maximum_fusion.2.own_ref), channel_id=1, source_target_pairs={{0,4},{1,5},{2,6},{3,7},{4,0},{5,1},{6,2},{7,3},{8,12},{9,13},{10,... | collective-permute-start | bytes 73736 | tf_op jit(solution)/shard_map/ppermute | solution.py:288
  46.6 5.0 %collective-permute-start.1 = (f32[2,24,128]{2,1,0:T(8,128)S(1)}, f32[2,24,128]{2,1,0:T(8,128)S(1)}, u32[]{:S(2)}, u32[]{:S(2)}) collective-permute-start(f32[2,24,128]{2,1,0:T(8,128)S(1)} %pad_maximum_fusion.2.own_ref), channel_id=1, source_target_pairs={{0,2},{1,3},{2,4},{3,5},{4,6},{5,7},{6,0},{7,1},{8,10},{9,11},{10,... | collective-permute-start | bytes 73736 | tf_op jit(solution)/shard_map/ppermute | solution.py:288
  54.1 6.8 %collective-permute-start.4 = (bf16[400,256]{1,0:T(8,128)(2,1)S(1)}, bf16[400,256]{1,0:T(8,128)(2,1)S(1)}, u32[]{:S(2)}, u32[]{:S(2)}) collective-permute-start(bf16[400,256]{1,0:T(8,128)(2,1)S(1)} %get-tuple-element.90.refs_1_), channel_id=1, source_target_pairs={{0,120},{1,9},{2,122},{3,11},{4,124},{5,13},{6,126},{7,15},{8,0},{... | collective-permute-start | bytes 614408 | tf_op jit(solution)/shard_map/ppermute | solution.py:298
  56.5 7.9 %collective-permute-start.6 = (bf16[400,256]{1,0:T(8,128)(2,1)S(1)}, bf16[400,256]{1,0:T(8,128)(2,1)S(1)}, u32[]{:S(2)}, u32[]{:S(2)}) collective-permute-start(bf16[400,256]{1,0:T(8,128)(2,1)S(1)} %get-tuple-element.90.refs_1_), channel_id=1, source_target_pairs={{0,8},{1,121},{2,10},{3,123},{4,12},{5,125},{6,14},{7,127},{8,16},... | collective-permute-start | bytes 614408 | tf_op jit(solution)/shard_map/ppermute | solution.py:298
  60.9 8.2 %collective-permute-start.5 = (bf16[400,256]{1,0:T(8,128)(2,1)S(1)}, bf16[400,256]{1,0:T(8,128)(2,1)S(1)}, u32[]{:S(2)}, u32[]{:S(2)}) collective-permute-start(bf16[400,256]{1,0:T(8,128)(2,1)S(1)} %collective-permute-done.4.refs_1_), channel_id=1, source_target_pairs={{0,120},{1,9},{2,122},{3,11},{4,124},{5,13},{6,126},{7,15},{8,0},{... | collective-permute-start | bytes 614408 | tf_op jit(solution)/shard_map/ppermute | solution.py:298
  64.4 8.4 %collective-permute-start.9 = (bf16[400,256]{1,0:T(8,128)(2,1)S(1)}, bf16[400,256]{1,0:T(8,128)(2,1)S(1)}, u32[]{:S(2)}, u32[]{:S(2)}) collective-permute-start(bf16[400,256]{1,0:T(8,128)(2,1)S(1)} %collective-permute-done.6.refs_2_), channel_id=1, source_target_pairs={{0,8},{1,121},{2,10},{3,123},{4,12},{5,125},{6,14},{7,127},{8,16},... | collective-permute-start | bytes 614408 | tf_op jit(solution)/shard_map/ppermute | solution.py:298
  69.1 8.1 %collective-permute-start.8 = (bf16[400,256]{1,0:T(8,128)(2,1)S(1)}, bf16[400,256]{1,0:T(8,128)(2,1)S(1)}, u32[]{:S(2)}, u32[]{:S(2)}) collective-permute-start(bf16[400,256]{1,0:T(8,128)(2,1)S(1)} %collective-permute-done.5.refs_1_), channel_id=1, source_target_pairs={{0,120},{1,9},{2,122},{3,11},{4,124},{5,13},{6,126},{7,15},{8,0},{... | collective-permute-start | bytes 614408 | tf_op jit(solution)/shard_map/ppermute | solution.py:298
  72.8 8.1 %collective-permute-start.11 = (bf16[400,256]{1,0:T(8,128)(2,1)S(1)}, bf16[400,256]{1,0:T(8,128)(2,1)S(1)}, u32[]{:S(2)}, u32[]{:S(2)}) collective-permute-start(bf16[400,256]{1,0:T(8,128)(2,1)S(1)} %collective-permute-done.9.refs_2_), channel_id=1, source_target_pairs={{0,8},{1,121},{2,10},{3,123},{4,12},{5,125},{6,14},{7,127},{8,16},... | collective-permute-start | bytes 614408 | tf_op jit(solution)/shard_map/ppermute | solution.py:298
  77.2 9.0 %collective-permute-start.10 = (bf16[400,256]{1,0:T(8,128)(2,1)S(1)}, bf16[400,256]{1,0:T(8,128)(2,1)S(1)}, u32[]{:S(2)}, u32[]{:S(2)}) collective-permute-start(bf16[400,256]{1,0:T(8,128)(2,1)S(1)} %collective-permute-done.8.refs_1_), channel_id=1, source_target_pairs={{0,120},{1,9},{2,122},{3,11},{4,124},{5,13},{6,126},{7,15},{8,0},{... | collective-permute-start | bytes 614408 | tf_op jit(solution)/shard_map/ppermute | solution.py:298
  80.9 9.0 %collective-permute-start.14 = (bf16[400,256]{1,0:T(8,128)(2,1)S(1)}, bf16[400,256]{1,0:T(8,128)(2,1)S(1)}, u32[]{:S(2)}, u32[]{:S(2)}) collective-permute-start(bf16[400,256]{1,0:T(8,128)(2,1)S(1)} %collective-permute-done.11.refs_2_), channel_id=1, source_target_pairs={{0,8},{1,121},{2,10},{3,123},{4,12},{5,125},{6,14},{7,127},{8,16},... | collective-permute-start | bytes 614408 | tf_op jit(solution)/shard_map/ppermute | solution.py:298
  86.2 8.1 %collective-permute-start.13 = (bf16[400,256]{1,0:T(8,128)(2,1)S(1)}, bf16[400,256]{1,0:T(8,128)(2,1)S(1)}, u32[]{:S(2)}, u32[]{:S(2)}) collective-permute-start(bf16[400,256]{1,0:T(8,128)(2,1)S(1)} %collective-permute-done.10.refs_1_), channel_id=1, source_target_pairs={{0,120},{1,9},{2,122},{3,11},{4,124},{5,13},{6,126},{7,15},{8,0},{... | collective-permute-start | bytes 614408 | tf_op jit(solution)/shard_map/ppermute | solution.py:298
  89.9 8.1 %collective-permute-start.16 = (bf16[400,256]{1,0:T(8,128)(2,1)S(1)}, bf16[400,256]{1,0:T(8,128)(2,1)S(1)}, u32[]{:S(2)}, u32[]{:S(2)}) collective-permute-start(bf16[400,256]{1,0:T(8,128)(2,1)S(1)} %collective-permute-done.14.refs_2_), channel_id=1, source_target_pairs={{0,8},{1,121},{2,10},{3,123},{4,12},{5,125},{6,14},{7,127},{8,16},... | collective-permute-start | bytes 614408 | tf_op jit(solution)/shard_map/ppermute | solution.py:298
  94.3 9.0 %collective-permute-start.15 = (bf16[400,256]{1,0:T(8,128)(2,1)S(1)}, bf16[400,256]{1,0:T(8,128)(2,1)S(1)}, u32[]{:S(2)}, u32[]{:S(2)}) collective-permute-start(bf16[400,256]{1,0:T(8,128)(2,1)S(1)} %collective-permute-done.13.refs_1_), channel_id=1, source_target_pairs={{0,120},{1,9},{2,122},{3,11},{4,124},{5,13},{6,126},{7,15},{8,0},{... | collective-permute-start | bytes 614408 | tf_op jit(solution)/shard_map/ppermute | solution.py:298
  98.0 9.0 %collective-permute-start.19 = (bf16[400,256]{1,0:T(8,128)(2,1)S(1)}, bf16[400,256]{1,0:T(8,128)(2,1)S(1)}, u32[]{:S(2)}, u32[]{:S(2)}) collective-permute-start(bf16[400,256]{1,0:T(8,128)(2,1)S(1)} %collective-permute-done.16.refs_2_), channel_id=1, source_target_pairs={{0,8},{1,121},{2,10},{3,123},{4,12},{5,125},{6,14},{7,127},{8,16},... | collective-permute-start | bytes 614408 | tf_op jit(solution)/shard_map/ppermute | solution.py:298
  103.3 8.1 %collective-permute-start.18 = (bf16[400,256]{1,0:T(8,128)(2,1)S(1)}, bf16[400,256]{1,0:T(8,128)(2,1)S(1)}, u32[]{:S(2)}, u32[]{:S(2)}) collective-permute-start(bf16[400,256]{1,0:T(8,128)(2,1)S(1)} %collective-permute-done.15.refs_1_), channel_id=1, source_target_pairs={{0,120},{1,9},{2,122},{3,11},{4,124},{5,13},{6,126},{7,15},{8,0},{... | collective-permute-start | bytes 614408 | tf_op jit(solution)/shard_map/ppermute | solution.py:298
  107.0 8.1 %collective-permute-start.21 = (bf16[400,256]{1,0:T(8,128)(2,1)S(1)}, bf16[400,256]{1,0:T(8,128)(2,1)}, u32[]{:S(2)}, u32[]{:S(2)}) collective-permute-start(bf16[400,256]{1,0:T(8,128)(2,1)S(1)} %collective-permute-done.19.refs_2_), channel_id=1, source_target_pairs={{0,8},{1,121},{2,10},{3,123},{4,12},{5,125},{6,14},{7,127},{8,16},... | collective-permute-start | bytes 614408 | tf_op jit(solution)/shard_map/ppermute | solution.py:298
  111.4 7.0 %collective-permute-start.20 = (bf16[400,256]{1,0:T(8,128)(2,1)S(1)}, bf16[400,256]{1,0:T(8,128)(2,1)S(1)}, u32[]{:S(2)}, u32[]{:S(2)}) collective-permute-start(bf16[400,256]{1,0:T(8,128)(2,1)S(1)} %collective-permute-done.18.refs_1_), channel_id=1, source_target_pairs={{0,120},{1,9},{2,122},{3,11},{4,124},{5,13},{6,126},{7,15},{8,0},{... | collective-permute-start | bytes 614408 | tf_op jit(solution)/shard_map/ppermute | solution.py:298
  122.7 7.1 %collective-permute-start.28 = (bf16[48,2048]{1,0:T(8,128)(2,1)S(1)}, bf16[48,2048]{1,0:T(8,128)(2,1)S(1)}, u32[]{:S(2)}, u32[]{:S(2)}) collective-permute-start(bf16[48,2048]{1,0:T(8,128)(2,1)S(1)} %get-tuple-element.161), channel_id=1, source_target_pairs={{0,6},{1,7},{2,0},{3,1},{4,2},{5,3},{6,4},{7,5},{8,14},{9,15},{10,... | collective-permute-start | bytes 589832 | tf_op jit(solution)/shard_map/ppermute | solution.py:288
  123.4 8.0 %collective-permute-start.24 = (bf16[48,2048]{1,0:T(8,128)(2,1)S(1)}, bf16[48,2048]{1,0:T(8,128)(2,1)S(1)}, u32[]{:S(2)}, u32[]{:S(2)}) collective-permute-start(bf16[48,2048]{1,0:T(8,128)(2,1)S(1)} %get-tuple-element.162), channel_id=1, source_target_pairs={{0,2},{1,3},{2,4},{3,5},{4,6},{5,7},{6,0},{7,1},{8,10},{9,11},{10,... | collective-permute-start | bytes 589832 | tf_op jit(solution)/shard_map/ppermute | solution.py:288
  131.5 7.9 %collective-permute-start.29 = (bf16[48,2048]{1,0:T(8,128)(2,1)S(1)}, bf16[48,2048]{1,0:T(8,128)(2,1)S(1)}, u32[]{:S(2)}, u32[]{:S(2)}) collective-permute-start(bf16[48,2048]{1,0:T(8,128)(2,1)S(1)} %get-tuple-element.155), channel_id=1, source_target_pairs={{0,6},{1,7},{2,0},{3,1},{4,2},{5,3},{6,4},{7,5},{8,14},{9,15},{10,... | collective-permute-start | bytes 589832 | tf_op jit(solution)/shard_map/ppermute | solution.py:288
  131.9 8.6 %collective-permute-start.25 = (bf16[48,2048]{1,0:T(8,128)(2,1)S(1)}, bf16[48,2048]{1,0:T(8,128)(2,1)S(1)}, u32[]{:S(2)}, u32[]{:S(2)}) collective-permute-start(bf16[48,2048]{1,0:T(8,128)(2,1)S(1)} %get-tuple-element.156), channel_id=1, source_target_pairs={{0,2},{1,3},{2,4},{3,5},{4,6},{5,7},{6,0},{7,1},{8,10},{9,11},{10,... | collective-permute-start | bytes 589832 | tf_op jit(solution)/shard_map/ppermute | solution.py:288
  133.6 8.1 %collective-permute-start.27 = (bf16[48,2048]{1,0:T(8,128)(2,1)S(1)}, bf16[48,2048]{1,0:T(8,128)(2,1)S(1)}, u32[]{:S(2)}, u32[]{:S(2)}) collective-permute-start(bf16[48,2048]{1,0:T(8,128)(2,1)S(1)} %get-tuple-element.157), channel_id=1, source_target_pairs={{0,6},{1,7},{2,0},{3,1},{4,2},{5,3},{6,4},{7,5},{8,14},{9,15},{10,... | collective-permute-start | bytes 589832 | tf_op jit(solution)/shard_map/ppermute | solution.py:288
  135.1 8.1 %collective-permute-start.26 = (bf16[48,2048]{1,0:T(8,128)(2,1)S(1)}, bf16[48,2048]{1,0:T(8,128)(2,1)S(1)}, u32[]{:S(2)}, u32[]{:S(2)}) collective-permute-start(bf16[48,2048]{1,0:T(8,128)(2,1)S(1)} %get-tuple-element.158), channel_id=1, source_target_pairs={{0,2},{1,3},{2,4},{3,5},{4,6},{5,7},{6,0},{7,1},{8,10},{9,11},{10,... | collective-permute-start | bytes 589832 | tf_op jit(solution)/shard_map/ppermute | solution.py:288
  (20 other events, 203.2 us)

commit v3 on v2

--- a/solution.py
+++ b/solution.py
@@ -203,14 +203,13 @@
     acc_ref[:, cols] = out
 
 
-def attend_kernel(latents, first, last, tok, beats, *refs):
+def attend_kernel(latents, first, last, tok, *refs):
     n_kv = len(latents)
     q_ref, kv_refs = refs[0], refs[1:1 + n_kv]
     at = 1 + n_kv
     if not first:
         m_in, l_in, acc_in = refs[at:at + 3]
         at += 3
-    at += beats
     if last:
         out_ref = refs[at]
         at += 1
@@ -243,7 +242,7 @@
             attend_block(q_ref, kv_refs, vt_refs, m_ref, l_ref, acc_ref, cols, latents)
 
 
-def attend(q, chunks, state, tok, beat=None, last=False):
+def attend(q, chunks, state, tok, last=False):
     queries = q.shape[0]
     first = state is None
     latents = [tok] * len(chunks)
@@ -257,8 +256,8 @@
     cost = pl.CostEstimate(
         flops=4 * rows * queries * HEAD, transcendentals=rows * queries, bytes_accessed=1 << 20
     )
-    operands = [q, *chunks] + ([] if first else list(state)) + ([] if beat is None else [beat])
-    kernel = functools.partial(attend_kernel, latents, first, last, tok, beat is not None)
+    operands = [q, *chunks] + ([] if first else list(state))
+    kernel = functools.partial(attend_kernel, latents, first, last, tok)
     if last:
         return pl.pallas_call(
             kernel,
@@ -402,15 +401,14 @@
     state = attend(q, [kv], None, tok)
     half = n_sp // 2
     for step in range(1, half):
-        beat = other_core(state[0]) if step in (1, 3, 5) else None
         right, m = lax.optimization_barrier((right, state[0]))
-        left, m = lax.optimization_barrier((left, m))
-        state = [m, *state[1:]]
-        now = [right, left]
-        right = along_ring(right, 1)
+        now, right = right, along_ring(right, 1)
+        state = attend(q, [now], [m, *state[1:]], tok)
+        left, m = lax.optimization_barrier((left, state[0]))
+        now = left
         if step + 1 < half:
             left = along_ring(left, -1)
-        state = attend(q, now, state, tok, beat=beat)
+        state = attend(q, [now], [m, *state[1:]], tok)
     attended = attend(q, [right], state, tok, last=True)
 
     n_x = lax.axis_size("tp") // 2
@@ -428,16 +426,13 @@
         return jnp.dot(rows, w_out, preferred_element_type=F32)
 
     far_sent = other_core(product(theirs, far).astype(BF16))
-    own_far, own_near, their_near = lax.optimization_barrier(
-        (product(mine, far), product(mine, near), product(theirs, near).astype(BF16))
-    )
-    far_sum = (own_far + far_sent.astype(F32)).astype(BF16)
-    their_near, far_sum = lax.optimization_barrier((their_near, far_sum))
-    near_sent = other_core(their_near)
+    far_sum = (product(mine, far) + far_sent.astype(F32)).astype(BF16)
+    theirs, far_sum = lax.optimization_barrier((theirs, far_sum))
+    near_sent = other_core(product(theirs, near).astype(BF16))
     h = width // 2
     from_left = shifted(far_sum[:, :h], "tp", 2)
     from_right = shifted(far_sum[:, h:], "tp", -2)
-    near_sum = own_near + near_sent.astype(F32)
+    near_sum = product(mine, near) + near_sent.astype(F32)
     nxt, prv, own = (near_sum[i * share:(i + 1) * share] for i in range(3))
     halves = (nxt[:, h:].astype(BF16), prv[:, :h].astype(BF16))
     a1 = shifted(halves[0], "tp", 2)

time: 144 us -> 137 us (0.951)
  waiting for transfers between devices: 37.7 us -> 21.4 us
  Pallas kernels: 30.2 us -> 35.4 us
  starting transfers between devices: 63.7 us -> 67.5 us
    ppermute x15, waiting for transfers between devices: 13.2 us -> 3.05 us  [along_ring(): return lax.ppermute(x, ('sp', 'tp'), pairs)]
    pallas_call x8 -> x15, Pallas kernels: 19 us -> 24.3 us  [attend(): pl.pallas_call(kernel, out_shape=shapes, in_specs=[VM] * len(operands), o...]
    ppermute x9, waiting for transfers between devices: 17.2 us -> 12.9 us  [shifted(): return lax.ppermute(x, axis, [(i, (i + by) % n) for i in range(n)])]
    ppermute x9, starting transfers between devices: 11.6 us -> 15.4 us  [shifted(): return lax.ppermute(x, axis, [(i, (i + by) % n) for i in range(n)])]
    ppermute x6 -> x3, waiting for transfers between devices: 4.7 us -> 2.85 us  [other_core(): return lax.ppermute(x, 'tp', [(i, i ^ 1) for i in range(n)])]
    unnamed x26 -> x30, local copies, waits for them, and re-layouts: 6.62 us -> 6.62 us
  transfers between devices with their start and end apart: 31 -> 28, of which waited for: 23 -> 16; matrix products, arithmetic and copies ran while one was open for 3% -> 2% of each run, Pallas kernels for 17% -> 22%
where the time goes in v3:
time: 137 us
  starting transfers between devices  67.5 us (49%)
  Pallas kernels  35.4 us (26%)
  waiting for transfers between devices  21.4 us (16%)
  local copies, waits for them, and re-layouts  6.73 us (5%)
  other arithmetic  3.01 us (2%)
  matrix products  2.01 us (1%)
    ppermute x15, starting transfers between devices, along_ring(): return lax.ppermute(x, ('sp', 'tp'), pairs)  27.7 us
    pallas_call x15, Pallas kernels, attend(): pl.pallas_call(kernel, out_shape=shapes, in_specs=[VM] * len(operands), o...  24.3 us
    all_to_all x1, starting transfers between devices, body(): lax.all_to_all(partial_mod, 'sp', split_axis=0, concat_axis=0, tiled=True)  24 us
    ppermute x9, starting transfers between devices, shifted(): return lax.ppermute(x, axis, [(i, (i + by) % n) for i in range(n)])  15.4 us
    ppermute x9, waiting for transfers between devices, shifted(): return lax.ppermute(x, axis, [(i, (i + by) % n) for i in range(n)])  12.9 us
    unnamed x30, local copies, waits for them, and re-layouts  6.62 us
    pallas_call x1, Pallas kernels, body(): pl.pallas_call(prepare_kernel, out_shape=[jax.ShapeDtypeStruct((tok, 128)...  3.46 us
    ppermute x15, waiting for transfers between devices, along_ring(): return lax.ppermute(x, ('sp', 'tp'), pairs)  3.05 us
  transfers between devices with their start and end apart: 28, of which 16 were waited for; matrix products, arithmetic and copies ran while one was open for 2% of the time, Pallas kernels for 22%

profile of v3, /device:TPU:40, one launch (start us, length us, event | category | flops | bytes accessed | tf_op | source)
XLA Modules:
  0.0 136.7 jit_solution(4185151353628011632)
XLA Ops:
  0.0 2.3 %modulation.1 = bf16[16,32,128]{2,1,0:T(8,128)(2,1)} custom-call(bf16[32,128]{1,0:T(8,128)(2,1)} %bitcast.42, bf16[32,128]{1,0:T(8,128)(2,1)} %bitcast.43, bf16[256,512]{1,0:T(8,128)(2,1)} %scale_hbm.1, bf16[256,512]{1,0:T(8,128)(2,1)} %shift_hbm.1, bf16[256,512]{1,0:T(8,128)(2,1)} %gate_hbm.1), custom_call_target="tpu_custom_call" | custom-call | tf_op jit(solution)/shard_map/modulation/pallas_call | solution.py:319
  2.3 24.0 %all-to-all-start = ((bf16[16,32,128]{2,1,0:T(8,128)(2,1)}), bf16[16,32,128]{2,1,0:T(8,128)(2,1)S(1)}, u32[]{:S(2)}, u32[]{:S(2)}) async-start(bf16[16,32,128]{2,1,0:T(8,128)(2,1)} %modulation.1), calls=%async_computation | async-start | bytes 262144 | tf_op jit(solution)/shard_map/all_to_all | solution.py:333
  26.4 1.9 %copy-done.1 = bf16[384,4096]{1,0:T(8,128)(2,1)S(1)} copy-done((bf16[384,4096]{1,0:T(8,128)(2,1)S(1)}, bf16[384,4096]{1,0:T(8,128)(2,1)}, u32[]{:S(2)}) %copy-start.1) | copy-done | bytes 3145752
  31.6 3.5 %prepare.1 = (f32[384,128]{1,0:T(8,128)S(1)}, f32[16,128]{1,0:T(8,128)S(1)}, bf16[4096,256]{1,0:T(8,128)(2,1)S(1)}) custom-call(bf16[384,4096]{1,0:T(8,128)(2,1)S(1)} %copy-done.1, bf16[16,4096]{1,0:T(8,128)(2,1)S(1)} %copy-done.8, bf16[4096,128]{1,0:T(8,128)(2,1)S(1)} %copy-done.6, bf16[4096,128]{1,0:T(8,128)(2,1)S(1)} %copy-done.7), custom_call_target="tpu_custom_call" | custom-call | flops 1073741824 | bytes 12582912 | tf_op jit(solution)/shard_map/prepare/pallas_call | solution.py:334
  38.3 2.6 %all-to-all-done.in_ref = bf16[16,32,128]{2,1,0:T(8,128)(2,1)S(1)} async-done(((bf16[16,32,128]{2,1,0:T(8,128)(2,1)}), bf16[16,32,128]{2,1,0:T(8,128)(2,1)S(1)}, u32[]{:S(2)}, u32[]{:S(2)}) %all-to-all-start) | async-done | bytes 131104 | tf_op jit(solution)/shard_map/all_to_all | solution.py:333
  45.5 2.1 %collective-permute-start.3 = (f32[2,24,128]{2,1,0:T(8,128)S(1)}, f32[2,24,128]{2,1,0:T(8,128)S(1)}, u32[]{:S(2)}, u32[]{:S(2)}) collective-permute-start(f32[2,24,128]{2,1,0:T(8,128)S(1)} %pad_maximum_fusion.2.own_ref), channel_id=1, source_target_pairs={{0,4},{1,5},{2,6},{3,7},{4,0},{5,1},{6,2},{7,3},{8,12},{9,13},{10,... | collective-permute-start | bytes 73736 | tf_op jit(solution)/shard_map/ppermute | solution.py:287
  47.7 3.1 %collective-permute-done.3.m2_ref = f32[2,24,128]{2,1,0:T(8,128)S(1)} collective-permute-done((f32[2,24,128]{2,1,0:T(8,128)S(1)}, f32[2,24,128]{2,1,0:T(8,128)S(1)}, u32[]{:S(2)}, u32[]{:S(2)}) %collective-permute-start.3) | collective-permute-done | bytes 24608 | tf_op jit(solution)/shard_map/ppermute | solution.py:287
  50.9 2.4 %project_kv.1 = (bf16[400,256]{1,0:T(8,128)(2,1)S(1)}, bf16[400,4096]{1,0:T(8,128)(2,1)S(1)}, f32[1,4096]{1,0:T(1,128)S(1)}) custom-call(bf16[384,4096]{1,0:T(8,128)(2,1)S(1)} %copy-done.2, bf16[16,4096]{1,0:T(8,128)(2,1)S(1)} %copy-done.9, f32[384,128]{1,0:T(8,128)S(1)} %get-tuple-element.100.rx_ref, f32[16,128]{1,0:T(8,128)S(1)} %get-tuple-element.101.rc_ref, ...), custom_call_target="tpu_custom_call" | custom-call | flops 805306368 | bytes 4194304 | tf_op jit(solution)/shard_map/project_kv/pallas_call | solution.py:369
  53.3 2.4 %collective-permute-start.4 = (bf16[400,256]{1,0:T(8,128)(2,1)S(1)}, bf16[400,256]{1,0:T(8,128)(2,1)S(1)}, u32[]{:S(2)}, u32[]{:S(2)}) collective-permute-start(bf16[400,256]{1,0:T(8,128)(2,1)S(1)} %get-tuple-element.108.refs_1_), channel_id=1, source_target_pairs={{0,120},{1,9},{2,122},{3,11},{4,124},{5,13},{6,126},{7,15},{8,0},{... | collective-permute-start | bytes 614408 | tf_op jit(solution)/shard_map/ppermute | solution.py:297
  55.8 1.7 %project_q.1.refs_0_ = bf16[768,128]{1,0:T(8,128)(2,1)S(1)} custom-call(bf16[400,4096]{1,0:T(8,128)(2,1)S(1)} %get-tuple-element.107.nm_ref, bf16[4096,256]{1,0:T(8,128)(2,1)S(1)} %copy-done.3, f32[1,128]{1,0:T(1,128)S(1)} %bitcast.39, f32[384,128]{1,0:T(8,128)S(1)} %pad_maximum_fusion.cos_ref, f32[384,128]{1,0:T(8,128)S(1)} %pad_maximum_fusion.1.sin_ref), custom_call_target="tpu_custom_call" | custom-call | flops 805306368 | bytes 4194304 | tf_op jit(solution)/shard_map/project_q/pallas_call | solution.py:391
  60.4 2.9 %collective-permute-start.5 = (bf16[400,256]{1,0:T(8,128)(2,1)S(1)}, bf16[400,256]{1,0:T(8,128)(2,1)S(1)}, u32[]{:S(2)}, u32[]{:S(2)}) collective-permute-start(bf16[400,256]{1,0:T(8,128)(2,1)S(1)} %collective-permute-done.4.refs_1_), channel_id=1, source_target_pairs={{0,120},{1,9},{2,122},{3,11},{4,124},{5,13},{6,126},{7,15},{8,0},{... | collective-permute-start | bytes 614408 | tf_op jit(solution)/shard_map/ppermute | solution.py:297
  67.6 3.7 %collective-permute-start.7 = (bf16[400,256]{1,0:T(8,128)(2,1)S(1)}, bf16[400,256]{1,0:T(8,128)(2,1)S(1)}, u32[]{:S(2)}, u32[]{:S(2)}) collective-permute-start(bf16[400,256]{1,0:T(8,128)(2,1)S(1)} %collective-permute-done.5.refs_1_), channel_id=1, source_target_pairs={{0,120},{1,9},{2,122},{3,11},{4,124},{5,13},{6,126},{7,15},{8,0},{... | collective-permute-start | bytes 614408 | tf_op jit(solution)/shard_map/ppermute | solution.py:297
  74.8 3.7 %collective-permute-start.9 = (bf16[400,256]{1,0:T(8,128)(2,1)S(1)}, bf16[400,256]{1,0:T(8,128)(2,1)S(1)}, u32[]{:S(2)}, u32[]{:S(2)}) collective-permute-start(bf16[400,256]{1,0:T(8,128)(2,1)S(1)} %collective-permute-done.7.refs_1_), channel_id=1, source_target_pairs={{0,120},{1,9},{2,122},{3,11},{4,124},{5,13},{6,126},{7,15},{8,0},{... | collective-permute-start | bytes 614408 | tf_op jit(solution)/shard_map/ppermute | solution.py:297
  81.9 3.5 %collective-permute-start.11 = (bf16[400,256]{1,0:T(8,128)(2,1)S(1)}, bf16[400,256]{1,0:T(8,128)(2,1)S(1)}, u32[]{:S(2)}, u32[]{:S(2)}) collective-permute-start(bf16[400,256]{1,0:T(8,128)(2,1)S(1)} %collective-permute-done.9.refs_1_), channel_id=1, source_target_pairs={{0,120},{1,9},{2,122},{3,11},{4,124},{5,13},{6,126},{7,15},{8,0},{... | collective-permute-start | bytes 614408 | tf_op jit(solution)/shard_map/ppermute | solution.py:297
  88.9 3.5 %collective-permute-start.13 = (bf16[400,256]{1,0:T(8,128)(2,1)S(1)}, bf16[400,256]{1,0:T(8,128)(2,1)S(1)}, u32[]{:S(2)}, u32[]{:S(2)}) collective-permute-start(bf16[400,256]{1,0:T(8,128)(2,1)S(1)} %collective-permute-done.11.refs_1_), channel_id=1, source_target_pairs={{0,120},{1,9},{2,122},{3,11},{4,124},{5,13},{6,126},{7,15},{8,0},{... | collective-permute-start | bytes 614408 | tf_op jit(solution)/shard_map/ppermute | solution.py:297
  96.1 3.7 %collective-permute-start.15 = (bf16[400,256]{1,0:T(8,128)(2,1)S(1)}, bf16[400,256]{1,0:T(8,128)(2,1)S(1)}, u32[]{:S(2)}, u32[]{:S(2)}) collective-permute-start(bf16[400,256]{1,0:T(8,128)(2,1)S(1)} %collective-permute-done.13.refs_1_), channel_id=1, source_target_pairs={{0,120},{1,9},{2,122},{3,11},{4,124},{5,13},{6,126},{7,15},{8,0},{... | collective-permute-start | bytes 614408 | tf_op jit(solution)/shard_map/ppermute | solution.py:297
  103.3 3.6 %collective-permute-start.17 = (bf16[400,256]{1,0:T(8,128)(2,1)S(1)}, bf16[400,256]{1,0:T(8,128)(2,1)S(1)}, u32[]{:S(2)}, u32[]{:S(2)}) collective-permute-start(bf16[400,256]{1,0:T(8,128)(2,1)S(1)} %collective-permute-done.15.refs_1_), channel_id=1, source_target_pairs={{0,120},{1,9},{2,122},{3,11},{4,124},{5,13},{6,126},{7,15},{8,0},{... | collective-permute-start | bytes 614408 | tf_op jit(solution)/shard_map/ppermute | solution.py:297
  112.3 1.7 %collective-permute-done.19 = bf16[48,4096]{1,0:T(8,128)(2,1)S(1)} collective-permute-done((bf16[48,4096]{1,0:T(8,128)(2,1)S(1)}, bf16[48,4096]{1,0:T(8,128)(2,1)S(1)}, u32[]{:S(2)}, u32[]{:S(2)}) %collective-permute-start.19) | collective-permute-done | bytes 393248 | tf_op jit(solution)/shard_map/ppermute | solution.py:302
  115.5 3.1 %collective-permute-start.25 = (bf16[48,2048]{1,0:T(8,128)(2,1)S(1)}, bf16[48,2048]{1,0:T(8,128)(2,1)S(1)}, u32[]{:S(2)}, u32[]{:S(2)}) collective-permute-start(bf16[48,2048]{1,0:T(8,128)(2,1)S(1)} %get-tuple-element.195), channel_id=1, source_target_pairs={{0,6},{1,7},{2,0},{3,1},{4,2},{5,3},{6,4},{7,5},{8,14},{9,15},{10,... | collective-permute-start | bytes 589832 | tf_op jit(solution)/shard_map/ppermute | solution.py:287
  119.2 4.6 %collective-permute-done.21 = bf16[48,2048]{1,0:T(8,128)(2,1)S(1)} collective-permute-done((bf16[48,2048]{1,0:T(8,128)(2,1)S(1)}, bf16[48,2048]{1,0:T(8,128)(2,1)S(1)}, u32[]{:S(2)}, u32[]{:S(2)}) %collective-permute-start.21) | collective-permute-done | bytes 196640 | tf_op jit(solution)/shard_map/ppermute | solution.py:287
  124.1 3.1 %collective-permute-start.26 = (bf16[48,2048]{1,0:T(8,128)(2,1)S(1)}, bf16[48,2048]{1,0:T(8,128)(2,1)S(1)}, u32[]{:S(2)}, u32[]{:S(2)}) collective-permute-start(bf16[48,2048]{1,0:T(8,128)(2,1)S(1)} %get-tuple-element.189), channel_id=1, source_target_pairs={{0,6},{1,7},{2,0},{3,1},{4,2},{5,3},{6,4},{7,5},{8,14},{9,15},{10,... | collective-permute-start | bytes 589832 | tf_op jit(solution)/shard_map/ppermute | solution.py:287
  127.4 3.2 %collective-permute-start.24 = (bf16[48,2048]{1,0:T(8,128)(2,1)S(1)}, bf16[48,2048]{1,0:T(8,128)(2,1)S(1)}, u32[]{:S(2)}, u32[]{:S(2)}) collective-permute-start(bf16[48,2048]{1,0:T(8,128)(2,1)S(1)} %get-tuple-element.191), channel_id=1, source_target_pairs={{0,6},{1,7},{2,0},{3,1},{4,2},{5,3},{6,4},{7,5},{8,14},{9,15},{10,... | collective-permute-start | bytes 589832 | tf_op jit(solution)/shard_map/ppermute | solution.py:287
  130.7 2.2 %collective-permute-done.22 = bf16[48,2048]{1,0:T(8,128)(2,1)S(1)} collective-permute-done((bf16[48,2048]{1,0:T(8,128)(2,1)S(1)}, bf16[48,2048]{1,0:T(8,128)(2,1)S(1)}, u32[]{:S(2)}, u32[]{:S(2)}) %collective-permute-start.22) | collective-permute-done | bytes 196640 | tf_op jit(solution)/shard_map/ppermute | solution.py:287
  132.9 2.8 %collective-permute-done.23 = bf16[48,2048]{1,0:T(8,128)(2,1)S(1)} collective-permute-done((bf16[48,2048]{1,0:T(8,128)(2,1)S(1)}, bf16[48,2048]{1,0:T(8,128)(2,1)S(1)}, u32[]{:S(2)}, u32[]{:S(2)}) %collective-permute-start.23) | collective-permute-done | bytes 196640 | tf_op jit(solution)/shard_map/ppermute | solution.py:287
  (102 shorter events, 44.8 us)
Async XLA Ops:
  2.3 38.6 %all-to-all-start = ((bf16[16,32,128]{2,1,0:T(8,128)(2,1)}), bf16[16,32,128]{2,1,0:T(8,128)(2,1)S(1)}, u32[]{:S(2)}, u32[]{:S(2)}) async-start(bf16[16,32,128]{2,1,0:T(8,128)(2,1)} %modulation.1), calls=%async_computation | async-start | bytes 262144 | tf_op jit(solution)/shard_map/all_to_all | solution.py:333
  42.3 5.3 %collective-permute-start.1 = (f32[2,24,128]{2,1,0:T(8,128)S(1)}, f32[2,24,128]{2,1,0:T(8,128)S(1)}, u32[]{:S(2)}, u32[]{:S(2)}) collective-permute-start(f32[2,24,128]{2,1,0:T(8,128)S(1)} %pad_maximum_fusion.2.own_ref), channel_id=1, source_target_pairs={{0,2},{1,3},{2,4},{3,5},{4,6},{5,7},{6,0},{7,1},{8,10},{9,11},{10,... | collective-permute-start | bytes 73736 | tf_op jit(solution)/shard_map/ppermute | solution.py:287
  45.5 5.3 %collective-permute-start.3 = (f32[2,24,128]{2,1,0:T(8,128)S(1)}, f32[2,24,128]{2,1,0:T(8,128)S(1)}, u32[]{:S(2)}, u32[]{:S(2)}) collective-permute-start(f32[2,24,128]{2,1,0:T(8,128)S(1)} %pad_maximum_fusion.2.own_ref), channel_id=1, source_target_pairs={{0,4},{1,5},{2,6},{3,7},{4,0},{5,1},{6,2},{7,3},{8,12},{9,13},{10,... | collective-permute-start | bytes 73736 | tf_op jit(solution)/shard_map/ppermute | solution.py:287
  53.3 7.1 %collective-permute-start.4 = (bf16[400,256]{1,0:T(8,128)(2,1)S(1)}, bf16[400,256]{1,0:T(8,128)(2,1)S(1)}, u32[]{:S(2)}, u32[]{:S(2)}) collective-permute-start(bf16[400,256]{1,0:T(8,128)(2,1)S(1)} %get-tuple-element.108.refs_1_), channel_id=1, source_target_pairs={{0,120},{1,9},{2,122},{3,11},{4,124},{5,13},{6,126},{7,15},{8,0},{... | collective-permute-start | bytes 614408 | tf_op jit(solution)/shard_map/ppermute | solution.py:297
  55.8 9.1 %collective-permute-start.6 = (bf16[400,256]{1,0:T(8,128)(2,1)S(1)}, bf16[400,256]{1,0:T(8,128)(2,1)S(1)}, u32[]{:S(2)}, u32[]{:S(2)}) collective-permute-start(bf16[400,256]{1,0:T(8,128)(2,1)S(1)} %get-tuple-element.108.refs_1_), channel_id=1, source_target_pairs={{0,8},{1,121},{2,10},{3,123},{4,12},{5,125},{6,14},{7,127},{8,16},... | collective-permute-start | bytes 614408 | tf_op jit(solution)/shard_map/ppermute | solution.py:297
  60.4 7.2 %collective-permute-start.5 = (bf16[400,256]{1,0:T(8,128)(2,1)S(1)}, bf16[400,256]{1,0:T(8,128)(2,1)S(1)}, u32[]{:S(2)}, u32[]{:S(2)}) collective-permute-start(bf16[400,256]{1,0:T(8,128)(2,1)S(1)} %collective-permute-done.4.refs_1_), channel_id=1, source_target_pairs={{0,120},{1,9},{2,122},{3,11},{4,124},{5,13},{6,126},{7,15},{8,0},{... | collective-permute-start | bytes 614408 | tf_op jit(solution)/shard_map/ppermute | solution.py:297
  64.9 8.0 %collective-permute-start.8 = (bf16[400,256]{1,0:T(8,128)(2,1)S(1)}, bf16[400,256]{1,0:T(8,128)(2,1)S(1)}, u32[]{:S(2)}, u32[]{:S(2)}) collective-permute-start(bf16[400,256]{1,0:T(8,128)(2,1)S(1)} %collective-permute-done.6.refs_1_), channel_id=1, source_target_pairs={{0,8},{1,121},{2,10},{3,123},{4,12},{5,125},{6,14},{7,127},{8,16},... | collective-permute-start | bytes 614408 | tf_op jit(solution)/shard_map/ppermute | solution.py:297
  67.6 7.2 %collective-permute-start.7 = (bf16[400,256]{1,0:T(8,128)(2,1)S(1)}, bf16[400,256]{1,0:T(8,128)(2,1)S(1)}, u32[]{:S(2)}, u32[]{:S(2)}) collective-permute-start(bf16[400,256]{1,0:T(8,128)(2,1)S(1)} %collective-permute-done.5.refs_1_), channel_id=1, source_target_pairs={{0,120},{1,9},{2,122},{3,11},{4,124},{5,13},{6,126},{7,15},{8,0},{... | collective-permute-start | bytes 614408 | tf_op jit(solution)/shard_map/ppermute | solution.py:297
  72.9 7.2 %collective-permute-start.10 = (bf16[400,256]{1,0:T(8,128)(2,1)S(1)}, bf16[400,256]{1,0:T(8,128)(2,1)S(1)}, u32[]{:S(2)}, u32[]{:S(2)}) collective-permute-start(bf16[400,256]{1,0:T(8,128)(2,1)S(1)} %collective-permute-done.8.refs_1_), channel_id=1, source_target_pairs={{0,8},{1,121},{2,10},{3,123},{4,12},{5,125},{6,14},{7,127},{8,16},... | collective-permute-start | bytes 614408 | tf_op jit(solution)/shard_map/ppermute | solution.py:297
  74.8 7.1 %collective-permute-start.9 = (bf16[400,256]{1,0:T(8,128)(2,1)S(1)}, bf16[400,256]{1,0:T(8,128)(2,1)S(1)}, u32[]{:S(2)}, u32[]{:S(2)}) collective-permute-start(bf16[400,256]{1,0:T(8,128)(2,1)S(1)} %collective-permute-done.7.refs_1_), channel_id=1, source_target_pairs={{0,120},{1,9},{2,122},{3,11},{4,124},{5,13},{6,126},{7,15},{8,0},{... | collective-permute-start | bytes 614408 | tf_op jit(solution)/shard_map/ppermute | solution.py:297
  80.1 7.1 %collective-permute-start.12 = (bf16[400,256]{1,0:T(8,128)(2,1)S(1)}, bf16[400,256]{1,0:T(8,128)(2,1)S(1)}, u32[]{:S(2)}, u32[]{:S(2)}) collective-permute-start(bf16[400,256]{1,0:T(8,128)(2,1)S(1)} %collective-permute-done.10.refs_1_), channel_id=1, source_target_pairs={{0,8},{1,121},{2,10},{3,123},{4,12},{5,125},{6,14},{7,127},{8,16},... | collective-permute-start | bytes 614408 | tf_op jit(solution)/shard_map/ppermute | solution.py:297
  81.9 7.0 %collective-permute-start.11 = (bf16[400,256]{1,0:T(8,128)(2,1)S(1)}, bf16[400,256]{1,0:T(8,128)(2,1)S(1)}, u32[]{:S(2)}, u32[]{:S(2)}) collective-permute-start(bf16[400,256]{1,0:T(8,128)(2,1)S(1)} %collective-permute-done.9.refs_1_), channel_id=1, source_target_pairs={{0,120},{1,9},{2,122},{3,11},{4,124},{5,13},{6,126},{7,15},{8,0},{... | collective-permute-start | bytes 614408 | tf_op jit(solution)/shard_map/ppermute | solution.py:297
  87.2 7.0 %collective-permute-start.14 = (bf16[400,256]{1,0:T(8,128)(2,1)S(1)}, bf16[400,256]{1,0:T(8,128)(2,1)S(1)}, u32[]{:S(2)}, u32[]{:S(2)}) collective-permute-start(bf16[400,256]{1,0:T(8,128)(2,1)S(1)} %collective-permute-done.12.refs_1_), channel_id=1, source_target_pairs={{0,8},{1,121},{2,10},{3,123},{4,12},{5,125},{6,14},{7,127},{8,16},... | collective-permute-start | bytes 614408 | tf_op jit(solution)/shard_map/ppermute | solution.py:297
  88.9 7.3 %collective-permute-start.13 = (bf16[400,256]{1,0:T(8,128)(2,1)S(1)}, bf16[400,256]{1,0:T(8,128)(2,1)S(1)}, u32[]{:S(2)}, u32[]{:S(2)}) collective-permute-start(bf16[400,256]{1,0:T(8,128)(2,1)S(1)} %collective-permute-done.11.refs_1_), channel_id=1, source_target_pairs={{0,120},{1,9},{2,122},{3,11},{4,124},{5,13},{6,126},{7,15},{8,0},{... | collective-permute-start | bytes 614408 | tf_op jit(solution)/shard_map/ppermute | solution.py:297
  94.2 7.5 %collective-permute-start.16 = (bf16[400,256]{1,0:T(8,128)(2,1)S(1)}, bf16[400,256]{1,0:T(8,128)(2,1)S(1)}, u32[]{:S(2)}, u32[]{:S(2)}) collective-permute-start(bf16[400,256]{1,0:T(8,128)(2,1)S(1)} %collective-permute-done.14.refs_1_), channel_id=1, source_target_pairs={{0,8},{1,121},{2,10},{3,123},{4,12},{5,125},{6,14},{7,127},{8,16},... | collective-permute-start | bytes 614408 | tf_op jit(solution)/shard_map/ppermute | solution.py:297
  96.1 7.1 %collective-permute-start.15 = (bf16[400,256]{1,0:T(8,128)(2,1)S(1)}, bf16[400,256]{1,0:T(8,128)(2,1)S(1)}, u32[]{:S(2)}, u32[]{:S(2)}) collective-permute-start(bf16[400,256]{1,0:T(8,128)(2,1)S(1)} %collective-permute-done.13.refs_1_), channel_id=1, source_target_pairs={{0,120},{1,9},{2,122},{3,11},{4,124},{5,13},{6,126},{7,15},{8,0},{... | collective-permute-start | bytes 614408 | tf_op jit(solution)/shard_map/ppermute | solution.py:297
  101.6 7.0 %collective-permute-start.18 = (bf16[400,256]{1,0:T(8,128)(2,1)S(1)}, bf16[400,256]{1,0:T(8,128)(2,1)S(1)}, u32[]{:S(2)}, u32[]{:S(2)}) collective-permute-start(bf16[400,256]{1,0:T(8,128)(2,1)S(1)} %collective-permute-done.16.refs_1_), channel_id=1, source_target_pairs={{0,8},{1,121},{2,10},{3,123},{4,12},{5,125},{6,14},{7,127},{8,16},... | collective-permute-start | bytes 614408 | tf_op jit(solution)/shard_map/ppermute | solution.py:297
  103.3 7.0 %collective-permute-start.17 = (bf16[400,256]{1,0:T(8,128)(2,1)S(1)}, bf16[400,256]{1,0:T(8,128)(2,1)S(1)}, u32[]{:S(2)}, u32[]{:S(2)}) collective-permute-start(bf16[400,256]{1,0:T(8,128)(2,1)S(1)} %collective-permute-done.15.refs_1_), channel_id=1, source_target_pairs={{0,120},{1,9},{2,122},{3,11},{4,124},{5,13},{6,126},{7,15},{8,0},{... | collective-permute-start | bytes 614408 | tf_op jit(solution)/shard_map/ppermute | solution.py:297
  115.3 8.5 %collective-permute-start.21 = (bf16[48,2048]{1,0:T(8,128)(2,1)S(1)}, bf16[48,2048]{1,0:T(8,128)(2,1)S(1)}, u32[]{:S(2)}, u32[]{:S(2)}) collective-permute-start(bf16[48,2048]{1,0:T(8,128)(2,1)S(1)} %get-tuple-element.196), channel_id=1, source_target_pairs={{0,2},{1,3},{2,4},{3,5},{4,6},{5,7},{6,0},{7,1},{8,10},{9,11},{10,... | collective-permute-start | bytes 589832 | tf_op jit(solution)/shard_map/ppermute | solution.py:287
  115.5 8.3 %collective-permute-start.25 = (bf16[48,2048]{1,0:T(8,128)(2,1)S(1)}, bf16[48,2048]{1,0:T(8,128)(2,1)S(1)}, u32[]{:S(2)}, u32[]{:S(2)}) collective-permute-start(bf16[48,2048]{1,0:T(8,128)(2,1)S(1)} %get-tuple-element.195), channel_id=1, source_target_pairs={{0,6},{1,7},{2,0},{3,1},{4,2},{5,3},{6,4},{7,5},{8,14},{9,15},{10,... | collective-permute-start | bytes 589832 | tf_op jit(solution)/shard_map/ppermute | solution.py:287
  123.9 9.0 %collective-permute-start.22 = (bf16[48,2048]{1,0:T(8,128)(2,1)S(1)}, bf16[48,2048]{1,0:T(8,128)(2,1)S(1)}, u32[]{:S(2)}, u32[]{:S(2)}) collective-permute-start(bf16[48,2048]{1,0:T(8,128)(2,1)S(1)} %get-tuple-element.190), channel_id=1, source_target_pairs={{0,2},{1,3},{2,4},{3,5},{4,6},{5,7},{6,0},{7,1},{8,10},{9,11},{10,... | collective-permute-start | bytes 589832 | tf_op jit(solution)/shard_map/ppermute | solution.py:287
  124.1 8.8 %collective-permute-start.26 = (bf16[48,2048]{1,0:T(8,128)(2,1)S(1)}, bf16[48,2048]{1,0:T(8,128)(2,1)S(1)}, u32[]{:S(2)}, u32[]{:S(2)}) collective-permute-start(bf16[48,2048]{1,0:T(8,128)(2,1)S(1)} %get-tuple-element.189), channel_id=1, source_target_pairs={{0,6},{1,7},{2,0},{3,1},{4,2},{5,3},{6,4},{7,5},{8,14},{9,15},{10,... | collective-permute-start | bytes 589832 | tf_op jit(solution)/shard_map/ppermute | solution.py:287
  127.3 8.5 %collective-permute-start.23 = (bf16[48,2048]{1,0:T(8,128)(2,1)S(1)}, bf16[48,2048]{1,0:T(8,128)(2,1)S(1)}, u32[]{:S(2)}, u32[]{:S(2)}) collective-permute-start(bf16[48,2048]{1,0:T(8,128)(2,1)S(1)} %get-tuple-element.192), channel_id=1, source_target_pairs={{0,2},{1,3},{2,4},{3,5},{4,6},{5,7},{6,0},{7,1},{8,10},{9,11},{10,... | collective-permute-start | bytes 589832 | tf_op jit(solution)/shard_map/ppermute | solution.py:287
  127.4 8.3 %collective-permute-start.24 = (bf16[48,2048]{1,0:T(8,128)(2,1)S(1)}, bf16[48,2048]{1,0:T(8,128)(2,1)S(1)}, u32[]{:S(2)}, u32[]{:S(2)}) collective-permute-start(bf16[48,2048]{1,0:T(8,128)(2,1)S(1)} %get-tuple-element.191), channel_id=1, source_target_pairs={{0,6},{1,7},{2,0},{3,1},{4,2},{5,3},{6,4},{7,5},{8,14},{9,15},{10,... | collective-permute-start | bytes 589832 | tf_op jit(solution)/shard_map/ppermute | solution.py:287
  (19 other events, 201.0 us)

commit v4 on v3

--- a/solution.py
+++ b/solution.py
@@ -226,19 +226,18 @@
     for kv_ref, vt_ref in zip(kv_refs, vt_refs, strict=True):
         vt_ref[...] = jnp.transpose(kv_ref[:, HEAD:])
     queries = q_ref.shape[0]
-    width = 256
     if last:
-        for i in range(0, queries, width):
-            attend_block(q_ref, kv_refs, vt_refs, m_ref, l_ref, acc_ref, slice(i, i + width), latents)
+        attend_block(q_ref, kv_refs, vt_refs, m_ref, l_ref, acc_ref, slice(0, queries), latents)
         for h in range(queries // tok):
             cols = slice(h * tok, (h + 1) * tok)
             done = acc_ref[:, cols] / l_ref[0:1, cols]
             out_ref[:, h * HEAD:(h + 1) * HEAD] = jnp.transpose(done).astype(BF16)
     else:
 
-        @pl.loop(0, queries // width)
+
+        @pl.loop(0, queries // tok)
         def _(i):
-            cols = pl.ds(pl.multiple_of(i * width, width), width)
+            cols = pl.ds(pl.multiple_of(i * tok, tok), tok)
             attend_block(q_ref, kv_refs, vt_refs, m_ref, l_ref, acc_ref, cols, latents)
 
 

time: 137 us -> 138 us (level)
  waiting for transfers between devices: 21.4 us -> 29.6 us
  Pallas kernels: 35.4 us -> 29.3 us
  starting transfers between devices: 67.5 us -> 66.1 us
    ppermute x15, waiting for transfers between devices: 3.05 us -> 11.2 us  [along_ring(): return lax.ppermute(x, ('sp', 'tp'), pairs)]
    pallas_call x15, Pallas kernels: 24.3 us -> 18.4 us  [attend(): pl.pallas_call(kernel, out_shape=shapes, in_specs=[VM] * len(operands), o...]
    ppermute x15, starting transfers between devices: 27.7 us -> 26.2 us  [along_ring(): return lax.ppermute(x, ('sp', 'tp'), pairs)]
  transfers between devices with their start and end apart: 28 -> 28, of which waited for: 16 -> 16; matrix products, arithmetic and copies ran while one was open for 2% -> 2% of each run, Pallas kernels for 22% -> 17%
where the time goes in v4:
time: 138 us; the launch traced here: 137 us
  starting transfers between devices  66.1 us (48%)
  waiting for transfers between devices  29.6 us (21%)
  Pallas kernels  29.3 us (21%)
  local copies, waits for them, and re-layouts  6.73 us (5%)
  other arithmetic  3.01 us (2%)
  matrix products  2 us (1%)
    ppermute x15, starting transfers between devices, along_ring(): return lax.ppermute(x, ('sp', 'tp'), pairs)  26.2 us
    all_to_all x1, starting transfers between devices, body(): lax.all_to_all(partial_mod, 'sp', split_axis=0, concat_axis=0, tiled=True)  24 us
    pallas_call x15, Pallas kernels, attend(): pl.pallas_call(kernel, out_shape=shapes, in_specs=[VM] * len(operands), o...  18.4 us
    ppermute x9, starting transfers between devices, shifted(): return lax.ppermute(x, axis, [(i, (i + by) % n) for i in range(n)])  15.4 us
    ppermute x9, waiting for transfers between devices, shifted(): return lax.ppermute(x, axis, [(i, (i + by) % n) for i in range(n)])  12.9 us
    ppermute x15, waiting for transfers between devices, along_ring(): return lax.ppermute(x, ('sp', 'tp'), pairs)  11.2 us
    unnamed x30, local copies, waits for them, and re-layouts  6.62 us
    pallas_call x1, Pallas kernels, body(): pl.pallas_call(prepare_kernel, out_shape=[jax.ShapeDtypeStruct((tok, 128)...  3.46 us
  transfers between devices with their start and end apart: 28, of which 16 were waited for; matrix products, arithmetic and copies ran while one was open for 2% of the time, Pallas kernels for 17%

profile of v4, /device:TPU:40, one launch (start us, length us, event | category | flops | bytes accessed | tf_op | source)
XLA Modules:
  0.0 137.2 jit_solution(18073908154545825336)
XLA Ops:
  0.0 2.3 %modulation.1 = bf16[16,32,128]{2,1,0:T(8,128)(2,1)} custom-call(bf16[32,128]{1,0:T(8,128)(2,1)} %bitcast.42, bf16[32,128]{1,0:T(8,128)(2,1)} %bitcast.43, bf16[256,512]{1,0:T(8,128)(2,1)} %scale_hbm.1, bf16[256,512]{1,0:T(8,128)(2,1)} %shift_hbm.1, bf16[256,512]{1,0:T(8,128)(2,1)} %gate_hbm.1), custom_call_target="tpu_custom_call" | custom-call | tf_op jit(solution)/shard_map/modulation/pallas_call | solution.py:318
  2.3 24.0 %all-to-all-start = ((bf16[16,32,128]{2,1,0:T(8,128)(2,1)}), bf16[16,32,128]{2,1,0:T(8,128)(2,1)S(1)}, u32[]{:S(2)}, u32[]{:S(2)}) async-start(bf16[16,32,128]{2,1,0:T(8,128)(2,1)} %modulation.1), calls=%async_computation | async-start | bytes 262144 | tf_op jit(solution)/shard_map/all_to_all | solution.py:332
  26.4 1.9 %copy-done.1 = bf16[384,4096]{1,0:T(8,128)(2,1)S(1)} copy-done((bf16[384,4096]{1,0:T(8,128)(2,1)S(1)}, bf16[384,4096]{1,0:T(8,128)(2,1)}, u32[]{:S(2)}) %copy-start.1) | copy-done | bytes 3145752
  31.6 3.5 %prepare.1 = (f32[384,128]{1,0:T(8,128)S(1)}, f32[16,128]{1,0:T(8,128)S(1)}, bf16[4096,256]{1,0:T(8,128)(2,1)S(1)}) custom-call(bf16[384,4096]{1,0:T(8,128)(2,1)S(1)} %copy-done.1, bf16[16,4096]{1,0:T(8,128)(2,1)S(1)} %copy-done.8, bf16[4096,128]{1,0:T(8,128)(2,1)S(1)} %copy-done.6, bf16[4096,128]{1,0:T(8,128)(2,1)S(1)} %copy-done.7), custom_call_target="tpu_custom_call" | custom-call | flops 1073741824 | bytes 12582912 | tf_op jit(solution)/shard_map/prepare/pallas_call | solution.py:333
  38.3 2.6 %all-to-all-done.in_ref = bf16[16,32,128]{2,1,0:T(8,128)(2,1)S(1)} async-done(((bf16[16,32,128]{2,1,0:T(8,128)(2,1)}), bf16[16,32,128]{2,1,0:T(8,128)(2,1)S(1)}, u32[]{:S(2)}, u32[]{:S(2)}) %all-to-all-start) | async-done | bytes 131104 | tf_op jit(solution)/shard_map/all_to_all | solution.py:332
  45.5 2.1 %collective-permute-start.3 = (f32[2,24,128]{2,1,0:T(8,128)S(1)}, f32[2,24,128]{2,1,0:T(8,128)S(1)}, u32[]{:S(2)}, u32[]{:S(2)}) collective-permute-start(f32[2,24,128]{2,1,0:T(8,128)S(1)} %pad_maximum_fusion.2.own_ref), channel_id=1, source_target_pairs={{0,4},{1,5},{2,6},{3,7},{4,0},{5,1},{6,2},{7,3},{8,12},{9,13},{10,... | collective-permute-start | bytes 73736 | tf_op jit(solution)/shard_map/ppermute | solution.py:286
  47.7 3.1 %collective-permute-done.3.m2_ref = f32[2,24,128]{2,1,0:T(8,128)S(1)} collective-permute-done((f32[2,24,128]{2,1,0:T(8,128)S(1)}, f32[2,24,128]{2,1,0:T(8,128)S(1)}, u32[]{:S(2)}, u32[]{:S(2)}) %collective-permute-start.3) | collective-permute-done | bytes 24608 | tf_op jit(solution)/shard_map/ppermute | solution.py:286
  50.9 2.4 %project_kv.1 = (bf16[400,256]{1,0:T(8,128)(2,1)S(1)}, bf16[400,4096]{1,0:T(8,128)(2,1)S(1)}, f32[1,4096]{1,0:T(1,128)S(1)}) custom-call(bf16[384,4096]{1,0:T(8,128)(2,1)S(1)} %copy-done.2, bf16[16,4096]{1,0:T(8,128)(2,1)S(1)} %copy-done.9, f32[384,128]{1,0:T(8,128)S(1)} %get-tuple-element.100.rx_ref, f32[16,128]{1,0:T(8,128)S(1)} %get-tuple-element.101.rc_ref, ...), custom_call_target="tpu_custom_call" | custom-call | flops 805306368 | bytes 4194304 | tf_op jit(solution)/shard_map/project_kv/pallas_call | solution.py:368
  53.3 2.4 %collective-permute-start.4 = (bf16[400,256]{1,0:T(8,128)(2,1)S(1)}, bf16[400,256]{1,0:T(8,128)(2,1)S(1)}, u32[]{:S(2)}, u32[]{:S(2)}) collective-permute-start(bf16[400,256]{1,0:T(8,128)(2,1)S(1)} %get-tuple-element.108.refs_1_), channel_id=1, source_target_pairs={{0,120},{1,9},{2,122},{3,11},{4,124},{5,13},{6,126},{7,15},{8,0},{... | collective-permute-start | bytes 614408 | tf_op jit(solution)/shard_map/ppermute | solution.py:296
  58.7 1.7 %collective-permute-done.4.refs_1_ = bf16[400,256]{1,0:T(8,128)(2,1)S(1)} collective-permute-done((bf16[400,256]{1,0:T(8,128)(2,1)S(1)}, bf16[400,256]{1,0:T(8,128)(2,1)S(1)}, u32[]{:S(2)}, u32[]{:S(2)}) %collective-permute-start.4) | collective-permute-done | bytes 204832 | tf_op jit(solution)/shard_map/ppermute | solution.py:296
  60.4 2.9 %collective-permute-start.5 = (bf16[400,256]{1,0:T(8,128)(2,1)S(1)}, bf16[400,256]{1,0:T(8,128)(2,1)S(1)}, u32[]{:S(2)}, u32[]{:S(2)}) collective-permute-start(bf16[400,256]{1,0:T(8,128)(2,1)S(1)} %collective-permute-done.4.refs_1_), channel_id=1, source_target_pairs={{0,120},{1,9},{2,122},{3,11},{4,124},{5,13},{6,126},{7,15},{8,0},{... | collective-permute-start | bytes 614408 | tf_op jit(solution)/shard_map/ppermute | solution.py:296
  66.9 3.7 %collective-permute-start.7 = (bf16[400,256]{1,0:T(8,128)(2,1)S(1)}, bf16[400,256]{1,0:T(8,128)(2,1)S(1)}, u32[]{:S(2)}, u32[]{:S(2)}) collective-permute-start(bf16[400,256]{1,0:T(8,128)(2,1)S(1)} %collective-permute-done.5.refs_1_), channel_id=1, source_target_pairs={{0,120},{1,9},{2,122},{3,11},{4,124},{5,13},{6,126},{7,15},{8,0},{... | collective-permute-start | bytes 614408 | tf_op jit(solution)/shard_map/ppermute | solution.py:296
  74.2 3.4 %collective-permute-start.9 = (bf16[400,256]{1,0:T(8,128)(2,1)S(1)}, bf16[400,256]{1,0:T(8,128)(2,1)S(1)}, u32[]{:S(2)}, u32[]{:S(2)}) collective-permute-start(bf16[400,256]{1,0:T(8,128)(2,1)S(1)} %collective-permute-done.7.refs_1_), channel_id=1, source_target_pairs={{0,120},{1,9},{2,122},{3,11},{4,124},{5,13},{6,126},{7,15},{8,0},{... | collective-permute-start | bytes 614408 | tf_op jit(solution)/shard_map/ppermute | solution.py:296
  81.5 3.3 %collective-permute-start.11 = (bf16[400,256]{1,0:T(8,128)(2,1)S(1)}, bf16[400,256]{1,0:T(8,128)(2,1)S(1)}, u32[]{:S(2)}, u32[]{:S(2)}) collective-permute-start(bf16[400,256]{1,0:T(8,128)(2,1)S(1)} %collective-permute-done.9.refs_1_), channel_id=1, source_target_pairs={{0,120},{1,9},{2,122},{3,11},{4,124},{5,13},{6,126},{7,15},{8,0},{... | collective-permute-start | bytes 614408 | tf_op jit(solution)/shard_map/ppermute | solution.py:296
  88.4 3.3 %collective-permute-start.13 = (bf16[400,256]{1,0:T(8,128)(2,1)S(1)}, bf16[400,256]{1,0:T(8,128)(2,1)S(1)}, u32[]{:S(2)}, u32[]{:S(2)}) collective-permute-start(bf16[400,256]{1,0:T(8,128)(2,1)S(1)} %collective-permute-done.11.refs_1_), channel_id=1, source_target_pairs={{0,120},{1,9},{2,122},{3,11},{4,124},{5,13},{6,126},{7,15},{8,0},{... | collective-permute-start | bytes 614408 | tf_op jit(solution)/shard_map/ppermute | solution.py:296
  95.7 3.4 %collective-permute-start.15 = (bf16[400,256]{1,0:T(8,128)(2,1)S(1)}, bf16[400,256]{1,0:T(8,128)(2,1)S(1)}, u32[]{:S(2)}, u32[]{:S(2)}) collective-permute-start(bf16[400,256]{1,0:T(8,128)(2,1)S(1)} %collective-permute-done.13.refs_1_), channel_id=1, source_target_pairs={{0,120},{1,9},{2,122},{3,11},{4,124},{5,13},{6,126},{7,15},{8,0},{... | collective-permute-start | bytes 614408 | tf_op jit(solution)/shard_map/ppermute | solution.py:296
  100.3 2.5 %collective-permute-done.16.refs_1_ = bf16[400,256]{1,0:T(8,128)(2,1)S(1)} collective-permute-done((bf16[400,256]{1,0:T(8,128)(2,1)S(1)}, bf16[400,256]{1,0:T(8,128)(2,1)S(1)}, u32[]{:S(2)}, u32[]{:S(2)}) %collective-permute-start.16) | collective-permute-done | bytes 204832 | tf_op jit(solution)/shard_map/ppermute | solution.py:296
  104.0 3.3 %collective-permute-start.17 = (bf16[400,256]{1,0:T(8,128)(2,1)S(1)}, bf16[400,256]{1,0:T(8,128)(2,1)S(1)}, u32[]{:S(2)}, u32[]{:S(2)}) collective-permute-start(bf16[400,256]{1,0:T(8,128)(2,1)S(1)} %collective-permute-done.15.refs_1_), channel_id=1, source_target_pairs={{0,120},{1,9},{2,122},{3,11},{4,124},{5,13},{6,126},{7,15},{8,0},{... | collective-permute-start | bytes 614408 | tf_op jit(solution)/shard_map/ppermute | solution.py:296
  116.1 3.0 %collective-permute-start.25 = (bf16[48,2048]{1,0:T(8,128)(2,1)S(1)}, bf16[48,2048]{1,0:T(8,128)(2,1)S(1)}, u32[]{:S(2)}, u32[]{:S(2)}) collective-permute-start(bf16[48,2048]{1,0:T(8,128)(2,1)S(1)} %get-tuple-element.195), channel_id=1, source_target_pairs={{0,6},{1,7},{2,0},{3,1},{4,2},{5,3},{6,4},{7,5},{8,14},{9,15},{10,... | collective-permute-start | bytes 589832 | tf_op jit(solution)/shard_map/ppermute | solution.py:286
  119.7 4.6 %collective-permute-done.21 = bf16[48,2048]{1,0:T(8,128)(2,1)S(1)} collective-permute-done((bf16[48,2048]{1,0:T(8,128)(2,1)S(1)}, bf16[48,2048]{1,0:T(8,128)(2,1)S(1)}, u32[]{:S(2)}, u32[]{:S(2)}) %collective-permute-start.21) | collective-permute-done | bytes 196640 | tf_op jit(solution)/shard_map/ppermute | solution.py:286
  124.8 2.9 %collective-permute-start.26 = (bf16[48,2048]{1,0:T(8,128)(2,1)S(1)}, bf16[48,2048]{1,0:T(8,128)(2,1)S(1)}, u32[]{:S(2)}, u32[]{:S(2)}) collective-permute-start(bf16[48,2048]{1,0:T(8,128)(2,1)S(1)} %get-tuple-element.189), channel_id=1, source_target_pairs={{0,6},{1,7},{2,0},{3,1},{4,2},{5,3},{6,4},{7,5},{8,14},{9,15},{10,... | collective-permute-start | bytes 589832 | tf_op jit(solution)/shard_map/ppermute | solution.py:286
  127.9 3.2 %collective-permute-start.24 = (bf16[48,2048]{1,0:T(8,128)(2,1)S(1)}, bf16[48,2048]{1,0:T(8,128)(2,1)S(1)}, u32[]{:S(2)}, u32[]{:S(2)}) collective-permute-start(bf16[48,2048]{1,0:T(8,128)(2,1)S(1)} %get-tuple-element.191), channel_id=1, source_target_pairs={{0,6},{1,7},{2,0},{3,1},{4,2},{5,3},{6,4},{7,5},{8,14},{9,15},{10,... | collective-permute-start | bytes 589832 | tf_op jit(solution)/shard_map/ppermute | solution.py:286
  131.2 2.2 %collective-permute-done.22 = bf16[48,2048]{1,0:T(8,128)(2,1)S(1)} collective-permute-done((bf16[48,2048]{1,0:T(8,128)(2,1)S(1)}, bf16[48,2048]{1,0:T(8,128)(2,1)S(1)}, u32[]{:S(2)}, u32[]{:S(2)}) %collective-permute-start.22) | collective-permute-done | bytes 196640 | tf_op jit(solution)/shard_map/ppermute | solution.py:286
  133.4 2.8 %collective-permute-done.23 = bf16[48,2048]{1,0:T(8,128)(2,1)S(1)} collective-permute-done((bf16[48,2048]{1,0:T(8,128)(2,1)S(1)}, bf16[48,2048]{1,0:T(8,128)(2,1)S(1)}, u32[]{:S(2)}, u32[]{:S(2)}) %collective-permute-start.23) | collective-permute-done | bytes 196640 | tf_op jit(solution)/shard_map/ppermute | solution.py:286
  (102 shorter events, 46.0 us)
Async XLA Ops:
  2.3 38.6 %all-to-all-start = ((bf16[16,32,128]{2,1,0:T(8,128)(2,1)}), bf16[16,32,128]{2,1,0:T(8,128)(2,1)S(1)}, u32[]{:S(2)}, u32[]{:S(2)}) async-start(bf16[16,32,128]{2,1,0:T(8,128)(2,1)} %modulation.1), calls=%async_computation | async-start | bytes 262144 | tf_op jit(solution)/shard_map/all_to_all | solution.py:332
  42.3 5.3 %collective-permute-start.1 = (f32[2,24,128]{2,1,0:T(8,128)S(1)}, f32[2,24,128]{2,1,0:T(8,128)S(1)}, u32[]{:S(2)}, u32[]{:S(2)}) collective-permute-start(f32[2,24,128]{2,1,0:T(8,128)S(1)} %pad_maximum_fusion.2.own_ref), channel_id=1, source_target_pairs={{0,2},{1,3},{2,4},{3,5},{4,6},{5,7},{6,0},{7,1},{8,10},{9,11},{10,... | collective-permute-start | bytes 73736 | tf_op jit(solution)/shard_map/ppermute | solution.py:286
  45.5 5.3 %collective-permute-start.3 = (f32[2,24,128]{2,1,0:T(8,128)S(1)}, f32[2,24,128]{2,1,0:T(8,128)S(1)}, u32[]{:S(2)}, u32[]{:S(2)}) collective-permute-start(f32[2,24,128]{2,1,0:T(8,128)S(1)} %pad_maximum_fusion.2.own_ref), channel_id=1, source_target_pairs={{0,4},{1,5},{2,6},{3,7},{4,0},{5,1},{6,2},{7,3},{8,12},{9,13},{10,... | collective-permute-start | bytes 73736 | tf_op jit(solution)/shard_map/ppermute | solution.py:286
  53.3 7.1 %collective-permute-start.4 = (bf16[400,256]{1,0:T(8,128)(2,1)S(1)}, bf16[400,256]{1,0:T(8,128)(2,1)S(1)}, u32[]{:S(2)}, u32[]{:S(2)}) collective-permute-start(bf16[400,256]{1,0:T(8,128)(2,1)S(1)} %get-tuple-element.108.refs_1_), channel_id=1, source_target_pairs={{0,120},{1,9},{2,122},{3,11},{4,124},{5,13},{6,126},{7,15},{8,0},{... | collective-permute-start | bytes 614408 | tf_op jit(solution)/shard_map/ppermute | solution.py:296
  55.8 8.7 %collective-permute-start.6 = (bf16[400,256]{1,0:T(8,128)(2,1)S(1)}, bf16[400,256]{1,0:T(8,128)(2,1)S(1)}, u32[]{:S(2)}, u32[]{:S(2)}) collective-permute-start(bf16[400,256]{1,0:T(8,128)(2,1)S(1)} %get-tuple-element.108.refs_1_), channel_id=1, source_target_pairs={{0,8},{1,121},{2,10},{3,123},{4,12},{5,125},{6,14},{7,127},{8,16},... | collective-permute-start | bytes 614408 | tf_op jit(solution)/shard_map/ppermute | solution.py:296
  60.4 6.5 %collective-permute-start.5 = (bf16[400,256]{1,0:T(8,128)(2,1)S(1)}, bf16[400,256]{1,0:T(8,128)(2,1)S(1)}, u32[]{:S(2)}, u32[]{:S(2)}) collective-permute-start(bf16[400,256]{1,0:T(8,128)(2,1)S(1)} %collective-permute-done.4.refs_1_), channel_id=1, source_target_pairs={{0,120},{1,9},{2,122},{3,11},{4,124},{5,13},{6,126},{7,15},{8,0},{... | collective-permute-start | bytes 614408 | tf_op jit(solution)/shard_map/ppermute | solution.py:296
  64.5 8.4 %collective-permute-start.8 = (bf16[400,256]{1,0:T(8,128)(2,1)S(1)}, bf16[400,256]{1,0:T(8,128)(2,1)S(1)}, u32[]{:S(2)}, u32[]{:S(2)}) collective-permute-start(bf16[400,256]{1,0:T(8,128)(2,1)S(1)} %collective-permute-done.6.refs_1_), channel_id=1, source_target_pairs={{0,8},{1,121},{2,10},{3,123},{4,12},{5,125},{6,14},{7,127},{8,16},... | collective-permute-start | bytes 614408 | tf_op jit(solution)/shard_map/ppermute | solution.py:296
  66.9 7.2 %collective-permute-start.7 = (bf16[400,256]{1,0:T(8,128)(2,1)S(1)}, bf16[400,256]{1,0:T(8,128)(2,1)S(1)}, u32[]{:S(2)}, u32[]{:S(2)}) collective-permute-start(bf16[400,256]{1,0:T(8,128)(2,1)S(1)} %collective-permute-done.5.refs_1_), channel_id=1, source_target_pairs={{0,120},{1,9},{2,122},{3,11},{4,124},{5,13},{6,126},{7,15},{8,0},{... | collective-permute-start | bytes 614408 | tf_op jit(solution)/shard_map/ppermute | solution.py:296
  72.9 7.3 %collective-permute-start.10 = (bf16[400,256]{1,0:T(8,128)(2,1)S(1)}, bf16[400,256]{1,0:T(8,128)(2,1)S(1)}, u32[]{:S(2)}, u32[]{:S(2)}) collective-permute-start(bf16[400,256]{1,0:T(8,128)(2,1)S(1)} %collective-permute-done.8.refs_1_), channel_id=1, source_target_pairs={{0,8},{1,121},{2,10},{3,123},{4,12},{5,125},{6,14},{7,127},{8,16},... | collective-permute-start | bytes 614408 | tf_op jit(solution)/shard_map/ppermute | solution.py:296
  74.2 7.3 %collective-permute-start.9 = (bf16[400,256]{1,0:T(8,128)(2,1)S(1)}, bf16[400,256]{1,0:T(8,128)(2,1)S(1)}, u32[]{:S(2)}, u32[]{:S(2)}) collective-permute-start(bf16[400,256]{1,0:T(8,128)(2,1)S(1)} %collective-permute-done.7.refs_1_), channel_id=1, source_target_pairs={{0,120},{1,9},{2,122},{3,11},{4,124},{5,13},{6,126},{7,15},{8,0},{... | collective-permute-start | bytes 614408 | tf_op jit(solution)/shard_map/ppermute | solution.py:296
  80.2 7.0 %collective-permute-start.12 = (bf16[400,256]{1,0:T(8,128)(2,1)S(1)}, bf16[400,256]{1,0:T(8,128)(2,1)S(1)}, u32[]{:S(2)}, u32[]{:S(2)}) collective-permute-start(bf16[400,256]{1,0:T(8,128)(2,1)S(1)} %collective-permute-done.10.refs_1_), channel_id=1, source_target_pairs={{0,8},{1,121},{2,10},{3,123},{4,12},{5,125},{6,14},{7,127},{8,16},... | collective-permute-start | bytes 614408 | tf_op jit(solution)/shard_map/ppermute | solution.py:296
  81.5 7.0 %collective-permute-start.11 = (bf16[400,256]{1,0:T(8,128)(2,1)S(1)}, bf16[400,256]{1,0:T(8,128)(2,1)S(1)}, u32[]{:S(2)}, u32[]{:S(2)}) collective-permute-start(bf16[400,256]{1,0:T(8,128)(2,1)S(1)} %collective-permute-done.9.refs_1_), channel_id=1, source_target_pairs={{0,120},{1,9},{2,122},{3,11},{4,124},{5,13},{6,126},{7,15},{8,0},{... | collective-permute-start | bytes 614408 | tf_op jit(solution)/shard_map/ppermute | solution.py:296
  87.2 7.2 %collective-permute-start.14 = (bf16[400,256]{1,0:T(8,128)(2,1)S(1)}, bf16[400,256]{1,0:T(8,128)(2,1)S(1)}, u32[]{:S(2)}, u32[]{:S(2)}) collective-permute-start(bf16[400,256]{1,0:T(8,128)(2,1)S(1)} %collective-permute-done.12.refs_1_), channel_id=1, source_target_pairs={{0,8},{1,121},{2,10},{3,123},{4,12},{5,125},{6,14},{7,127},{8,16},... | collective-permute-start | bytes 614408 | tf_op jit(solution)/shard_map/ppermute | solution.py:296
  88.4 7.2 %collective-permute-start.13 = (bf16[400,256]{1,0:T(8,128)(2,1)S(1)}, bf16[400,256]{1,0:T(8,128)(2,1)S(1)}, u32[]{:S(2)}, u32[]{:S(2)}) collective-permute-start(bf16[400,256]{1,0:T(8,128)(2,1)S(1)} %collective-permute-done.11.refs_1_), channel_id=1, source_target_pairs={{0,120},{1,9},{2,122},{3,11},{4,124},{5,13},{6,126},{7,15},{8,0},{... | collective-permute-start | bytes 614408 | tf_op jit(solution)/shard_map/ppermute | solution.py:296
  94.4 8.4 %collective-permute-start.16 = (bf16[400,256]{1,0:T(8,128)(2,1)S(1)}, bf16[400,256]{1,0:T(8,128)(2,1)S(1)}, u32[]{:S(2)}, u32[]{:S(2)}) collective-permute-start(bf16[400,256]{1,0:T(8,128)(2,1)S(1)} %collective-permute-done.14.refs_1_), channel_id=1, source_target_pairs={{0,8},{1,121},{2,10},{3,123},{4,12},{5,125},{6,14},{7,127},{8,16},... | collective-permute-start | bytes 614408 | tf_op jit(solution)/shard_map/ppermute | solution.py:296
  95.7 8.4 %collective-permute-start.15 = (bf16[400,256]{1,0:T(8,128)(2,1)S(1)}, bf16[400,256]{1,0:T(8,128)(2,1)S(1)}, u32[]{:S(2)}, u32[]{:S(2)}) collective-permute-start(bf16[400,256]{1,0:T(8,128)(2,1)S(1)} %collective-permute-done.13.refs_1_), channel_id=1, source_target_pairs={{0,120},{1,9},{2,122},{3,11},{4,124},{5,13},{6,126},{7,15},{8,0},{... | collective-permute-start | bytes 614408 | tf_op jit(solution)/shard_map/ppermute | solution.py:296
  102.8 7.0 %collective-permute-start.18 = (bf16[400,256]{1,0:T(8,128)(2,1)S(1)}, bf16[400,256]{1,0:T(8,128)(2,1)S(1)}, u32[]{:S(2)}, u32[]{:S(2)}) collective-permute-start(bf16[400,256]{1,0:T(8,128)(2,1)S(1)} %collective-permute-done.16.refs_1_), channel_id=1, source_target_pairs={{0,8},{1,121},{2,10},{3,123},{4,12},{5,125},{6,14},{7,127},{8,16},... | collective-permute-start | bytes 614408 | tf_op jit(solution)/shard_map/ppermute | solution.py:296
  104.0 7.0 %collective-permute-start.17 = (bf16[400,256]{1,0:T(8,128)(2,1)S(1)}, bf16[400,256]{1,0:T(8,128)(2,1)S(1)}, u32[]{:S(2)}, u32[]{:S(2)}) collective-permute-start(bf16[400,256]{1,0:T(8,128)(2,1)S(1)} %collective-permute-done.15.refs_1_), channel_id=1, source_target_pairs={{0,120},{1,9},{2,122},{3,11},{4,124},{5,13},{6,126},{7,15},{8,0},{... | collective-permute-start | bytes 614408 | tf_op jit(solution)/shard_map/ppermute | solution.py:296
  115.8 8.5 %collective-permute-start.21 = (bf16[48,2048]{1,0:T(8,128)(2,1)S(1)}, bf16[48,2048]{1,0:T(8,128)(2,1)S(1)}, u32[]{:S(2)}, u32[]{:S(2)}) collective-permute-start(bf16[48,2048]{1,0:T(8,128)(2,1)S(1)} %get-tuple-element.196), channel_id=1, source_target_pairs={{0,2},{1,3},{2,4},{3,5},{4,6},{5,7},{6,0},{7,1},{8,10},{9,11},{10,... | collective-permute-start | bytes 589832 | tf_op jit(solution)/shard_map/ppermute | solution.py:286
  116.1 8.1 %collective-permute-start.25 = (bf16[48,2048]{1,0:T(8,128)(2,1)S(1)}, bf16[48,2048]{1,0:T(8,128)(2,1)S(1)}, u32[]{:S(2)}, u32[]{:S(2)}) collective-permute-start(bf16[48,2048]{1,0:T(8,128)(2,1)S(1)} %get-tuple-element.195), channel_id=1, source_target_pairs={{0,6},{1,7},{2,0},{3,1},{4,2},{5,3},{6,4},{7,5},{8,14},{9,15},{10,... | collective-permute-start | bytes 589832 | tf_op jit(solution)/shard_map/ppermute | solution.py:286
  124.4 9.0 %collective-permute-start.22 = (bf16[48,2048]{1,0:T(8,128)(2,1)S(1)}, bf16[48,2048]{1,0:T(8,128)(2,1)S(1)}, u32[]{:S(2)}, u32[]{:S(2)}) collective-permute-start(bf16[48,2048]{1,0:T(8,128)(2,1)S(1)} %get-tuple-element.190), channel_id=1, source_target_pairs={{0,2},{1,3},{2,4},{3,5},{4,6},{5,7},{6,0},{7,1},{8,10},{9,11},{10,... | collective-permute-start | bytes 589832 | tf_op jit(solution)/shard_map/ppermute | solution.py:286
  124.8 8.6 %collective-permute-start.26 = (bf16[48,2048]{1,0:T(8,128)(2,1)S(1)}, bf16[48,2048]{1,0:T(8,128)(2,1)S(1)}, u32[]{:S(2)}, u32[]{:S(2)}) collective-permute-start(bf16[48,2048]{1,0:T(8,128)(2,1)S(1)} %get-tuple-element.189), channel_id=1, source_target_pairs={{0,6},{1,7},{2,0},{3,1},{4,2},{5,3},{6,4},{7,5},{8,14},{9,15},{10,... | collective-permute-start | bytes 589832 | tf_op jit(solution)/shard_map/ppermute | solution.py:286
  127.8 8.5 %collective-permute-start.23 = (bf16[48,2048]{1,0:T(8,128)(2,1)S(1)}, bf16[48,2048]{1,0:T(8,128)(2,1)S(1)}, u32[]{:S(2)}, u32[]{:S(2)}) collective-permute-start(bf16[48,2048]{1,0:T(8,128)(2,1)S(1)} %get-tuple-element.192), channel_id=1, source_target_pairs={{0,2},{1,3},{2,4},{3,5},{4,6},{5,7},{6,0},{7,1},{8,10},{9,11},{10,... | collective-permute-start | bytes 589832 | tf_op jit(solution)/shard_map/ppermute | solution.py:286
  127.9 8.3 %collective-permute-start.24 = (bf16[48,2048]{1,0:T(8,128)(2,1)S(1)}, bf16[48,2048]{1,0:T(8,128)(2,1)S(1)}, u32[]{:S(2)}, u32[]{:S(2)}) collective-permute-start(bf16[48,2048]{1,0:T(8,128)(2,1)S(1)} %get-tuple-element.191), channel_id=1, source_target_pairs={{0,6},{1,7},{2,0},{3,1},{4,2},{5,3},{6,4},{7,5},{8,14},{9,15},{10,... | collective-permute-start | bytes 589832 | tf_op jit(solution)/shard_map/ppermute | solution.py:286
  (19 other events, 201.5 us)

commit v5 on v3

--- a/solution.py
+++ b/solution.py
@@ -228,8 +228,7 @@
     queries = q_ref.shape[0]
     width = 256
     if last:
-        for i in range(0, queries, width):
-            attend_block(q_ref, kv_refs, vt_refs, m_ref, l_ref, acc_ref, slice(i, i + width), latents)
+        attend_block(q_ref, kv_refs, vt_refs, m_ref, l_ref, acc_ref, slice(0, queries), latents)
         for h in range(queries // tok):
             cols = slice(h * tok, (h + 1) * tok)
             done = acc_ref[:, cols] / l_ref[0:1, cols]
@@ -352,7 +351,8 @@
     cos = jnp.concatenate([jnp.cos(row), jnp.cos(row), jnp.cos(col), jnp.cos(col)], axis=1)
     sin = jnp.concatenate([-jnp.sin(row), jnp.sin(row), -jnp.sin(col), jnp.sin(col)], axis=1)
 
-    gathered, rx, rc, w_kv, cos, sin = lax.optimization_barrier((gathered, rx, rc, w_kv, cos, sin))
+    w_other = other_core(w_out)
+    gathered, rx, rc, w_kv, cos, sin, w_other = lax.optimization_barrier((gathered, rx, rc, w_kv, cos, sin, w_other))
     summed = pl.pallas_call(
         sum_kernel,
         out_shape=jax.ShapeDtypeStruct((lines, 128), F32),
@@ -421,18 +421,17 @@
     theirs = lax.dynamic_index_in_dim(parts, 1 - core, 1, keepdims=False)
     far, near = (2,), (1, 3, 0)
 
-    def product(side, which):
+    def product(side, weights, which):
         rows = jnp.concatenate([side[i] for i in which]) if len(which) > 1 else side[which[0]]
-        return jnp.dot(rows, w_out, preferred_element_type=F32)
-
-    far_sent = other_core(product(theirs, far).astype(BF16))
-    far_sum = (product(mine, far) + far_sent.astype(F32)).astype(BF16)
-    theirs, far_sum = lax.optimization_barrier((theirs, far_sum))
-    near_sent = other_core(product(theirs, near).astype(BF16))
+        return jnp.dot(rows, weights, preferred_element_type=F32)
+
+    others = other_core(theirs)
+    own_far, own_near = lax.optimization_barrier((product(mine, w_out, far), product(mine, w_out, near)))
+    far_sum = (own_far + product(others, w_other, far)).astype(BF16)
     h = width // 2
     from_left = shifted(far_sum[:, :h], "tp", 2)
     from_right = shifted(far_sum[:, h:], "tp", -2)
-    near_sum = product(mine, near) + near_sent.astype(F32)
+    near_sum = own_near + product(others, w_other, near)
     nxt, prv, own = (near_sum[i * share:(i + 1) * share] for i in range(3))
     halves = (nxt[:, h:].astype(BF16), prv[:, :h].astype(BF16))
     a1 = shifted(halves[0], "tp", 2)

time: 137 us -> 135 us (0.985)
  starting transfers between devices: 67.5 us -> 63.8 us
  matrix products: 2.01 us -> 5.2 us
    ppermute x9, starting transfers between devices: 15.4 us -> 11.7 us  [shifted(): return lax.ppermute(x, axis, [(i, (i + by) % n) for i in range(n)])]
    dot_general x4, matrix products: 2.01 us -> 5.2 us  [product(): return jnp.dot(rows, weights, preferred_element_type=F32)]
    ppermute x3, waiting for transfers between devices: 2.85 us -> 1.45 us  [other_core(): return lax.ppermute(x, 'tp', [(i, i ^ 1) for i in range(n)])]
    unnamed x30 -> x22, local copies, waits for them, and re-layouts: 6.62 us -> 5.27 us
  transfers between devices with their start and end apart: 28 -> 28, of which waited for: 16 -> 19; matrix products, arithmetic and copies ran while one was open for 2% -> 4% of each run, Pallas kernels for 22% -> 23%
where the time goes in v5:
time: 135 us; the launch traced here: 134 us
  starting transfers between devices  63.8 us (47%)
  Pallas kernels  35 us (26%)
  waiting for transfers between devices  21.4 us (16%)
  local copies, waits for them, and re-layouts  5.39 us (4%)
  matrix products  5.2 us (4%)
  other arithmetic  3 us (2%)
    ppermute x15, starting transfers between devices, along_ring(): return lax.ppermute(x, ('sp', 'tp'), pairs)  27.8 us
    pallas_call x15, Pallas kernels, attend(): pl.pallas_call(kernel, out_shape=shapes, in_specs=[VM] * len(operands), o...  24.3 us
    all_to_all x1, starting transfers between devices, body(): lax.all_to_all(partial_mod, 'sp', split_axis=0, concat_axis=0, tiled=True)  24 us
    ppermute x9, waiting for transfers between devices, shifted(): return lax.ppermute(x, axis, [(i, (i + by) % n) for i in range(n)])  12.9 us
    ppermute x9, starting transfers between devices, shifted(): return lax.ppermute(x, axis, [(i, (i + by) % n) for i in range(n)])  11.7 us
    unnamed x22, local copies, waits for them, and re-layouts  5.27 us
    dot_general x4, matrix products, product(): return jnp.dot(rows, weights, preferred_element_type=F32)  5.2 us
    ppermute x15, waiting for transfers between devices, along_ring(): return lax.ppermute(x, ('sp', 'tp'), pairs)  3.87 us
  transfers between devices with their start and end apart: 28, of which 19 were waited for; matrix products, arithmetic and copies ran while one was open for 4% of the time, Pallas kernels for 23%

profile of v5, /device:TPU:40, one launch (start us, length us, event | category | flops | bytes accessed | tf_op | source)
XLA Modules:
  0.0 134.3 jit_solution(3255659028236117736)
XLA Ops:
  0.0 2.1 %modulation.1 = bf16[16,32,128]{2,1,0:T(8,128)(2,1)} custom-call(bf16[32,128]{1,0:T(8,128)(2,1)} %bitcast.40, bf16[32,128]{1,0:T(8,128)(2,1)} %bitcast.41, bf16[256,512]{1,0:T(8,128)(2,1)} %scale_hbm.1, bf16[256,512]{1,0:T(8,128)(2,1)} %shift_hbm.1, bf16[256,512]{1,0:T(8,128)(2,1)} %gate_hbm.1), custom_call_target="tpu_custom_call" | custom-call | tf_op jit(solution)/shard_map/modulation/pallas_call | solution.py:318
  2.2 24.0 %all-to-all-start = ((bf16[16,32,128]{2,1,0:T(8,128)(2,1)}), bf16[16,32,128]{2,1,0:T(8,128)(2,1)S(1)}, u32[]{:S(2)}, u32[]{:S(2)}) async-start(bf16[16,32,128]{2,1,0:T(8,128)(2,1)} %modulation.1), calls=%async_computation | async-start | bytes 262144 | tf_op jit(solution)/shard_map/all_to_all | solution.py:332
  26.2 1.9 %copy-done = bf16[384,4096]{1,0:T(8,128)(2,1)S(1)} copy-done((bf16[384,4096]{1,0:T(8,128)(2,1)S(1)}, bf16[384,4096]{1,0:T(8,128)(2,1)}, u32[]{:S(2)}) %copy-start) | copy-done | bytes 3145752
  31.4 3.5 %prepare.1 = (f32[384,128]{1,0:T(8,128)S(1)}, f32[16,128]{1,0:T(8,128)S(1)}, bf16[4096,256]{1,0:T(8,128)(2,1)S(1)}) custom-call(bf16[384,4096]{1,0:T(8,128)(2,1)S(1)} %copy-done, bf16[16,4096]{1,0:T(8,128)(2,1)S(1)} %copy-done.5, bf16[4096,128]{1,0:T(8,128)(2,1)S(1)} %copy-done.3, bf16[4096,128]{1,0:T(8,128)(2,1)S(1)} %copy-done.4), custom_call_target="tpu_custom_call" | custom-call | flops 1073741824 | bytes 12582912 | tf_op jit(solution)/shard_map/prepare/pallas_call | solution.py:333
  36.8 3.2 %all-to-all-done.in_ref = bf16[16,32,128]{2,1,0:T(8,128)(2,1)S(1)} async-done(((bf16[16,32,128]{2,1,0:T(8,128)(2,1)}), bf16[16,32,128]{2,1,0:T(8,128)(2,1)S(1)}, u32[]{:S(2)}, u32[]{:S(2)}) %all-to-all-start) | async-done | bytes 131104 | tf_op jit(solution)/shard_map/all_to_all | solution.py:332
  41.4 3.3 %collective-permute-start.4 = (f32[2,24,128]{2,1,0:T(8,128)S(1)}, f32[2,24,128]{2,1,0:T(8,128)S(1)}, u32[]{:S(2)}, u32[]{:S(2)}) collective-permute-start(f32[2,24,128]{2,1,0:T(8,128)S(1)} %pad_maximum_fusion.2.own_ref), channel_id=1, source_target_pairs={{0,4},{1,5},{2,6},{3,7},{4,0},{5,1},{6,2},{7,3},{8,12},{9,13},{10,... | collective-permute-start | bytes 73736 | tf_op jit(solution)/shard_map/ppermute | solution.py:286
  46.7 1.8 %collective-permute-done.3.m3_ref = f32[2,24,128]{2,1,0:T(8,128)S(1)} collective-permute-done((f32[2,24,128]{2,1,0:T(8,128)S(1)}, f32[2,24,128]{2,1,0:T(8,128)S(1)}, u32[]{:S(2)}, u32[]{:S(2)}) %collective-permute-start.3) | collective-permute-done | bytes 24608 | tf_op jit(solution)/shard_map/ppermute | solution.py:286
  48.5 2.2 %collective-permute-done.2.m1_ref = f32[2,24,128]{2,1,0:T(8,128)S(1)} collective-permute-done((f32[2,24,128]{2,1,0:T(8,128)S(1)}, f32[2,24,128]{2,1,0:T(8,128)S(1)}, u32[]{:S(2)}, u32[]{:S(2)}) %collective-permute-start.2) | collective-permute-done | bytes 24608 | tf_op jit(solution)/shard_map/ppermute | solution.py:286
  50.8 2.4 %project_kv.1 = (bf16[400,256]{1,0:T(8,128)(2,1)S(1)}, bf16[400,4096]{1,0:T(8,128)(2,1)S(1)}, f32[1,4096]{1,0:T(1,128)S(1)}) custom-call(bf16[384,4096]{1,0:T(8,128)(2,1)S(1)} %copy-done.1, bf16[16,4096]{1,0:T(8,128)(2,1)S(1)} %copy-done.6, f32[384,128]{1,0:T(8,128)S(1)} %get-tuple-element.101.rx_ref, f32[16,128]{1,0:T(8,128)S(1)} %get-tuple-element.102.rc_ref, ...), custom_call_target="tpu_custom_call" | custom-call | flops 805306368 | bytes 4194304 | tf_op jit(solution)/shard_map/project_kv/pallas_call | solution.py:369
  53.2 3.7 %collective-permute-start.5 = (bf16[400,256]{1,0:T(8,128)(2,1)S(1)}, bf16[400,256]{1,0:T(8,128)(2,1)S(1)}, u32[]{:S(2)}, u32[]{:S(2)}) collective-permute-start(bf16[400,256]{1,0:T(8,128)(2,1)S(1)} %get-tuple-element.109.refs_1_), channel_id=1, source_target_pairs={{0,120},{1,9},{2,122},{3,11},{4,124},{5,13},{6,126},{7,15},{8,0},{... | collective-permute-start | bytes 614408 | tf_op jit(solution)/shard_map/ppermute | solution.py:296
  56.9 1.7 %project_q.1.refs_0_ = bf16[768,128]{1,0:T(8,128)(2,1)S(1)} custom-call(bf16[400,4096]{1,0:T(8,128)(2,1)S(1)} %get-tuple-element.108.nm_ref, bf16[4096,256]{1,0:T(8,128)(2,1)S(1)} %copy-done.2, f32[1,128]{1,0:T(1,128)S(1)} %bitcast.38, f32[384,128]{1,0:T(8,128)S(1)} %pad_maximum_fusion.cos_ref, f32[384,128]{1,0:T(8,128)S(1)} %pad_maximum_fusion.1.sin_ref), custom_call_target="tpu_custom_call" | custom-call | flops 805306368 | bytes 4194304 | tf_op jit(solution)/shard_map/project_q/pallas_call | solution.py:391
  60.7 3.1 %collective-permute-start.6 = (bf16[400,256]{1,0:T(8,128)(2,1)S(1)}, bf16[400,256]{1,0:T(8,128)(2,1)S(1)}, u32[]{:S(2)}, u32[]{:S(2)}) collective-permute-start(bf16[400,256]{1,0:T(8,128)(2,1)S(1)} %collective-permute-done.5.refs_1_), channel_id=1, source_target_pairs={{0,120},{1,9},{2,122},{3,11},{4,124},{5,13},{6,126},{7,15},{8,0},{... | collective-permute-start | bytes 614408 | tf_op jit(solution)/shard_map/ppermute | solution.py:296
  68.0 3.7 %collective-permute-start.8 = (bf16[400,256]{1,0:T(8,128)(2,1)S(1)}, bf16[400,256]{1,0:T(8,128)(2,1)S(1)}, u32[]{:S(2)}, u32[]{:S(2)}) collective-permute-start(bf16[400,256]{1,0:T(8,128)(2,1)S(1)} %collective-permute-done.6.refs_1_), channel_id=1, source_target_pairs={{0,120},{1,9},{2,122},{3,11},{4,124},{5,13},{6,126},{7,15},{8,0},{... | collective-permute-start | bytes 614408 | tf_op jit(solution)/shard_map/ppermute | solution.py:296
  75.7 3.3 %collective-permute-start.10 = (bf16[400,256]{1,0:T(8,128)(2,1)S(1)}, bf16[400,256]{1,0:T(8,128)(2,1)S(1)}, u32[]{:S(2)}, u32[]{:S(2)}) collective-permute-start(bf16[400,256]{1,0:T(8,128)(2,1)S(1)} %collective-permute-done.8.refs_1_), channel_id=1, source_target_pairs={{0,120},{1,9},{2,122},{3,11},{4,124},{5,13},{6,126},{7,15},{8,0},{... | collective-permute-start | bytes 614408 | tf_op jit(solution)/shard_map/ppermute | solution.py:296
  83.2 3.3 %collective-permute-start.12 = (bf16[400,256]{1,0:T(8,128)(2,1)S(1)}, bf16[400,256]{1,0:T(8,128)(2,1)S(1)}, u32[]{:S(2)}, u32[]{:S(2)}) collective-permute-start(bf16[400,256]{1,0:T(8,128)(2,1)S(1)} %collective-permute-done.10.refs_1_), channel_id=1, source_target_pairs={{0,120},{1,9},{2,122},{3,11},{4,124},{5,13},{6,126},{7,15},{8,0},{... | collective-permute-start | bytes 614408 | tf_op jit(solution)/shard_map/ppermute | solution.py:296
  88.5 1.6 %attend.23 = (f32[8,768]{1,0:T(8,128)S(1)}, f32[8,768]{1,0:T(8,128)S(1)}, f32[128,768]{1,0:T(8,128)S(1)}) custom-call(bf16[768,128]{1,0:T(8,128)(2,1)S(1)} %project_q.1.refs_0_, bf16[400,256]{1,0:T(8,128)(2,1)S(1)} %collective-permute-done.13.refs_1_, ...), custom_call_target="tpu_custom_call", output_to_operand_aliasing={{0}: (2, {}), {1}: (3, {}), {2}: (4, {})} | custom-call | flops 157286400 | bytes 1048576 | tf_op jit(solution)/shard_map/attend/pallas_call | solution.py:271
  90.1 3.3 %collective-permute-start.14 = (bf16[400,256]{1,0:T(8,128)(2,1)S(1)}, bf16[400,256]{1,0:T(8,128)(2,1)S(1)}, u32[]{:S(2)}, u32[]{:S(2)}) collective-permute-start(bf16[400,256]{1,0:T(8,128)(2,1)S(1)} %collective-permute-done.12.refs_1_), channel_id=1, source_target_pairs={{0,120},{1,9},{2,122},{3,11},{4,124},{5,13},{6,126},{7,15},{8,0},{... | collective-permute-start | bytes 614408 | tf_op jit(solution)/shard_map/ppermute | solution.py:296
  97.1 3.3 %collective-permute-start.16 = (bf16[400,256]{1,0:T(8,128)(2,1)S(1)}, bf16[400,256]{1,0:T(8,128)(2,1)S(1)}, u32[]{:S(2)}, u32[]{:S(2)}) collective-permute-start(bf16[400,256]{1,0:T(8,128)(2,1)S(1)} %collective-permute-done.14.refs_1_), channel_id=1, source_target_pairs={{0,120},{1,9},{2,122},{3,11},{4,124},{5,13},{6,126},{7,15},{8,0},{... | collective-permute-start | bytes 614408 | tf_op jit(solution)/shard_map/ppermute | solution.py:296
  104.1 3.6 %collective-permute-start.18 = (bf16[400,256]{1,0:T(8,128)(2,1)S(1)}, bf16[400,256]{1,0:T(8,128)(2,1)S(1)}, u32[]{:S(2)}, u32[]{:S(2)}) collective-permute-start(bf16[400,256]{1,0:T(8,128)(2,1)S(1)} %collective-permute-done.16.refs_1_), channel_id=1, source_target_pairs={{0,120},{1,9},{2,122},{3,11},{4,124},{5,13},{6,126},{7,15},{8,0},{... | collective-permute-start | bytes 614408 | tf_op jit(solution)/shard_map/ppermute | solution.py:296
  113.6 2.1 %fusion = bf16[48,4096]{1,0:T(8,128)(2,1)S(1)} fusion(f32[48,4096]{1,0:T(8,128)S(1)} %fusion.20, bf16[256,4096]{1,0:T(8,128)(2,1)} %collective-permute-done, bf16[4,48,256]{2,1,0:T(8,128)(2,1)S(1)} %collective-permute-done.20), kind=kOutput, calls=%fused_computation.2 | convolution fusion | flops 101056512 | bytes 3301376 | tf_op jit(solution)/shard_map/dot_general | solution.py:426
  116.0 1.8 %collective-permute-start.21 = (bf16[48,2048]{1,0:T(8,128)(2,1)S(1)}, bf16[48,2048]{1,0:T(8,128)(2,1)S(1)}, u32[]{:S(2)}, u32[]{:S(2)}) collective-permute-start(bf16[48,2048]{1,0:T(8,128)(2,1)S(1)} %get-tuple-element.198), channel_id=1, source_target_pairs={{0,2},{1,3},{2,4},{3,5},{4,6},{5,7},{6,0},{7,1},{8,10},{9,11},{10,... | collective-permute-start | bytes 589832 | tf_op jit(solution)/shard_map/ppermute | solution.py:286
  117.8 2.2 %fusion.30 = (bf16[144,4096]{1,0:T(8,128)(2,1)S(1)}, f32[144,4096]{1,0:T(8,128)S(1)}) fusion(f32[144,4096]{1,0:T(8,128)S(1)} %fusion.7, bf16[256,4096]{1,0:T(8,128)(2,1)} %collective-permute-done, bf16[48,256]{1,0:T(8,128)(2,1)S(1)} %get-tuple-element.202, bf16[48,256]{1,0:T(8,128)(2,1)S(1)} %get-tuple-element.203, bf16[48,256]{1,0:T(8,128)(2,1)S(1)} %get-tuple-element.201), kind=kOutput, calls=%fused_computation.64 | convolution fusion | flops 303390720 | bytes 8069120 | tf_op jit(solution)/shard_map/dot_general | solution.py:426
  127.8 2.7 %collective-permute-done.23 = bf16[48,2048]{1,0:T(8,128)(2,1)S(1)} collective-permute-done((bf16[48,2048]{1,0:T(8,128)(2,1)S(1)}, bf16[48,2048]{1,0:T(8,128)(2,1)S(1)}, u32[]{:S(2)}, u32[]{:S(2)}) %collective-permute-start.23) | collective-permute-done | bytes 196640 | tf_op jit(solution)/shard_map/ppermute | solution.py:286
  131.2 2.1 %collective-permute-done.22 = bf16[48,2048]{1,0:T(8,128)(2,1)S(1)} collective-permute-done((bf16[48,2048]{1,0:T(8,128)(2,1)S(1)}, bf16[48,2048]{1,0:T(8,128)(2,1)S(1)}, u32[]{:S(2)}, u32[]{:S(2)}) %collective-permute-start.22) | collective-permute-done | bytes 196640 | tf_op jit(solution)/shard_map/ppermute | solution.py:286
  (94 shorter events, 47.8 us)
Async XLA Ops:
  0.0 40.0 %collective-permute-start = (bf16[256,4096]{1,0:T(8,128)(2,1)}, bf16[256,4096]{1,0:T(8,128)(2,1)}, u32[]{:S(2)}, u32[]{:S(2)}) collective-permute-start(bf16[256,4096]{1,0:T(8,128)(2,1)} %param.27), channel_id=1, source_target_pairs={{0,1},{1,0},{2,3},{3,2},{4,5},{5,4},{6,7},{7,6},{8,9},{9,8},{10,11... | collective-permute-start | bytes 6291464 | tf_op jit(solution)/shard_map/ppermute | solution.py:301
  2.2 37.9 %all-to-all-start = ((bf16[16,32,128]{2,1,0:T(8,128)(2,1)}), bf16[16,32,128]{2,1,0:T(8,128)(2,1)S(1)}, u32[]{:S(2)}, u32[]{:S(2)}) async-start(bf16[16,32,128]{2,1,0:T(8,128)(2,1)} %modulation.1), calls=%async_computation | async-start | bytes 262144 | tf_op jit(solution)/shard_map/all_to_all | solution.py:332
  41.4 5.3 %collective-permute-start.4 = (f32[2,24,128]{2,1,0:T(8,128)S(1)}, f32[2,24,128]{2,1,0:T(8,128)S(1)}, u32[]{:S(2)}, u32[]{:S(2)}) collective-permute-start(f32[2,24,128]{2,1,0:T(8,128)S(1)} %pad_maximum_fusion.2.own_ref), channel_id=1, source_target_pairs={{0,4},{1,5},{2,6},{3,7},{4,0},{5,1},{6,2},{7,3},{8,12},{9,13},{10,... | collective-permute-start | bytes 73736 | tf_op jit(solution)/shard_map/ppermute | solution.py:286
  53.2 7.6 %collective-permute-start.5 = (bf16[400,256]{1,0:T(8,128)(2,1)S(1)}, bf16[400,256]{1,0:T(8,128)(2,1)S(1)}, u32[]{:S(2)}, u32[]{:S(2)}) collective-permute-start(bf16[400,256]{1,0:T(8,128)(2,1)S(1)} %get-tuple-element.109.refs_1_), channel_id=1, source_target_pairs={{0,120},{1,9},{2,122},{3,11},{4,124},{5,13},{6,126},{7,15},{8,0},{... | collective-permute-start | bytes 614408 | tf_op jit(solution)/shard_map/ppermute | solution.py:296
  56.9 8.6 %collective-permute-start.7 = (bf16[400,256]{1,0:T(8,128)(2,1)S(1)}, bf16[400,256]{1,0:T(8,128)(2,1)S(1)}, u32[]{:S(2)}, u32[]{:S(2)}) collective-permute-start(bf16[400,256]{1,0:T(8,128)(2,1)S(1)} %get-tuple-element.109.refs_1_), channel_id=1, source_target_pairs={{0,8},{1,121},{2,10},{3,123},{4,12},{5,125},{6,14},{7,127},{8,16},... | collective-permute-start | bytes 614408 | tf_op jit(solution)/shard_map/ppermute | solution.py:296
  60.7 7.3 %collective-permute-start.6 = (bf16[400,256]{1,0:T(8,128)(2,1)S(1)}, bf16[400,256]{1,0:T(8,128)(2,1)S(1)}, u32[]{:S(2)}, u32[]{:S(2)}) collective-permute-start(bf16[400,256]{1,0:T(8,128)(2,1)S(1)} %collective-permute-done.5.refs_1_), channel_id=1, source_target_pairs={{0,120},{1,9},{2,122},{3,11},{4,124},{5,13},{6,126},{7,15},{8,0},{... | collective-permute-start | bytes 614408 | tf_op jit(solution)/shard_map/ppermute | solution.py:296
  65.5 8.6 %collective-permute-start.9 = (bf16[400,256]{1,0:T(8,128)(2,1)S(1)}, bf16[400,256]{1,0:T(8,128)(2,1)S(1)}, u32[]{:S(2)}, u32[]{:S(2)}) collective-permute-start(bf16[400,256]{1,0:T(8,128)(2,1)S(1)} %collective-permute-done.7.refs_1_), channel_id=1, source_target_pairs={{0,8},{1,121},{2,10},{3,123},{4,12},{5,125},{6,14},{7,127},{8,16},... | collective-permute-start | bytes 614408 | tf_op jit(solution)/shard_map/ppermute | solution.py:296
  68.0 7.7 %collective-permute-start.8 = (bf16[400,256]{1,0:T(8,128)(2,1)S(1)}, bf16[400,256]{1,0:T(8,128)(2,1)S(1)}, u32[]{:S(2)}, u32[]{:S(2)}) collective-permute-start(bf16[400,256]{1,0:T(8,128)(2,1)S(1)} %collective-permute-done.6.refs_1_), channel_id=1, source_target_pairs={{0,120},{1,9},{2,122},{3,11},{4,124},{5,13},{6,126},{7,15},{8,0},{... | collective-permute-start | bytes 614408 | tf_op jit(solution)/shard_map/ppermute | solution.py:296
  74.1 7.4 %collective-permute-start.11 = (bf16[400,256]{1,0:T(8,128)(2,1)S(1)}, bf16[400,256]{1,0:T(8,128)(2,1)S(1)}, u32[]{:S(2)}, u32[]{:S(2)}) collective-permute-start(bf16[400,256]{1,0:T(8,128)(2,1)S(1)} %collective-permute-done.9.refs_1_), channel_id=1, source_target_pairs={{0,8},{1,121},{2,10},{3,123},{4,12},{5,125},{6,14},{7,127},{8,16},... | collective-permute-start | bytes 614408 | tf_op jit(solution)/shard_map/ppermute | solution.py:296
  75.7 7.4 %collective-permute-start.10 = (bf16[400,256]{1,0:T(8,128)(2,1)S(1)}, bf16[400,256]{1,0:T(8,128)(2,1)S(1)}, u32[]{:S(2)}, u32[]{:S(2)}) collective-permute-start(bf16[400,256]{1,0:T(8,128)(2,1)S(1)} %collective-permute-done.8.refs_1_), channel_id=1, source_target_pairs={{0,120},{1,9},{2,122},{3,11},{4,124},{5,13},{6,126},{7,15},{8,0},{... | collective-permute-start | bytes 614408 | tf_op jit(solution)/shard_map/ppermute | solution.py:296
  81.5 7.0 %collective-permute-start.13 = (bf16[400,256]{1,0:T(8,128)(2,1)S(1)}, bf16[400,256]{1,0:T(8,128)(2,1)S(1)}, u32[]{:S(2)}, u32[]{:S(2)}) collective-permute-start(bf16[400,256]{1,0:T(8,128)(2,1)S(1)} %collective-permute-done.11.refs_1_), channel_id=1, source_target_pairs={{0,8},{1,121},{2,10},{3,123},{4,12},{5,125},{6,14},{7,127},{8,16},... | collective-permute-start | bytes 614408 | tf_op jit(solution)/shard_map/ppermute | solution.py:296
  83.2 7.0 %collective-permute-start.12 = (bf16[400,256]{1,0:T(8,128)(2,1)S(1)}, bf16[400,256]{1,0:T(8,128)(2,1)S(1)}, u32[]{:S(2)}, u32[]{:S(2)}) collective-permute-start(bf16[400,256]{1,0:T(8,128)(2,1)S(1)} %collective-permute-done.10.refs_1_), channel_id=1, source_target_pairs={{0,120},{1,9},{2,122},{3,11},{4,124},{5,13},{6,126},{7,15},{8,0},{... | collective-permute-start | bytes 614408 | tf_op jit(solution)/shard_map/ppermute | solution.py:296
  88.5 7.0 %collective-permute-start.15 = (bf16[400,256]{1,0:T(8,128)(2,1)S(1)}, bf16[400,256]{1,0:T(8,128)(2,1)S(1)}, u32[]{:S(2)}, u32[]{:S(2)}) collective-permute-start(bf16[400,256]{1,0:T(8,128)(2,1)S(1)} %collective-permute-done.13.refs_1_), channel_id=1, source_target_pairs={{0,8},{1,121},{2,10},{3,123},{4,12},{5,125},{6,14},{7,127},{8,16},... | collective-permute-start | bytes 614408 | tf_op jit(solution)/shard_map/ppermute | solution.py:296
  90.1 7.0 %collective-permute-start.14 = (bf16[400,256]{1,0:T(8,128)(2,1)S(1)}, bf16[400,256]{1,0:T(8,128)(2,1)S(1)}, u32[]{:S(2)}, u32[]{:S(2)}) collective-permute-start(bf16[400,256]{1,0:T(8,128)(2,1)S(1)} %collective-permute-done.12.refs_1_), channel_id=1, source_target_pairs={{0,120},{1,9},{2,122},{3,11},{4,124},{5,13},{6,126},{7,15},{8,0},{... | collective-permute-start | bytes 614408 | tf_op jit(solution)/shard_map/ppermute | solution.py:296
  95.5 7.0 %collective-permute-start.17 = (bf16[400,256]{1,0:T(8,128)(2,1)S(1)}, bf16[400,256]{1,0:T(8,128)(2,1)S(1)}, u32[]{:S(2)}, u32[]{:S(2)}) collective-permute-start(bf16[400,256]{1,0:T(8,128)(2,1)S(1)} %collective-permute-done.15.refs_1_), channel_id=1, source_target_pairs={{0,8},{1,121},{2,10},{3,123},{4,12},{5,125},{6,14},{7,127},{8,16},... | collective-permute-start | bytes 614408 | tf_op jit(solution)/shard_map/ppermute | solution.py:296
  97.1 7.0 %collective-permute-start.16 = (bf16[400,256]{1,0:T(8,128)(2,1)S(1)}, bf16[400,256]{1,0:T(8,128)(2,1)S(1)}, u32[]{:S(2)}, u32[]{:S(2)}) collective-permute-start(bf16[400,256]{1,0:T(8,128)(2,1)S(1)} %collective-permute-done.14.refs_1_), channel_id=1, source_target_pairs={{0,120},{1,9},{2,122},{3,11},{4,124},{5,13},{6,126},{7,15},{8,0},{... | collective-permute-start | bytes 614408 | tf_op jit(solution)/shard_map/ppermute | solution.py:296
  102.4 7.0 %collective-permute-start.19 = (bf16[400,256]{1,0:T(8,128)(2,1)S(1)}, bf16[400,256]{1,0:T(8,128)(2,1)S(1)}, u32[]{:S(2)}, u32[]{:S(2)}) collective-permute-start(bf16[400,256]{1,0:T(8,128)(2,1)S(1)} %collective-permute-done.17.refs_1_), channel_id=1, source_target_pairs={{0,8},{1,121},{2,10},{3,123},{4,12},{5,125},{6,14},{7,127},{8,16},... | collective-permute-start | bytes 614408 | tf_op jit(solution)/shard_map/ppermute | solution.py:296
  104.1 7.0 %collective-permute-start.18 = (bf16[400,256]{1,0:T(8,128)(2,1)S(1)}, bf16[400,256]{1,0:T(8,128)(2,1)S(1)}, u32[]{:S(2)}, u32[]{:S(2)}) collective-permute-start(bf16[400,256]{1,0:T(8,128)(2,1)S(1)} %collective-permute-done.16.refs_1_), channel_id=1, source_target_pairs={{0,120},{1,9},{2,122},{3,11},{4,124},{5,13},{6,126},{7,15},{8,0},{... | collective-permute-start | bytes 614408 | tf_op jit(solution)/shard_map/ppermute | solution.py:296
  115.7 7.5 %collective-permute-start.25 = (bf16[48,2048]{1,0:T(8,128)(2,1)S(1)}, bf16[48,2048]{1,0:T(8,128)(2,1)S(1)}, u32[]{:S(2)}, u32[]{:S(2)}) collective-permute-start(bf16[48,2048]{1,0:T(8,128)(2,1)S(1)} %get-tuple-element.197), channel_id=1, source_target_pairs={{0,6},{1,7},{2,0},{3,1},{4,2},{5,3},{6,4},{7,5},{8,14},{9,15},{10,... | collective-permute-start | bytes 589832 | tf_op jit(solution)/shard_map/ppermute | solution.py:286
  116.0 8.2 %collective-permute-start.21 = (bf16[48,2048]{1,0:T(8,128)(2,1)S(1)}, bf16[48,2048]{1,0:T(8,128)(2,1)S(1)}, u32[]{:S(2)}, u32[]{:S(2)}) collective-permute-start(bf16[48,2048]{1,0:T(8,128)(2,1)S(1)} %get-tuple-element.198), channel_id=1, source_target_pairs={{0,2},{1,3},{2,4},{3,5},{4,6},{5,7},{6,0},{7,1},{8,10},{9,11},{10,... | collective-permute-start | bytes 589832 | tf_op jit(solution)/shard_map/ppermute | solution.py:286
  120.1 7.8 %collective-permute-start.24 = (bf16[48,2048]{1,0:T(8,128)(2,1)S(1)}, bf16[48,2048]{1,0:T(8,128)(2,1)S(1)}, u32[]{:S(2)}, u32[]{:S(2)}) collective-permute-start(bf16[48,2048]{1,0:T(8,128)(2,1)S(1)} %get-tuple-element.193), channel_id=1, source_target_pairs={{0,6},{1,7},{2,0},{3,1},{4,2},{5,3},{6,4},{7,5},{8,14},{9,15},{10,... | collective-permute-start | bytes 589832 | tf_op jit(solution)/shard_map/ppermute | solution.py:286
  121.6 8.9 %collective-permute-start.23 = (bf16[48,2048]{1,0:T(8,128)(2,1)S(1)}, bf16[48,2048]{1,0:T(8,128)(2,1)S(1)}, u32[]{:S(2)}, u32[]{:S(2)}) collective-permute-start(bf16[48,2048]{1,0:T(8,128)(2,1)S(1)} %get-tuple-element.194), channel_id=1, source_target_pairs={{0,2},{1,3},{2,4},{3,5},{4,6},{5,7},{6,0},{7,1},{8,10},{9,11},{10,... | collective-permute-start | bytes 589832 | tf_op jit(solution)/shard_map/ppermute | solution.py:286
  124.2 7.0 %collective-permute-start.26 = (bf16[48,2048]{1,0:T(8,128)(2,1)S(1)}, bf16[48,2048]{1,0:T(8,128)(2,1)S(1)}, u32[]{:S(2)}, u32[]{:S(2)}) collective-permute-start(bf16[48,2048]{1,0:T(8,128)(2,1)S(1)} %get-tuple-element.191), channel_id=1, source_target_pairs={{0,6},{1,7},{2,0},{3,1},{4,2},{5,3},{6,4},{7,5},{8,14},{9,15},{10,... | collective-permute-start | bytes 589832 | tf_op jit(solution)/shard_map/ppermute | solution.py:286
  125.0 8.4 %collective-permute-start.22 = (bf16[48,2048]{1,0:T(8,128)(2,1)S(1)}, bf16[48,2048]{1,0:T(8,128)(2,1)S(1)}, u32[]{:S(2)}, u32[]{:S(2)}) collective-permute-start(bf16[48,2048]{1,0:T(8,128)(2,1)S(1)} %get-tuple-element.192), channel_id=1, source_target_pairs={{0,2},{1,3},{2,4},{3,5},{4,6},{5,7},{6,0},{7,1},{8,10},{9,11},{10,... | collective-permute-start | bytes 589832 | tf_op jit(solution)/shard_map/ppermute | solution.py:286
  (15 other events, 76.7 us)
